TPU v7x, 512 devices: a whole 4x8x8 slice. The times are simulated.
512 devices in a mesh: sp: 64 (over z, y), tp: 8 (over x, core).
Axes of the slice: x: 4, y: 8, z: 8, core: 2. Of those that a mesh axis runs over, the one named last changes fastest.
Arguments:
- inputs: bfloat16 [16384, 2048], P('sp', 'tp'), may hold values from -200 to 200
- input_gain: bfloat16 [2048], P('tp'), may hold values from 0.099609375 to 1.8984375
- stick_query_w: bfloat16 [2048, 1024], P(None, 'tp'), may hold values from -0.3125 to 0.3125
- stick_key_w: bfloat16 [2048, 1024], P(None, 'tp'), may hold values from -0.125 to 0.125
- stick_value_w: bfloat16 [2048, 1024], P(None, 'tp'), may hold values from -0.125 to 0.125
- ret_query_w: bfloat16 [2048, 2048], P(None, 'tp'), may hold values from -0.125 to 0.125
- ret_key_w: bfloat16 [2048, 2048], P(None, 'tp'), may hold values from -0.125 to 0.125
- ret_value_w: bfloat16 [2048, 2048], P(None, 'tp'), may hold values from -0.125 to 0.125
- stick_offset: float32 [8], P('tp'), may hold values from -17 to -2
- ret_log_decay: float32 [8], P('tp'), may hold values from -0.04 to 0, as said below
- initial_state: float32 [8, 256, 256], P('tp', 'sp'), may hold values from -76.8 to 76.8
- stick_gain: float32 [1024], P('tp'), may hold values from 0.1 to 1.9
- ret_gain: float32 [2048], P('tp'), may hold values from 0.1 to 1.9
- stick_out_w: bfloat16 [1024, 2048], P('tp', 'sp'), may hold values from -0.125 to 0.125
- ret_out_w: bfloat16 [2048, 2048], P('tp', 'sp'), may hold values from -0.09375 to 0.09375
Outputs:
- layer_out: bfloat16 [16384, 2048], P(('sp', 'tp'))
Inputs may be any that keep to these rules, and one draw needn't show every extreme that they name: `ret_log_decay`: every entry is negative.
All inputs are finite; a program needn't handle non-finite values.
Results may differ from a plain program's by a relative error of at most 0.017.
Values may be sent and summed in bfloat16 or wider, within the bound.
No kernel may reach another device: no remote copies, remote signals or barrier semaphores. Data moves between devices by JAX's collectives and lax.ppermute only.
A program may use at most 64 MiB of HBM per device.

v0:
```python
import jax
import jax.numpy as jnp
from jax import lax
from jax.sharding import Mesh
from jax.sharding import PartitionSpec as P

D = 2048
STICK_HEADS = 8
STICK_DIM = 128
SP = ("sp_0", "sp_1")
SP_TP = ("sp_0", "sp_1", "tp")


epsilon = 1e-06
rope_base = 10000.0


def sent_together(arrays, axis, dim, along):
    widths = [a.shape[along] for a in arrays]
    both = jnp.concatenate(arrays, axis=along)
    result = lax.all_gather(both, axis, axis=dim, tiled=True)
    return tuple(jnp.split(result, [sum(widths[:k]) for k in range(1, len(widths))], axis=along))


def neutral_like(x, identity):
    return jax.tree.map(
        lambda a, e: jnp.broadcast_to(jnp.asarray(e, a.dtype), a.shape), x, identity
    )


def prefix_by_axis(x, axes, combine, identity):
    before = start = neutral_like(x, identity)
    running = x
    for axis in reversed(axes):
        length, mine = (lax.axis_size(axis), lax.axis_index(axis))
        pieces = jax.tree.map(lambda part: lax.all_gather(part, axis), running)
        inside, running = (start, start)
        for k in range(length):
            passed = k < mine
            running = combine(running, jax.tree.map(lambda part: part[k], pieces))
            inside = jax.tree.map(lambda new, old: jnp.where(passed, new, old), running, inside)
        before = combine(inside, before)
    return before


def turned_gather(arrays, axis, dims):
    turned = [jnp.moveaxis(a, dim, 0) for a, dim in zip(arrays, dims)]
    widths = [t[0].size for t in turned]
    both = jnp.concatenate([t.reshape(-1, w) for t, w in zip(turned, widths)], axis=1)
    result = lax.all_gather(both, axis, axis=0, tiled=True)
    parts = jnp.split(result, [sum(widths[:k]) for k in range(1, len(widths))], axis=1)
    return tuple(
        (
            jnp.moveaxis(b.reshape(-1, *t.shape[1:]), 0, dim)
            for b, t, dim in zip(parts, turned, dims)
        )
    )


def in_blocks(x, dim, length):
    before, after = (x.shape[:dim], x.shape[dim + 1 :])
    return jnp.moveaxis(x.reshape(*before, length, -1, *after), dim, 0)


def summed_on_arrival(x, axis, dim):
    parts = in_blocks(x, dim, lax.axis_size(axis))
    arrived = lax.all_to_all(parts, axis, split_axis=0, concat_axis=0, tiled=True)
    return arrived.astype(jnp.float32).sum(axis=0)


def rotate(values, positions):
    half_width = values.shape[-1] // 2
    inverse = rope_base ** (-jnp.arange(half_width, dtype=jnp.float32) / half_width)
    angles = positions.astype(jnp.float32)[:, None] * inverse[None, :]
    cosine = jnp.cos(angles)[:, None, :]
    sine_table = jnp.sin(angles)[:, None, :]
    first_half = values[..., :half_width]
    second_half = values[..., half_width:]
    return jnp.concatenate(
        [
            first_half * cosine - second_half * sine_table,
            second_half * cosine + first_half * sine_table,
        ],
        axis=-1,
    )


def stick_block(partial_state, queries, key_rows, value_rows, offsets, query_pos, key_pos):
    running, before = partial_state
    score_scale = queries.shape[2] ** (-0.5)
    scores = (
        jnp.einsum("thd,shd->hts", queries, key_rows, preferred_element_type=jnp.float32)
        * score_scale
        + offsets[:, None, None]
    )
    allowed = ((key_pos[None, :] < query_pos[:, None]) & (key_pos[None, :] >= 0))[None]
    remain = jnp.where(allowed, jax.nn.log_sigmoid(-scores), 0.0)
    suffix = lax.cumsum(remain, axis=2, reverse=True) - remain + before[:, :, None]
    weights = jnp.where(allowed, jnp.exp(jax.nn.log_sigmoid(scores) + suffix), 0.0).astype(
        jnp.bfloat16
    )
    running = running + jnp.einsum(
        "hts,shd->thd", weights, value_rows, preferred_element_type=jnp.float32
    )
    return (running, before + jnp.sum(remain, axis=2))


def sweep_keys(keys_all, values_all, query_rows, positions, offsets, key_span):
    row_count, head_count, head_width = query_rows.shape
    span_offsets = jnp.arange(key_span, dtype=jnp.int32)
    needed = (positions[row_count - 1] + key_span) // key_span

    def visit(visit_index, partial_state):
        key_start = (needed - 1 - visit_index) * key_span
        key_rows = lax.dynamic_slice_in_dim(keys_all, key_start, key_span, 0).reshape(
            key_span, head_count, head_width
        )
        value_rows = lax.dynamic_slice_in_dim(values_all, key_start, key_span, 0).reshape(
            key_span, head_count, head_width
        )
        return stick_block(
            partial_state,
            query_rows,
            key_rows,
            value_rows,
            offsets,
            positions,
            key_start + span_offsets,
        )

    start_carry = (
        jnp.zeros((row_count, head_count, head_width), jnp.float32),
        jnp.zeros((head_count, row_count), jnp.float32),
    )
    final_state = lax.fori_loop(0, needed, visit, start_carry)
    return final_state[0]


def body(
    inputs,
    input_gain,
    stick_query_w,
    stick_key_w,
    stick_value_w,
    ret_query_w,
    ret_key_w,
    ret_value_w,
    stick_offset,
    ret_log_decay,
    initial_state,
    stick_gain,
    ret_gain,
    stick_out_w,
    ret_out_w,
):
    tok_rows = inputs.shape[0]
    matrices = (stick_query_w, stick_key_w, stick_value_w, ret_query_w, ret_key_w, ret_value_w)
    own_squares = jnp.sum(jnp.square(inputs.astype(jnp.float32)), axis=1)
    squares = lax.psum(own_squares, "tp")
    pieces = sent_together((inputs, input_gain[None, :]), "tp", 1, 0)
    scaled = (pieces[0].astype(jnp.float32) * pieces[1].astype(jnp.float32)).astype(jnp.bfloat16)
    projected = tuple(
        (jnp.dot(scaled, matrix, preferred_element_type=jnp.float32) for matrix in matrices)
    )
    row_scale = lax.rsqrt(squares / D + epsilon)
    stick_query, stick_key, stick_value, ret_query, ret_key, ret_value = tuple(
        ((running * row_scale[:, None]).astype(jnp.bfloat16) for running in projected)
    )
    head_count = stick_offset.shape[0]
    head_width = stick_query.shape[1] // head_count
    first_pos = lax.axis_index(SP) * tok_rows
    query_pos = first_pos + jnp.arange(tok_rows, dtype=jnp.int32)
    queries = stick_query.reshape(tok_rows, head_count, head_width)
    key_span = 4 * tok_rows
    keys_all, values_all = sent_together((stick_key, stick_value), SP, 0, 1)
    stick_total = sweep_keys(keys_all, values_all, queries, query_pos, stick_offset, key_span)
    stick_local = jnp.sum(jnp.square(stick_total), axis=(1, 2))
    stick_squares = lax.psum(stick_local, "tp")
    stick_scale = lax.rsqrt(stick_squares / (STICK_HEADS * STICK_DIM) + epsilon)
    stick_normed = (
        stick_total.reshape(tok_rows, head_count * head_width) * stick_scale[:, None] * stick_gain
    ).astype(jnp.bfloat16)
    state_full = lax.all_gather(initial_state, SP, axis=1, tiled=True)
    ret_heads = ret_log_decay.shape[0]
    ret_width = ret_query.shape[1] // ret_heads
    turned_query = rotate(
        ret_query.reshape(tok_rows, ret_heads, ret_width).astype(jnp.float32), query_pos
    )
    turned_key = rotate(
        ret_key.reshape(tok_rows, ret_heads, ret_width).astype(jnp.float32), query_pos
    ) * ret_width ** (-0.5)
    ret_values = ret_value.reshape(tok_rows, ret_heads, ret_width).astype(jnp.float32)
    local_pos = jnp.arange(tok_rows, dtype=jnp.float32)
    distance = local_pos[:, None] - local_pos[None, :]
    decay_mask = jnp.where(
        distance[None] >= 0.0,
        jnp.exp(ret_log_decay[:, None, None] * jnp.maximum(distance, 0.0)[None]),
        0.0,
    )
    highest = lax.Precision.HIGHEST
    scores = jnp.einsum("thd,shd->hts", turned_query, turned_key, precision=highest) * decay_mask
    inner_part = jnp.einsum("hts,she->the", scores, ret_values, precision=highest)
    key_decay = jnp.exp(ret_log_decay[None, :] * (tok_rows - 1.0 - local_pos[:, None]))
    own_state = jnp.einsum(
        "shd,she->hde", turned_key * key_decay[:, :, None], ret_values, precision=highest
    )
    block_decay = jnp.exp(ret_log_decay * tok_rows)

    def join_states(earlier, later):
        return (earlier[0] * later[1][:, None, None] + later[0], earlier[1] * later[1])

    prefix_state, _ = prefix_by_axis(
        (own_state, block_decay),
        SP,
        join_states,
        (jnp.zeros_like(own_state), jnp.ones_like(block_decay)),
    )
    entering = (
        prefix_state
        + jnp.exp(ret_log_decay * first_pos.astype(jnp.float32))[:, None, None] * state_full
    )
    query_decay = jnp.exp(ret_log_decay[None, :] * (local_pos[:, None] + 1.0))
    cross_part = (
        jnp.einsum("thd,hde->the", turned_query, entering, precision=highest)
        * query_decay[:, :, None]
    )
    ret_total = inner_part + cross_part
    centered = ret_total - jnp.mean(ret_total, axis=2, keepdims=True)
    normed = centered * lax.rsqrt(jnp.mean(centered * centered, axis=2, keepdims=True) + epsilon)
    ret_normed = (normed.reshape(tok_rows, ret_heads * ret_width) * ret_gain).astype(jnp.bfloat16)
    stick_cols, ret_cols = turned_gather((stick_out_w, ret_out_w), SP, (1, 1))
    stick_part = jnp.dot(stick_normed, stick_cols, preferred_element_type=jnp.float32)
    layer_sum = summed_on_arrival(
        (stick_part + jnp.dot(ret_normed, ret_cols, preferred_element_type=jnp.float32)).astype(
            jnp.bfloat16
        ),
        "tp",
        0,
    )
    return layer_sum.astype(jnp.bfloat16)


def solution(mesh):
    split = Mesh(mesh.devices.reshape(8, 8, mesh.shape["tp"]), ("sp_0", "sp_1", "tp"))
    in_specs = (
        P(SP, "tp"),
        P("tp"),
        P(None, "tp"),
        P(None, "tp"),
        P(None, "tp"),
        P(None, "tp"),
        P(None, "tp"),
        P(None, "tp"),
        P("tp"),
        P("tp"),
        P("tp", SP, None),
        P("tp"),
        P("tp"),
        P("tp", SP),
        P("tp", SP),
    )
    out_specs = P(SP_TP, None)
    return jax.shard_map(body, mesh=split, in_specs=in_specs, out_specs=out_specs, check_vma=False)
```

profile of v0, /device:TPU:504, one launch (start us, length us, event | category | flops | bytes accessed | tf_op | source)
XLA Modules:
  0.0 488.8 jit_solution(14377370868597560384)
XLA Ops:
  10.6 14.6 %psum.14 = f32[256]{0:T(256)S(1)} all-reduce(f32[256]{0:T(256)S(1)} %multiply_reduce_fusion.1), channel_id=1, replica_groups=mesh['sp_0'=8,'sp_1'=8,'tp'=8] {'tp'}, use_global_device_ids=true, to_apply=%region_1.0 | all-reduce | flops 256 | bytes 2048 | tf_op jit(solution)/shard_map/psum | solution.py:159
  25.3 11.8 %all-gather.9.cloned.1.call-done = bf16[257,2048]{1,0:T(8,128)(2,1)} async-done(((bf16[257,256]{1,0:T(8,128)(2,1)}), bf16[257,2048]{1,0:T(8,128)(2,1)}) %all-gather.9.cloned.1.call-update) | async-done | bytes 1052688 | tf_op jit(solution)/shard_map/all_gather | solution.py:21
  44.7 15.2 %all-reduce = f32[8]{0:T(128)S(1)} all-reduce(f32[8]{0:T(128)S(1)} %exponential_dynamic-update-slice_fusion), channel_id=2, replica_groups=mesh['sp_0'=8,'sp_1'=8,'tp'=8] {'sp_1'}, use_global_device_ids=true, to_apply=%add | all-reduce | flops 8 | bytes 64
  62.4 23.9 %all-gather.17.cloned.1.call-done = f32[2048,256]{1,0:T(8,128)} async-done(((f32[256,256]{1,0:T(8,128)}), f32[2048,256]{1,0:T(8,128)}) %all-gather.17.cloned.1.call-update) | async-done | bytes 2097168 | tf_op jit(solution)/shard_map/all_gather | solution.py:36
  86.3 6.7 %bitcast_add_fusion.5 = f32[1,1,256,256]{3,2,1,0:T(8,128)} fusion(f32[2048,256]{1,0:T(8,128)} %all-gather.17.cloned.1.call-done, f32[]{:T(128)} %bitcast.29, f32[]{:T(128)} %bitcast.27, f32[]{:T(128)} %bitcast.25, f32[]{:T(128)} %bitcast.23, f32[]{:T(128)} %bitcast.21, f32[]{:T(128)} %bitcast.20, f32[]{:T(128)} %bitcast.19, f32[]{:T(128)} %bitcast.18), kind=kLoop, calls=%fused_computation.93 | loop fusion | flops 983040 | bytes 2359328 | tf_op jit(solution)/shard_map/add | solution.py:210
  101.6 15.0 %all-reduce.1 = f32[8]{0:T(128)S(1)} all-reduce(f32[8]{0:T(128)S(1)} %dynamic-update-slice.1), channel_id=3, replica_groups=mesh['sp_0'=8,'sp_1'=8,'tp'=8] {'sp_0'}, use_global_device_ids=true, to_apply=%add.1 | all-reduce | flops 8 | bytes 64
  118.0 49.0 %all_gather.44 = f32[1,256,256]{2,0,1:T(1,128)S(1)} all-gather(f32[1,4,256]{2,0,1:T(1,128)S(1)} %copy.40), channel_id=1, replica_groups=mesh['sp_0'=8,'sp_1'=8,'tp'=8] {'sp_0','sp_1'}, dimensions={1}, use_global_device_ids=true | all-gather | bytes 266240 | tf_op jit(solution)/shard_map/all_gather | solution.py:183
  175.0 11.8 %fusion.155 = (f32[256]{0:T(256)S(1)}, f32[1,256,256]{2,1,0:T(8,128)S(1)}) fusion(f32[1,256,256]{2,1,0:T(8,128)S(1)} %convolution_bitcast_fusion.2, f32[256]{0:T(256)S(1)} %multiply_exponential_fusion, f32[256,1,128]{2,0,1:T(8,128)S(1)} %get-tuple-element.211, f32[256,1,128]{2,0,1:T(8,128)S(1)} %get-tuple-element.210, ...), kind=kOutput, calls=%fused_computation.219 | convolution fusion | flops 204865280 | bytes 5245016 | tf_op jit(solution)/shard_map/thd,hde->the/dot_general | solution.py:224
  188.0 54.7 %all-gather.11.cloned.1.call-done = bf16[16384,256]{0,1:T(8,128)(2,1)} async-done(((bf16[256,256]{0,1:T(8,128)(2,1)}), bf16[16384,256]{0,1:T(8,128)(2,1)}) %all-gather.11.cloned.1.call-update) | async-done | bytes 8388624 | tf_op jit(solution)/shard_map/all_gather | solution.py:21
  242.8 5.8 %fusion.153 = (bf16[16384,128]{0,1:T(8,128)(2,1)}, bf16[16384,128]{0,1:T(8,128)(2,1)}) fusion(bf16[16384,256]{0,1:T(8,128)(2,1)} %all-gather.11.cloned.1.call-done), kind=kLoop, calls=%fused_computation.217 | loop fusion | bytes 16777216 | tf_op jit(solution)/shard_map/split | solution.py:22
  249.1 199.1 %while.15 = (s32[]{:T(128)}, f32[256,1,128]{0,2,1:T(8,128)S(1)}, f32[1,256]{1,0:T(1,128)}, s32[]{:T(128)}, s32[]{:T(128)}, /*index=5*/bf16[16384,128]{0,1:T(8,12...) while((s32[]{:T(128)}, f32[256,1,128]{0,2,1:T(8,128)S(1)}, ...), condition=%wide.region_6.7_spmd.clone, body=%wide.region_2.6_spmd.clone.sunk | while | flops 175164416 | bytes 11457415 | solution.py:135
  249.2 4.0 fusion.176
  253.2 2.5 fusion.177
  261.6 4.0 fusion.176
  274.1 4.0 fusion.176
  278.1 2.5 fusion.177
  286.5 4.0 fusion.176
  298.9 4.0 fusion.176
  303.0 2.5 fusion.177
  311.4 4.0 fusion.176
  323.8 4.0 fusion.176
  336.3 4.0 fusion.176
  348.7 4.0 fusion.176
  361.2 4.0 fusion.176
  373.6 4.0 fusion.176
  386.1 4.0 fusion.176
  398.5 4.0 fusion.176
  411.0 4.0 fusion.176
  423.4 4.0 fusion.176
  435.9 4.0 fusion.176
  448.3 12.4 %psum.15 = f32[256]{0:T(256)S(1)} all-reduce(f32[256]{0:T(256)S(1)} %multiply_reduce_fusion.2), channel_id=1, replica_groups=mesh['sp_0'=8,'sp_1'=8,'tp'=8] {'tp'}, use_global_device_ids=true, to_apply=%region_8.9 | all-reduce | flops 256 | bytes 2048 | tf_op jit(solution)/shard_map/psum | solution.py:178
  463.1 18.4 %all_to_all.5 = bf16[8,32,2048]{2,1,0:T(8,128)(2,1)S(1)} all-to-all(bf16[8,32,2048]{2,1,0:T(8,128)(2,1)S(1)} %bitcast.246), channel_id=1, replica_groups=mesh['sp_0'=8,'sp_1'=8,'tp'=8] {'tp'}, dimensions={0} | all-to-all | bytes 2097152 | tf_op jit(solution)/shard_map/all_to_all | solution.py:67
  (445 shorter events, 155.1 us)
Async XLA Ops:
  6.5 31.5 %copy-start = (bf16[2048,256]{1,0:T(8,128)(2,1)S(1)}, bf16[2048,256]{1,0:T(8,128)(2,1)}, u32[]{:S(2)}) copy-start(bf16[2048,256]{1,0:T(8,128)(2,1)} %param.23) | copy-start | bytes 3145732
  6.5 30.6 %all-gather.9.cloned.1.call-start = ((), (), s32[]{:S(2)}) async-start(), calls=%async_computation.1 | async-start | bytes 1216512 | tf_op jit(solution)/shard_map/all_gather | solution.py:21
  8.9 77.4 %all-gather.17.cloned.1.call-start = ((), (), s32[]{:S(2)}) async-start(), calls=%async_computation.5 | async-start | bytes 2359296 | tf_op jit(solution)/shard_map/all_gather | solution.py:36
  42.6 132.4 %all-gather.15.cloned.1.call-start = ((), (), s32[]{:S(2)}) async-start(), calls=%async_computation.4 | async-start | bytes 2359296 | tf_op jit(solution)/shard_map/all_gather | solution.py:36
  93.0 25.0 %copy-start.13 = (f32[1,4,256]{2,1,0:T(4,128)S(1)}, f32[1,4,256]{2,1,0:T(4,128)}, u32[]{:S(2)}) copy-start(f32[1,4,256]{2,1,0:T(4,128)} %param.27) | copy-start | bytes 12292
  93.0 149.7 %all-gather.11.cloned.1.call-start = ((), (), s32[]{:S(2)}) async-start(), calls=%async_computation.2 | async-start | bytes 8519680 | tf_op jit(solution)/shard_map/all_gather | solution.py:21
  96.8 363.9 %all-gather.13.cloned.1.call-start = ((), (), s32[]{:S(2)}) async-start(), calls=%async_computation.3 | async-start | bytes 1597440 | tf_op jit(solution)/shard_map/all_gather | solution.py:50
  249.1 4.0 copy-start.2
  261.6 4.0 copy-start.2
  274.0 4.0 copy-start.2
  286.5 4.0 copy-start.2
  286.5 4.0 copy-start.5
  298.9 4.0 copy-start.2
  298.9 4.0 copy-start.5
  311.4 4.0 copy-start.2
  323.8 4.0 copy-start.2
  336.2 4.0 copy-start.2
  348.7 4.0 copy-start.2
  348.7 4.0 copy-start.5
  361.1 4.0 copy-start.2
  373.6 4.0 copy-start.2
  373.6 4.0 copy-start.5
  386.0 4.0 copy-start.2
  398.5 4.0 copy-start.2
  398.5 4.0 copy-start.5
  410.9 4.0 copy-start.2
  423.4 4.0 copy-start.2
  423.4 4.0 copy-start.5
  435.8 4.0 copy-start.2
  448.3 14.2 %copy-start.10 = (f32[256]{0:T(256)S(1)}, f32[256]{0:T(256)}, u32[]{:S(2)}) copy-start(f32[256]{0:T(256)} %copy-done.9) | copy-start | bytes 3076
  448.3 14.2 %copy-start.12 = (f32[256]{0:T(256)S(1)}, f32[256]{0:T(256)}, u32[]{:S(2)}) copy-start(f32[256]{0:T(256)} %add_rsqrt_fusion) | copy-start | bytes 3076
  448.3 14.2 %copy-start.14 = (f32[256]{0:T(256)S(1)}, f32[256]{0:T(256)}, u32[]{:S(2)}) copy-start(f32[256]{0:T(256)} %param.29) | copy-start | bytes 3076
  (81 other events, 245.5 us)
Sparse Core Ops, SparseCore 0:
  9.4 27.6 all-gather.8
  42.7 43.5 all-gather.16
  93.1 41.8 all-gather.14
  137.9 104.8 all-gather.10
  245.6 78.1 all-gather.12
where the time goes:
time: 492 us; the launch traced here: 489 us
  blocking collectives  125 us (25%)
  other arithmetic  107 us (22%)
  matrix products  106 us (22%)
  waiting for transfers between devices  90.6 us (18%)
  local copies, waits for them, and re-layouts  37.9 us (8%)
  between operations  21 us (4%)
    all_gather x2, waiting for transfers between devices, sent_together(): result = lax.all_gather(both, axis, axis=dim, tiled=True)  66.6 us
    dot_general x16, matrix products, stick_block(): jnp.einsum('thd,shd->hts', queries, key_rows, preferred_element_type=jnp....  64 us
    another operation x32, other arithmetic  51.8 us
    all_gather x1, blocking collectives, body(): state_full = lax.all_gather(initial_state, SP, axis=1, tiled=True)  49 us
    convert_element_type x16, other arithmetic, stick_block(): jnp.where(allowed, jnp.exp(jax.nn.log_sigmoid(scores) + suffix), 0.0)  38.2 us
    unnamed x2, blocking collectives  30.2 us
    all_gather x2, waiting for transfers between devices, prefix_by_axis(): pieces = jax.tree.map(lambda part: lax.all_gather(part, axis), running)  23.9 us
    dot_general x16, matrix products, stick_block(): jnp.einsum('hts,shd->thd', weights, value_rows, preferred_element_type=jn...  19.1 us
  transfers between devices with their start and end apart: 5, of which 3 were waited for; matrix products, arithmetic and copies ran while one was open for 46% of the time, Pallas kernels for 0%

commit v1 on v0

v1 whole, which is shorter than its diff:
```python
import functools

import jax
import jax.numpy as jnp
from jax import lax
from jax.experimental import pallas as pl
from jax.experimental.pallas import tpu as pltpu
from jax.sharding import Mesh
from jax.sharding import PartitionSpec as P

D = 2048
STICK_WIDTH = 1024
ROWS = 256
SD = 128
RD = 256
NZ = 8
NY = 8
SLICE = RD // NY
LOG2E = 1.4426950408889634

SP = ("z", "y")
TP = ("x", "c")
ALL = ("z", "y", "x", "c")

epsilon = 1e-06
rope_base = 10000.0
bf16 = jnp.bfloat16
f32 = jnp.float32

VMEM = pl.BlockSpec(memory_space=pltpu.VMEM)
SMEM = pl.BlockSpec(memory_space=pltpu.SMEM)


def mm(a, b, dims=((1,), (0,))):
    return lax.dot_general(a, b, (dims, ((), ())), preferred_element_type=f32)


def iota(shape, dim):
    return lax.broadcasted_iota(jnp.int32, shape, dim)


def slice_order():
    r = iota((RD, RD), 0)
    c = iota((RD, RD), 1)
    j, z, k = r // SLICE, (r % SLICE) // 4, r % 4
    return (c == SLICE * z + 4 * j + k).astype(f32).astype(bf16)


def call(kernel, out, in_specs, flops, scratch=()):
    return pl.pallas_call(
        kernel,
        out_shape=out,
        in_specs=in_specs,
        out_specs=jax.tree.map(lambda _: VMEM, out),
        scratch_shapes=list(scratch),
        compiler_params=pltpu.CompilerParams(vmem_limit_bytes=48 * 1024 * 1024),
        cost_estimate=pl.CostEstimate(flops=flops, bytes_accessed=1 << 20, transcendentals=0),
    )


def project_kernel(
    pos, lam, own, other, cos, sin, wsq, wsk, wsv, wrq, wrk, wrv, kvs, sq, tq, tk, rv
):
    core = pos[2]
    widths = (SD, SD, SD, RD, RD, RD)
    sums = [jnp.zeros((ROWS, w), f32) for w in widths]
    squares = jnp.zeros((ROWS, RD), f32)
    for part, ref in ((core, own), (1 - core, other)):
        for x in range(4):
            raw = ref[x, :ROWS, :].astype(f32)
            gain = ref[x, ROWS : ROWS + 1, :].astype(f32)
            squares = squares + raw * raw
            scaled = (raw * gain).astype(bf16)
            row = pl.multiple_of((2 * x + part) * RD, RD)
            for k, w in enumerate((wsq, wsk, wsv, wrq, wrk, wrv)):
                sums[k] = sums[k] + mm(scaled, w[pl.ds(row, RD), :])
    scale = lax.rsqrt(jnp.sum(squares, axis=1, keepdims=True) / D + epsilon)
    sq_v, sk_v, sv_v, rq_v, rk_v, rv_v = [(s * scale).astype(bf16) for s in sums]
    sq[...] = sq_v
    rv[...] = rv_v
    cosine, sine = cos[...], sin[...]
    half = RD // 2

    def turn(v):
        a, b = v[:, :half].astype(f32), v[:, half:].astype(f32)
        return jnp.concatenate([a * cosine - b * sine, b * cosine + a * sine], axis=1)

    tq[...] = turn(rq_v).astype(bf16)
    key = turn(rk_v) * (RD**-0.5)
    tk[...] = key.astype(bf16)
    left = (ROWS - 1 - iota((ROWS, RD), 0)).astype(f32)
    decayed = (key * jnp.exp(lam[0] * left)).astype(bf16)
    state = mm(decayed, rv_v, ((0,), (0,))).astype(bf16)
    ordered = mm(slice_order(), state).astype(bf16)
    for y in range(NY):
        kvs[y, :ROWS, :SD] = sk_v
        kvs[y, :ROWS, SD:] = sv_v
        kvs[y, ROWS:, :] = ordered[SLICE * y : SLICE * (y + 1), :]


def inner_kernel(lam, tq, tk, rv, inner):
    gap = (iota((ROWS, ROWS), 0) - iota((ROWS, ROWS), 1)).astype(f32)
    decay = jnp.where(gap >= 0.0, jnp.exp(lam[0] * jnp.maximum(gap, 0.0)), 0.0)
    scores = mm(tq[...], tk[...], ((1,), (1,))) * decay
    inner[...] = mm(scores.astype(bf16), rv[...])


def totals_kernel(lam, kvs, sq, init, out):
    step = jnp.exp(jnp.full((1, RD), lam[0] * ROWS, f32))
    run = jnp.zeros((SLICE, RD), f32)
    for y in range(NY):
        run = run * step + kvs[y, ROWS:, :].astype(f32)
    total = run.astype(bf16)
    first = init[...].astype(bf16)
    for z in range(NZ):
        out[z, :ROWS, :] = sq[...]
        out[z, ROWS : ROWS + SLICE, :] = total[:, :SD]
        out[z, ROWS + SLICE : ROWS + 2 * SLICE, :] = total[:, SD:]
        out[z, ROWS + 2 * SLICE :, :] = first


def entering_kernel(pos, lam, kvs, zq, out, start):
    mine = pos[0]
    step = jnp.exp(jnp.full((1, RD), lam[0] * ROWS, f32))
    row_step = jnp.exp(jnp.full((1, RD), lam[0] * (ROWS * NY), f32))
    top = ROWS + 2 * SLICE
    for z in range(NZ):
        both = zq[z, top : top + 8, :].astype(f32)
        start[4 * z : 4 * z + 4, :SD] = both[:4]
        start[4 * z : 4 * z + 4, SD:] = both[4:]
    before = start[...]
    for z in range(NZ):
        total = jnp.concatenate(
            [zq[z, ROWS : ROWS + SLICE, :], zq[z, ROWS + SLICE : ROWS + 2 * SLICE, :]], axis=1
        ).astype(f32)
        before = jnp.where(z < mine, before * row_step + total, before)
    run = before
    for y in range(NY):
        out[y, :, :] = run.astype(bf16)
        run = run * step + kvs[y, ROWS:, :].astype(f32)


def stick_kernel(pos, off, kvs, zq, out, acc, car, upper):
    mine, col = pos[0], pos[1]
    c1 = (SD**-0.5) * LOG2E
    c2 = off[0] * LOG2E
    upper[...] = (iota((ROWS, ROWS), 0) > iota((ROWS, ROWS), 1)).astype(f32).astype(bf16)

    def block(q, y, carry, total, masked):
        keys = kvs[y, :ROWS, :SD]
        values = kvs[y, :ROWS, SD:]
        s = mm(q, keys, ((1,), (1,))) * c1 + c2
        soft = jnp.maximum(s, 0.0) + jnp.log2(1.0 + jnp.exp2(-jnp.abs(s)))
        power = s - soft
        if masked:
            allowed = iota((ROWS, ROWS), 1) < iota((ROWS, ROWS), 0)
            soft = jnp.where(allowed, soft, 0.0)
        rounded = soft.astype(bf16)
        later = mm(rounded, upper[...])
        weight = jnp.exp2(power - later - carry)
        if masked:
            weight = jnp.where(allowed, weight, 0.0)
        total = total + mm(weight.astype(bf16), values)
        carry = carry + later[:, :1] + rounded[:, :1].astype(f32)
        return carry, total

    def finish(z, carry, total):
        out[z, :ROWS, :] = total.astype(bf16)
        wide = jnp.transpose(jnp.broadcast_to(carry, (ROWS, SD)))[:8, :]
        a, b = wide[:, :SD], wide[:, SD:]
        ha, hb = a.astype(bf16).astype(f32), b.astype(bf16).astype(f32)
        row = iota((8, SD), 0)
        packed = jnp.where(
            row == 0,
            ha,
            jnp.where(row == 1, hb, jnp.where(row == 2, a - ha, jnp.where(row == 3, b - hb, 0.0))),
        )
        out[z, ROWS:, :] = packed.astype(bf16)

    def nothing(z, _):
        out[z, :, :] = jnp.zeros((ROWS + 8, SD), bf16)
        return 0

    lax.fori_loop(0, mine, nothing, 0)

    q = zq[mine, :ROWS, :]
    carry, total = block(
        q, col, jnp.zeros((ROWS, 1), f32), jnp.zeros((ROWS, SD), f32), True
    )
    car[...] = jnp.broadcast_to(carry, (ROWS, SD))
    acc[...] = total

    def earlier(k, _):
        c, t = block(zq[mine, :ROWS, :], col - 1 - k, car[:, :1], acc[...], False)
        car[...] = jnp.broadcast_to(c, (ROWS, SD))
        acc[...] = t
        return 0

    lax.fori_loop(0, col, earlier, 0)
    finish(mine, car[:, :1], acc[...])

    def later_rows(z, _):
        q = zq[z, :ROWS, :]
        carry, total = jnp.zeros((ROWS, 1), f32), jnp.zeros((ROWS, SD), f32)
        for y in reversed(range(NY)):
            carry, total = block(q, y, carry, total, False)
        finish(z, carry, total)
        return 0

    lax.fori_loop(mine + 1, NZ, later_rows, 0)


def join_kernel(parts, total, squares):
    rows = []
    run = jnp.zeros((1, ROWS), f32)
    for i in reversed(range(NZ)):
        rows.append(jnp.exp2(-run))
        p = parts[i, ROWS:, :].astype(f32)
        run = run + jnp.concatenate([p[0:1] + p[2:3], p[1:2] + p[3:4]], axis=1)
    factors = jnp.concatenate(rows + [jnp.zeros((SD - NZ, ROWS), f32)], axis=0)
    factors = jnp.transpose(factors)
    out = jnp.zeros((ROWS, SD), f32)
    for k, i in enumerate(reversed(range(NZ))):
        out = out + factors[:, k : k + 1] * parts[i, :ROWS, :].astype(f32)
    total[...] = out
    own = jnp.sum(out * out, axis=1, keepdims=True)
    row = jnp.transpose(jnp.broadcast_to(own, (ROWS, SD)))[:8, :]
    for t in range(8):
        squares[t, :, :] = row


def retain_kernel(lam, tq, inner, entering, gain, out):
    turned = mm(tq[...], slice_order(), ((1,), (1,))).astype(bf16)
    state = jnp.concatenate([entering[y] for y in range(NY)], axis=0)
    steps = (iota((ROWS, RD), 0) + 1).astype(f32)
    value = inner[...] + mm(turned, state) * jnp.exp(lam[0] * steps)
    value = value - jnp.mean(value, axis=1, keepdims=True)
    value = value * lax.rsqrt(jnp.mean(value * value, axis=1, keepdims=True) + epsilon)
    out[...] = (value * gain[...]).astype(bf16)


def output_kernel(total, squares, gain, ret, weights, out):
    mean = jnp.zeros((8, ROWS), f32)
    for t in range(8):
        mean = mean + squares[t]
    scale = lax.rsqrt(mean / STICK_WIDTH + epsilon)
    scale = jnp.concatenate([scale] * (SD // 8), axis=0)
    scale = jnp.transpose(scale)
    stick = (total[...] * scale * gain[...]).astype(bf16)
    both = jnp.concatenate([stick, ret[...]], axis=1)
    for n in range(8):
        cols = slice(n * 256, (n + 1) * 256)
        part = mm(both, weights[cols, :], ((1,), (1,))).astype(bf16)
        for t in range(8):
            out[t % 2, t // 2, :, cols] = part[t * 32 : (t + 1) * 32, :]


def to_all(x, axis):
    return lax.all_to_all(x, axis, 0, 0, tiled=True)


def body(
    inputs,
    input_gain,
    stick_query_w,
    stick_key_w,
    stick_value_w,
    ret_query_w,
    ret_key_w,
    ret_value_w,
    stick_offset,
    ret_log_decay,
    initial_state,
    stick_gain,
    ret_gain,
    stick_out_w,
    ret_out_w,
):
    sds = jax.ShapeDtypeStruct
    z, y, core = lax.axis_index("z"), lax.axis_index("y"), lax.axis_index("c")
    pos = jnp.stack([z, y, core]).astype(jnp.int32)

    shard = jnp.concatenate([stick_out_w, ret_out_w], axis=0).T
    weights = lax.all_gather(shard, SP, axis=0, tiled=True)

    piece = jnp.concatenate(
        [inputs, jnp.broadcast_to(input_gain[None, :], (8, input_gain.shape[0]))], axis=0
    )
    own = to_all(jnp.broadcast_to(piece[None], (4,) + piece.shape), "x")
    other = lax.ppermute(own, "c", [(0, 1), (1, 0)])

    position = ((z * NY + y) * ROWS + jnp.arange(ROWS, dtype=jnp.int32)).astype(f32)
    half = RD // 2
    inverse = rope_base ** (-jnp.arange(half, dtype=f32) / half)
    angles = position[:, None] * inverse[None, :]

    kvs, sq, tq, tk, rv = call(
        project_kernel,
        (
            sds((NY, ROWS + SLICE, RD), bf16),
            sds((ROWS, SD), bf16),
            sds((ROWS, RD), bf16),
            sds((ROWS, RD), bf16),
            sds((ROWS, RD), bf16),
        ),
        [SMEM, SMEM] + [VMEM] * 10,
        1200000000,
    )(
        pos,
        ret_log_decay,
        own,
        other,
        jnp.cos(angles),
        jnp.sin(angles),
        stick_query_w,
        stick_key_w,
        stick_value_w,
        ret_query_w,
        ret_key_w,
        ret_value_w,
    )

    row_kvs = to_all(kvs, "y")
    inner = call(inner_kernel, sds((ROWS, RD), f32), [SMEM] + [VMEM] * 3, 2000000000)(
        ret_log_decay, tq, tk, rv
    )

    first = initial_state.reshape(4, RD)
    first = jnp.concatenate([first[:, :SD], first[:, SD:]], axis=0)
    zq = call(
        totals_kernel, sds((NZ, ROWS + 2 * SLICE + 8, SD), bf16), [SMEM] + [VMEM] * 3, 10000000
    )(ret_log_decay, row_kvs, sq, first)
    col_q = to_all(zq, "z")

    slices = call(
        entering_kernel,
        sds((NY, SLICE, RD), bf16),
        [SMEM, SMEM, VMEM, VMEM],
        10000000,
        [pltpu.VMEM((SLICE, RD), f32)],
    )(pos, ret_log_decay, row_kvs, col_q)
    entering = to_all(slices, "y")

    parts = call(
        stick_kernel,
        sds((NZ, ROWS + 8, SD), bf16),
        [SMEM, SMEM, VMEM, VMEM],
        4000000000,
        [pltpu.VMEM((ROWS, SD), f32), pltpu.VMEM((ROWS, SD), f32), pltpu.VMEM((ROWS, ROWS), bf16)],
    )(pos, stick_offset, row_kvs, col_q)
    parts = to_all(parts, "z")

    total, squares = call(
        join_kernel,
        (sds((ROWS, SD), f32), sds((8, 8, ROWS), f32)),
        [VMEM],
        10000000,
    )(parts)
    squares = to_all(squares, TP)

    ret_normed = call(retain_kernel, sds((ROWS, RD), bf16), [SMEM] + [VMEM] * 4, 100000000)(
        ret_log_decay, tq, inner, entering, ret_gain[None, :]
    )

    out = call(output_kernel, sds((2, 4, 32, D), bf16), [VMEM] * 5, 400000000)(
        total, squares, stick_gain[None, :], ret_normed, weights
    )
    pair = to_all(out, "c").astype(f32).sum(axis=0).astype(bf16)
    layer = to_all(pair, "x").astype(f32).sum(axis=0)
    return layer.astype(bf16)


def solution(mesh):
    split = Mesh(mesh.devices.reshape(NZ, NY, 4, 2), ALL)
    in_specs = (
        P(SP, TP),
        P(TP),
        P(None, TP),
        P(None, TP),
        P(None, TP),
        P(None, TP),
        P(None, TP),
        P(None, TP),
        P(TP),
        P(TP),
        P(TP, SP, None),
        P(TP),
        P(TP),
        P(TP, SP),
        P(TP, SP),
    )
    return jax.shard_map(
        body, mesh=split, in_specs=in_specs, out_specs=P(ALL, None), check_vma=False
    )
```

time: 492 us -> 194 us (0.39)
  the two profiles are of different devices: /device:TPU:504 before, /device:TPU:1 now
where the time goes in v1:
time: 194 us; the launch traced here: 193 us
  waiting for transfers between devices  86 us (44%)
  starting transfers between devices  40.4 us (21%)
  Pallas kernels  25.9 us (13%)
  blocking collectives  16.6 us (9%)
  between operations  14.8 us (8%)
  local copies, waits for them, and re-layouts  6.51 us (3%)
  other arithmetic  3.21 us (2%)
    all_to_all x6, waiting for transfers between devices, to_all(): return lax.all_to_all(x, axis, 0, 0, tiled=True)  85 us
    all_to_all x6, starting transfers between devices, to_all(): return lax.all_to_all(x, axis, 0, 0, tiled=True)  31.9 us
    all_to_all x2, blocking collectives, to_all(): return lax.all_to_all(x, axis, 0, 0, tiled=True)  16.6 us
    pallas_call x1, Pallas kernels, body(): call(stick_kernel, sds((NZ, ROWS + 8, SD), bf16), [SMEM, SMEM, VMEM, VMEM...  16.1 us
    ppermute x1, starting transfers between devices, body(): other = lax.ppermute(own, 'c', [(0, 1), (1, 0)])  8.5 us
    unnamed x22, local copies, waits for them, and re-layouts  4.86 us
    pallas_call x1, Pallas kernels, body(): call(project_kernel, (sds((NY, ROWS + SLICE, RD), bf16), sds((ROWS, SD),...  4.6 us
  transfers between devices with their start and end apart: 8, of which 7 were waited for; matrix products, arithmetic and copies ran while one was open for 1% of the time, Pallas kernels for 11%

profile of v1, /device:TPU:1, one launch (start us, length us, event | category | flops | bytes accessed | tf_op | source)
XLA Modules:
  0.0 193.4 jit_solution(12086171876111896726)
XLA Ops:
  6.5 0.8 broadcast_in_dim.8
  7.3 0.9 pad_maximum_fusion
  8.3 0.8 broadcast_in_dim.9
  9.1 4.8 %all-to-all-start = ((bf16[4,264,256]{2,1,0:T(8,128)(2,1)}), bf16[4,264,256]{2,1,0:T(8,128)(2,1)S(1)}, u32[]{:S(2)}, u32[]{:S(2)}) async-start(bf16[4,264,256]{2,1,0:T(8,128)(2,1)} %broadcast_in_dim.9), calls=%async_computation | async-start | bytes 1081344 | tf_op jit(solution)/shard_map/all_to_all | solution.py:259
  14.6 6.4 %all-to-all-done.own = bf16[4,264,256]{2,1,0:T(8,128)(2,1)S(1)} async-done(((bf16[4,264,256]{2,1,0:T(8,128)(2,1)}), bf16[4,264,256]{2,1,0:T(8,128)(2,1)S(1)}, u32[]{:S(2)}, u32[]{:S(2)}) %all-to-all-start) | async-done | bytes 540704 | tf_op jit(solution)/shard_map/all_to_all | solution.py:259
  21.0 8.5 %collective-permute-start = (bf16[4,264,256]{2,1,0:T(8,128)(2,1)S(1)}, bf16[4,264,256]{2,1,0:T(8,128)(2,1)S(1)}, u32[]{:S(2)}, u32[]{:S(2)}) collective-permute-start(bf16[4,264,256]{2,1,0:T(8,128)(2,1)S(1)} %all-to-all-done.own), channel_id=1, source_target_pairs={{0,1},{1,0},{2,3},{3,2},{4,5},{5,4},{6,7},{7,6},{8,9},{9,8},{10,11... | collective-permute-start | bytes 1622024 | tf_op jit(solution)/shard_map/ppermute | solution.py:290
  30.1 0.9 collective-permute-done.other
  31.0 1.0 copy-done.3
  32.1 1.0 copy-done.4
  33.1 1.0 copy-done.5
  34.1 4.6 %shard_map.145 = (bf16[8,288,256]{2,1,0:T(8,128)(2,1)}, bf16[256,128]{1,0:T(8,128)(2,1)S(1)}, bf16[256,256]{1,0:T(8,128)(2,1)S(1)}, bf16[256,256]{1,0:T(8,128)(2,1)S(1)}, bf16[256,256]{1,0:T(8,128)(2,1)S(1)}) custom-call(s32[3]{0:T(128)S(1)} %pad_add_fusion.pos, f32[1]{0:T(128)S(6)} %copy.17.lam, bf16[4,264,256]{2,1,0:T(8,128)(2,1)S(1)} %all-to-all-done.own, ...), custom_call_target="tpu_custom_call" | custom-call | flops 1200000000 | bytes 1048576 | tf_op jit(solution)/shard_map/pallas_call | solution.py:297
  38.7 3.9 %all-to-all-start.1 = ((bf16[8,288,256]{2,1,0:T(8,128)(2,1)}), bf16[8,288,256]{2,1,0:T(8,128)(2,1)S(1)}, u32[]{:S(2)}, u32[]{:S(2)}) async-start(bf16[8,288,256]{2,1,0:T(8,128)(2,1)} %get-tuple-element.12), calls=%async_computation.1 | async-start | bytes 2359296 | tf_op jit(solution)/shard_map/all_to_all | solution.py:259
  42.7 0.6 maximum_bitcast_fusion
  43.4 31.5 %all-to-all-done.1.kvs = bf16[8,288,256]{2,1,0:T(8,128)(2,1)S(1)} async-done(((bf16[8,288,256]{2,1,0:T(8,128)(2,1)}), bf16[8,288,256]{2,1,0:T(8,128)(2,1)S(1)}, u32[]{:S(2)}, u32[]{:S(2)}) %all-to-all-start.1) | async-done | bytes 1179680 | tf_op jit(solution)/shard_map/all_to_all | solution.py:259
  74.9 0.9 shard_map.146
  75.9 10.2 %all-to-all-start.2 = ((bf16[8,328,128]{2,1,0:T(8,128)(2,1)}), bf16[8,328,128]{2,1,0:T(8,128)(2,1)S(1)}, u32[]{:S(2)}, u32[]{:S(2)}) async-start(bf16[8,328,128]{2,1,0:T(8,128)(2,1)} %shard_map.146), calls=%async_computation.2 | async-start | bytes 1343488 | tf_op jit(solution)/shard_map/all_to_all | solution.py:259
  86.7 20.6 %all-to-all-done.2.zq = bf16[8,328,128]{2,1,0:T(8,128)(2,1)S(1)} async-done(((bf16[8,328,128]{2,1,0:T(8,128)(2,1)}), bf16[8,328,128]{2,1,0:T(8,128)(2,1)S(1)}, u32[]{:S(2)}, u32[]{:S(2)}) %all-to-all-start.2) | async-done | bytes 671776 | tf_op jit(solution)/shard_map/all_to_all | solution.py:259
  107.3 16.1 %shard_map.147 = bf16[8,264,128]{2,1,0:T(8,128)(2,1)} custom-call(s32[3]{0:T(128)S(1)} %pad_add_fusion.pos, f32[1]{0:T(128)S(6)} %copy.16.off, bf16[8,288,256]{2,1,0:T(8,128)(2,1)S(1)} %all-to-all-done.1.kvs, bf16[8,328,128]{2,1,0:T(8,128)(2,1)S(1)} %all-to-all-done.2.zq), custom_call_target="tpu_custom_call" | custom-call | flops 4000000000 | bytes 1048576 | tf_op jit(solution)/shard_map/pallas_call | solution.py:344
  123.4 3.5 %all-to-all-start.3 = ((bf16[8,264,128]{2,1,0:T(8,128)(2,1)}), bf16[8,264,128]{2,1,0:T(8,128)(2,1)S(1)}, u32[]{:S(2)}, u32[]{:S(2)}) async-start(bf16[8,264,128]{2,1,0:T(8,128)(2,1)} %shard_map.147), calls=%async_computation.3 | async-start | bytes 1081344 | tf_op jit(solution)/shard_map/all_to_all | solution.py:259
  127.0 1.3 shard_map.150
  128.3 16.3 %all-to-all-done.3.parts = bf16[8,264,128]{2,1,0:T(8,128)(2,1)S(1)} async-done(((bf16[8,264,128]{2,1,0:T(8,128)(2,1)}), bf16[8,264,128]{2,1,0:T(8,128)(2,1)S(1)}, u32[]{:S(2)}, u32[]{:S(2)}) %all-to-all-start.3) | async-done | bytes 540704 | tf_op jit(solution)/shard_map/all_to_all | solution.py:259
  144.5 3.7 %all-to-all-start.5 = ((bf16[8,32,256]{2,1,0:T(8,128)(2,1)}), bf16[8,32,256]{2,1,0:T(8,128)(2,1)S(1)}, u32[]{:S(2)}, u32[]{:S(2)}) async-start(bf16[8,32,256]{2,1,0:T(8,128)(2,1)} %shard_map.150), calls=%async_computation.5 | async-start | bytes 262144 | tf_op jit(solution)/shard_map/all_to_all | solution.py:259
  148.2 1.3 shard_map.148
  149.6 6.7 %all-to-all-done.5.entering = bf16[8,32,256]{2,1,0:T(8,128)(2,1)S(1)} async-done(((bf16[8,32,256]{2,1,0:T(8,128)(2,1)}), bf16[8,32,256]{2,1,0:T(8,128)(2,1)S(1)}, u32[]{:S(2)}, u32[]{:S(2)}) %all-to-all-start.5) | async-done | bytes 131104 | tf_op jit(solution)/shard_map/all_to_all | solution.py:259
  156.3 5.6 %all-to-all-start.4 = ((f32[8,8,256]{2,1,0:T(8,128)}), f32[8,8,256]{2,1,0:T(8,128)S(1)}, u32[]{:S(2)}, u32[]{:S(2)}) async-start(f32[8,8,256]{2,1,0:T(8,128)} %get-tuple-element.15), calls=%async_computation.4 | async-start | bytes 131072 | tf_op jit(solution)/shard_map/all_to_all | solution.py:259
  162.6 0.5 shard_map.151.ret
  163.1 3.6 %all-to-all-done.4.squares = f32[8,8,256]{2,1,0:T(8,128)S(1)} async-done(((f32[8,8,256]{2,1,0:T(8,128)}), f32[8,8,256]{2,1,0:T(8,128)S(1)}, u32[]{:S(2)}, u32[]{:S(2)}) %all-to-all-start.4) | async-done | bytes 65568 | tf_op jit(solution)/shard_map/all_to_all | solution.py:259
  166.8 1.4 copy-done
  168.2 0.8 shard_map.152
  168.9 5.0 %all_to_all.40 = bf16[2,4,32,2048]{3,2,1,0:T(8,128)(2,1)S(1)} all-to-all(bf16[2,4,32,2048]{3,2,1,0:T(8,128)(2,1)S(1)} %shard_map.152), channel_id=1, replica_groups=mesh['z'=8,'y'=8,'x'=4,'c'=2] {'c'}, dimensions={0} | all-to-all | bytes 2097152 | tf_op jit(solution)/shard_map/all_to_all | solution.py:259
  174.2 11.6 %all_to_all.41 = bf16[4,32,2048]{2,1,0:T(8,128)(2,1)S(1)} all-to-all(bf16[4,32,2048]{2,1,0:T(8,128)(2,1)S(1)} %reduce_sum.24), channel_id=1, replica_groups=mesh['z'=8,'y'=8,'x'=4,'c'=2] {'x'}, dimensions={0} | all-to-all | bytes 1048576 | tf_op jit(solution)/shard_map/all_to_all | solution.py:259
  185.8 0.7 reduce_sum.25
  (29 shorter events, 1.8 us)
Async XLA Ops:
  6.5 24.5 %copy-start.1 = (bf16[2048,256]{1,0:T(8,128)(2,1)S(1)}, bf16[2048,256]{1,0:T(8,128)(2,1)}, u32[]{:S(2)}) copy-start(bf16[2048,256]{1,0:T(8,128)(2,1)} %wrq.1) | copy-start | bytes 3145732
  6.5 24.5 %copy-start.2 = (bf16[2048,256]{1,0:T(8,128)(2,1)S(1)}, bf16[2048,256]{1,0:T(8,128)(2,1)}, u32[]{:S(2)}) copy-start(bf16[2048,256]{1,0:T(8,128)(2,1)} %wrk.1) | copy-start | bytes 3145732
  9.1 11.9 %all-to-all-start = ((bf16[4,264,256]{2,1,0:T(8,128)(2,1)}), bf16[4,264,256]{2,1,0:T(8,128)(2,1)S(1)}, u32[]{:S(2)}, u32[]{:S(2)}) async-start(bf16[4,264,256]{2,1,0:T(8,128)(2,1)} %broadcast_in_dim.9), calls=%async_computation | async-start | bytes 1081344 | tf_op jit(solution)/shard_map/all_to_all | solution.py:259
  21.0 10.0 %collective-permute-start = (bf16[4,264,256]{2,1,0:T(8,128)(2,1)S(1)}, bf16[4,264,256]{2,1,0:T(8,128)(2,1)S(1)}, u32[]{:S(2)}, u32[]{:S(2)}) collective-permute-start(bf16[4,264,256]{2,1,0:T(8,128)(2,1)S(1)} %all-to-all-done.own), channel_id=1, source_target_pairs={{0,1},{1,0},{2,3},{3,2},{4,5},{5,4},{6,7},{7,6},{8,9},{9,8},{10,11... | collective-permute-start | bytes 1622024 | tf_op jit(solution)/shard_map/ppermute | solution.py:290
  31.0 1.0 copy-start.3
  32.0 1.0 copy-start.4
  33.1 1.0 copy-start.5
  38.7 4.0 %copy-start.8 = (bf16[256,32]{0,1:T(8,128)(2,1)S(1)}, bf16[256,32]{0,1:T(8,128)(2,1)}, u32[]{:S(2)}) copy-start(bf16[256,32]{0,1:T(8,128)(2,1)} %param.29) | copy-start | bytes 49156
  38.7 4.0 %copy-start.9 = (bf16[128,32]{0,1:T(8,128)(2,1)S(1)}, bf16[128,32]{0,1:T(8,128)(2,1)}, u32[]{:S(2)}) copy-start(bf16[128,32]{0,1:T(8,128)(2,1)} %param.28) | copy-start | bytes 24580
  38.7 4.7 %copy-start.10 = (f32[1,4,256]{2,1,0:T(4,128)S(1)}, f32[1,4,256]{2,1,0:T(4,128)}, u32[]{:S(2)}) copy-start(f32[1,4,256]{2,1,0:T(4,128)} %param.25) | copy-start | bytes 12292
  38.7 36.2 %all-to-all-start.1 = ((bf16[8,288,256]{2,1,0:T(8,128)(2,1)}), bf16[8,288,256]{2,1,0:T(8,128)(2,1)S(1)}, u32[]{:S(2)}, u32[]{:S(2)}) async-start(bf16[8,288,256]{2,1,0:T(8,128)(2,1)} %get-tuple-element.12), calls=%async_computation.1 | async-start | bytes 2359296 | tf_op jit(solution)/shard_map/all_to_all | solution.py:259
  42.7 120.5 %all-gather.2.cloned.1.call-start = ((), (), s32[]{:S(2)}) async-start(), calls=%async_computation.8 | async-start | bytes 1597440 | tf_op jit(solution)/shard_map/all_gather | solution.py:284
  75.9 31.5 %all-to-all-start.2 = ((bf16[8,328,128]{2,1,0:T(8,128)(2,1)}), bf16[8,328,128]{2,1,0:T(8,128)(2,1)S(1)}, u32[]{:S(2)}, u32[]{:S(2)}) async-start(bf16[8,328,128]{2,1,0:T(8,128)(2,1)} %shard_map.146), calls=%async_computation.2 | async-start | bytes 1343488 | tf_op jit(solution)/shard_map/all_to_all | solution.py:259
  123.4 21.1 %all-to-all-start.3 = ((bf16[8,264,128]{2,1,0:T(8,128)(2,1)}), bf16[8,264,128]{2,1,0:T(8,128)(2,1)S(1)}, u32[]{:S(2)}, u32[]{:S(2)}) async-start(bf16[8,264,128]{2,1,0:T(8,128)(2,1)} %shard_map.147), calls=%async_computation.3 | async-start | bytes 1081344 | tf_op jit(solution)/shard_map/all_to_all | solution.py:259
  144.5 11.8 %all-to-all-start.5 = ((bf16[8,32,256]{2,1,0:T(8,128)(2,1)}), bf16[8,32,256]{2,1,0:T(8,128)(2,1)S(1)}, u32[]{:S(2)}, u32[]{:S(2)}) async-start(bf16[8,32,256]{2,1,0:T(8,128)(2,1)} %shard_map.150), calls=%async_computation.5 | async-start | bytes 262144 | tf_op jit(solution)/shard_map/all_to_all | solution.py:259
  156.3 10.5 %all-to-all-start.4 = ((f32[8,8,256]{2,1,0:T(8,128)}), f32[8,8,256]{2,1,0:T(8,128)S(1)}, u32[]{:S(2)}, u32[]{:S(2)}) async-start(f32[8,8,256]{2,1,0:T(8,128)} %get-tuple-element.15), calls=%async_computation.4 | async-start | bytes 131072 | tf_op jit(solution)/shard_map/all_to_all | solution.py:259
  161.9 0.7 copy-start.6
  161.9 4.9 %copy-start.7 = (f32[128]{0:T(128)S(1)}, f32[128]{0:T(128)}, u32[]{:S(2)}) copy-start(f32[128]{0:T(128)} %param.26) | copy-start | bytes 1540
  166.8 1.4 copy-start
Sparse Core Ops, SparseCore 0:
  46.5 86.9 all-gather.1

commit v2 on v1

v2 whole, which is shorter than its diff:
```python
import functools

import jax
import jax.numpy as jnp
from jax import lax
from jax.experimental import pallas as pl
from jax.experimental.pallas import tpu as pltpu
from jax.sharding import Mesh
from jax.sharding import PartitionSpec as P

D = 2048
STICK_WIDTH = 1024
ROWS = 256
SD = 128
RD = 256
NZ = 8
NY = 8
SLICE = RD // NY
LOG2E = 1.4426950408889634

SP = ("z", "y")
TP = ("x", "c")
ALL = ("z", "y", "x", "c")

epsilon = 1e-06
rope_base = 10000.0
bf16 = jnp.bfloat16
f32 = jnp.float32

VMEM = pl.BlockSpec(memory_space=pltpu.VMEM)
SMEM = pl.BlockSpec(memory_space=pltpu.SMEM)
HBM = pl.BlockSpec(memory_space=pltpu.HBM)


def mm(a, b, dims=((1,), (0,))):
    return lax.dot_general(a, b, (dims, ((), ())), preferred_element_type=f32)


def iota(shape, dim):
    return lax.broadcasted_iota(jnp.int32, shape, dim)


def slice_order():
    r = iota((RD, RD), 0)
    c = iota((RD, RD), 1)
    j, z, k = r // SLICE, (r % SLICE) // 4, r % 4
    return (c == SLICE * z + 4 * j + k).astype(f32).astype(bf16)


def call(kernel, out, in_specs, flops, scratch=()):
    return pl.pallas_call(
        kernel,
        out_shape=out,
        in_specs=in_specs,
        out_specs=jax.tree.map(lambda _: VMEM, out),
        scratch_shapes=list(scratch),
        compiler_params=pltpu.CompilerParams(vmem_limit_bytes=48 * 1024 * 1024),
        cost_estimate=pl.CostEstimate(flops=flops, bytes_accessed=1 << 20, transcendentals=0),
    )


def piece_kernel(inputs, gain, out):
    for x in range(4):
        out[x, :ROWS, :] = inputs[...]
        out[x, ROWS:, :] = jnp.broadcast_to(gain[...], (8, RD))


WIDTHS = (SD, SD, SD, RD, RD, RD)
STARTS = (0, SD, 2 * SD, 3 * SD, 3 * SD + RD, 3 * SD + 2 * RD)
ALL_WIDTH = sum(WIDTHS)


def chunk_copies(part, matrices, buffers, sems):
    return [
        [
            pltpu.make_async_copy(
                w.at[pl.ds(pl.multiple_of((2 * x + part) * RD, RD), RD), :],
                buf.at[x],
                sems.at[x, k],
            )
            for k, (w, buf) in enumerate(zip(matrices, buffers))
        ]
        for x in range(4)
    ]


def projected(copies, feats, buffers, sums, squares):
    for x in range(4):
        raw = feats[x, :ROWS, :].astype(f32)
        gain = feats[x, ROWS : ROWS + 1, :].astype(f32)
        squares = squares + raw * raw
        scaled = (raw * gain).astype(bf16)
        for copy in copies[x]:
            copy.wait()
        for k, buf in enumerate(buffers):
            new = mm(scaled, buf[x])
            sums[k] = new if sums[k] is None else sums[k] + new
    return sums, squares


def first_half_kernel(pos, feats, *refs):
    matrices, (sums, squares), buffers, sems = refs[:6], refs[6:8], refs[8:14], refs[14]
    copies = chunk_copies(pos[2], matrices, buffers, sems)
    for per_chunk in copies:
        for copy in per_chunk:
            copy.start()
    out, square = projected(copies, feats, buffers, [None] * 6, jnp.zeros((ROWS, RD), f32))
    for k in range(6):
        sums[:, STARTS[k] : STARTS[k] + WIDTHS[k]] = out[k]
    squares[...] = square


def second_half_kernel(pos, lam, feats, before, before_squares, cos, sin, columns, *refs):
    matrices, outs, buffers, sems = refs[:6], refs[6:12], refs[12:18], refs[18]
    kv, states, sq, tq, tk, rv = outs
    copies = chunk_copies(1 - pos[2], matrices, buffers, sems)
    for per_chunk in copies:
        for copy in per_chunk:
            copy.start()
    start = [before[:, STARTS[k] : STARTS[k] + WIDTHS[k]] for k in range(6)]
    sums, squares = projected(copies, feats, buffers, start, before_squares[...])
    scale = lax.rsqrt(jnp.sum(squares, axis=1, keepdims=True) / D + epsilon)
    sq_v, sk_v, sv_v, rq_v, rk_v, rv_v = [(s * scale).astype(bf16) for s in sums]
    kv[:, :SD] = sk_v
    kv[:, SD:] = sv_v
    sq[...] = sq_v
    rv[...] = rv_v
    cosine, sine = cos[...], sin[...]
    half = RD // 2

    def turn(v):
        a, b = v[:, :half].astype(f32), v[:, half:].astype(f32)
        return jnp.concatenate([a * cosine - b * sine, b * cosine + a * sine], axis=1)

    tq[...] = turn(rq_v).astype(bf16)
    key = turn(rk_v) * (RD**-0.5)
    tk[...] = key.astype(bf16)
    left = (ROWS - 1 - iota((ROWS, RD), 0)).astype(f32)
    decayed = (key * jnp.exp(lam[0] * left)).astype(bf16)
    state = mm(decayed, rv_v, ((0,), (0,))).astype(bf16)
    ordered = mm(slice_order(), state).astype(bf16)
    for y in range(NY):
        rows = slice(SLICE * y, SLICE * (y + 1))
        states[y, :SLICE, :] = ordered[rows, :SD]
        states[y, SLICE : 2 * SLICE, :] = ordered[rows, SD:]
        states[y, 2 * SLICE :, :] = columns[...]


def inner_kernel(lam, tq, tk, rv, inner):
    gap = (iota((ROWS, ROWS), 0) - iota((ROWS, ROWS), 1)).astype(f32)
    decay = jnp.where(gap >= 0.0, jnp.exp(lam[0] * jnp.maximum(gap, 0.0)), 0.0)
    scores = mm(tq[...], tk[...], ((1,), (1,))) * decay
    inner[...] = mm(scores.astype(bf16), rv[...])


def halves(ref, i, top):
    return jnp.concatenate(
        [ref[i, top : top + SLICE, :], ref[i, top + SLICE : top + 2 * SLICE, :]], axis=1
    ).astype(f32)


def totals_kernel(lam, states, sq, init, out):
    step = jnp.exp(jnp.full((1, RD), lam[0] * ROWS, f32))
    run = jnp.zeros((SLICE, RD), f32)
    for y in range(NY):
        run = run * step + halves(states, y, 0)
    total = run.astype(bf16)
    first = init[...].astype(bf16)
    for z in range(NZ):
        out[z, :ROWS, :] = sq[...]
        out[z, ROWS : ROWS + SLICE, :] = total[:, :SD]
        out[z, ROWS + SLICE : ROWS + 2 * SLICE, :] = total[:, SD:]
        out[z, ROWS + 2 * SLICE :, :] = first


def entering_kernel(pos, lam, states, zq, out, start):
    mine = pos[0]
    step = jnp.exp(jnp.full((1, RD), lam[0] * ROWS, f32))
    row_step = jnp.exp(jnp.full((1, RD), lam[0] * (ROWS * NY), f32))
    top = ROWS + 2 * SLICE
    for z in range(NZ):
        both = zq[z, top : top + 8, :].astype(f32)
        start[4 * z : 4 * z + 4, :SD] = both[:4]
        start[4 * z : 4 * z + 4, SD:] = both[4:]
    before = start[...]
    for z in range(NZ):
        before = jnp.where(z < mine, before * row_step + halves(zq, z, ROWS), before)
    run = before
    for y in range(NY):
        out[y, :, :] = run.astype(bf16)
        run = run * step + halves(states, y, 0)


PAIR = 2
TALL = PAIR * ROWS


def stick_kernel(pos, off, kvs, zq, out, upper, twice, split, acc, car, local, sems):
    copies = [pltpu.make_async_copy(kvs.at[y], local.at[y], sems.at[y]) for y in range(NY)]
    for copy in copies:
        copy.start()
    mine, col = pos[0], pos[1]
    c1 = (SD**-0.5) * LOG2E
    c2 = off[0] * LOG2E
    upper[...] = (iota((ROWS, ROWS), 0) > iota((ROWS, ROWS), 1)).astype(f32).astype(bf16)
    for y in range(NY):
        copies[y].wait()
        twice[y, :, :SD] = local[y, :, :SD]
        twice[y, :, SD:] = local[y, :, :SD]

    def rows_of(c, masked):
        for k in range(PAIR):
            rows = slice(k * ROWS, (k + 1) * ROWS)
            q = zq[c * PAIR + k, :ROWS, :].astype(f32) * c1
            high = q.astype(bf16)
            split[rows, :SD] = high
            split[rows, SD:] = (q - high.astype(f32)).astype(bf16)
        carry = jnp.zeros((TALL, 1), f32)
        total = jnp.zeros((TALL, SD), f32)
        for y in reversed(range(NY)):
            s = mm(split[...], twice[y], ((1,), (1,))) + c2
            soft = jnp.maximum(jnp.log2(1.0 + jnp.exp2(jnp.minimum(s, 126.0))), s)
            power = s - soft
            if masked:
                row = iota((TALL, ROWS), 0)
                row = (row % ROWS) + (row // ROWS) * (NY * ROWS)
                first = ((c * PAIR - mine) * NY + col - y) * ROWS
                allowed = iota((TALL, ROWS), 1) - row < first
                soft = jnp.where(allowed, soft, 0.0)
            rounded = soft.astype(bf16)
            later = mm(rounded, upper[...])
            weight = jnp.exp2(power - (later + carry))
            if masked:
                weight = jnp.where(allowed, weight, 0.0)
            total = total + mm(weight.astype(bf16), local[y, :, SD:])
            carry = carry + (later[:, :1] + rounded[:, :1].astype(f32))
        acc[...] = total
        car[...] = jnp.broadcast_to(carry, (TALL, SD))
        for k in range(PAIR):
            rows = slice(k * ROWS, (k + 1) * ROWS)
            out[c * PAIR + k, :ROWS, :] = acc[rows, :].astype(bf16)
            wide = jnp.transpose(car[rows, :])[:8, :]
            a, b = wide[:, :SD], wide[:, SD:]
            ha, hb = a.astype(bf16).astype(f32), b.astype(bf16).astype(f32)
            row = iota((8, SD), 0)
            low = jnp.where(row == 2, a - ha, jnp.where(row == 3, b - hb, 0.0))
            packed = jnp.where(row == 0, ha, jnp.where(row == 1, hb, low))
            out[c * PAIR + k, ROWS:, :] = packed.astype(bf16)

    own = mine // PAIR

    def nothing(z, _):
        out[z, :, :] = jnp.zeros((ROWS + 8, SD), bf16)
        return 0

    def full(c, _):
        rows_of(c, False)
        return 0

    lax.fori_loop(0, own * PAIR, nothing, 0)
    rows_of(own, True)
    lax.fori_loop(own + 1, NZ // PAIR, full, 0)


def join_kernel(parts, total, squares):
    rows = []
    run = jnp.zeros((1, ROWS), f32)
    for i in reversed(range(NZ)):
        rows.append(jnp.exp2(-run))
        p = parts[i, ROWS:, :].astype(f32)
        run = run + jnp.concatenate([p[0:1] + p[2:3], p[1:2] + p[3:4]], axis=1)
    factors = jnp.concatenate(rows + [jnp.zeros((SD - NZ, ROWS), f32)], axis=0)
    factors = jnp.transpose(factors)
    out = jnp.zeros((ROWS, SD), f32)
    for k, i in enumerate(reversed(range(NZ))):
        out = out + factors[:, k : k + 1] * parts[i, :ROWS, :].astype(f32)
    total[...] = out
    own = jnp.sum(out * out, axis=1, keepdims=True)
    row = jnp.transpose(jnp.broadcast_to(own, (ROWS, SD)))[:8, :]
    for t in range(8):
        squares[t, :, :] = row


def retain_kernel(lam, tq, inner, entering, gain, out):
    turned = mm(tq[...], slice_order(), ((1,), (1,))).astype(bf16)
    state = jnp.concatenate([entering[y] for y in range(NY)], axis=0)
    steps = (iota((ROWS, RD), 0) + 1).astype(f32)
    value = inner[...] + mm(turned, state) * jnp.exp(lam[0] * steps)
    value = value - jnp.mean(value, axis=1, keepdims=True)
    value = value * lax.rsqrt(jnp.mean(value * value, axis=1, keepdims=True) + epsilon)
    out[...] = (value * gain[...]).astype(bf16)


def output_kernel(total, squares, gain, ret, weights, out, local, sems):
    copies = [pltpu.make_async_copy(weights.at[n], local.at[n], sems.at[n]) for n in range(NZ)]
    for copy in copies:
        copy.start()
    mean = jnp.zeros((8, ROWS), f32)
    for t in range(8):
        mean = mean + squares[t]
    scale = lax.rsqrt(mean / STICK_WIDTH + epsilon)
    scale = jnp.concatenate([scale] * (SD // 8), axis=0)
    scale = jnp.transpose(scale)
    stick = (total[...] * scale * gain[...]).astype(bf16)
    both = jnp.concatenate([stick, ret[...]], axis=1)
    for n in range(8):
        cols = slice(n * 256, (n + 1) * 256)
        copies[n].wait()
        block = jnp.concatenate(
            [
                jnp.concatenate([local[n, y, 32 * b : 32 * b + 32, :] for y in range(NY)], axis=0)
                for b in range(3)
            ],
            axis=1,
        )
        part = mm(both, block, ((1,), (1,))).astype(bf16)
        for t in range(8):
            out[t % 2, t // 2, :, cols] = part[t * 32 : (t + 1) * 32, :]


def to_all(x, axis):
    return lax.all_to_all(x, axis, 0, 0, tiled=True)


def body(
    inputs,
    input_gain,
    stick_query_w,
    stick_key_w,
    stick_value_w,
    ret_query_w,
    ret_key_w,
    ret_value_w,
    stick_offset,
    ret_log_decay,
    initial_state,
    stick_gain,
    ret_gain,
    stick_out_w,
    ret_out_w,
):
    sds = jax.ShapeDtypeStruct
    z, y, core = lax.axis_index("z"), lax.axis_index("y"), lax.axis_index("c")
    pos = jnp.stack([z, y, core]).astype(jnp.int32)

    ret_cols = ret_out_w.T
    columns = jnp.concatenate([stick_out_w.T, ret_cols[:, :SD], ret_cols[:, SD:]], axis=0)

    piece = call(piece_kernel, sds((4, ROWS + 8, RD), bf16), [VMEM, VMEM], 1000)(
        inputs, input_gain[None, :]
    )
    own = to_all(piece, "x")
    other = lax.ppermute(own, "c", [(0, 1), (1, 0)])

    position = ((z * NY + y) * ROWS + jnp.arange(ROWS, dtype=jnp.int32)).astype(f32)
    half = RD // 2
    inverse = rope_base ** (-jnp.arange(half, dtype=f32) / half)
    angles = position[:, None] * inverse[None, :]

    matrices = (stick_query_w, stick_key_w, stick_value_w, ret_query_w, ret_key_w, ret_value_w)
    buffers = [pltpu.VMEM((4, RD, w), bf16) for w in WIDTHS] + [pltpu.SemaphoreType.DMA((4, 6))]
    sums, squares = call(
        first_half_kernel,
        (sds((ROWS, ALL_WIDTH), f32), sds((ROWS, RD), f32)),
        [SMEM, VMEM] + [HBM] * 6,
        600000000,
        buffers,
    )(pos, own, *matrices)
    kv, states, sq, tq, tk, rv = call(
        second_half_kernel,
        (
            sds((ROWS, 2 * SD), bf16),
            sds((NY, 2 * SLICE + 96, SD), bf16),
            sds((ROWS, SD), bf16),
            sds((ROWS, RD), bf16),
            sds((ROWS, RD), bf16),
            sds((ROWS, RD), bf16),
        ),
        [SMEM, SMEM] + [VMEM] * 6 + [HBM] * 6,
        600000000,
        buffers,
    )(
        pos,
        ret_log_decay,
        other,
        sums,
        squares,
        jnp.cos(angles),
        jnp.sin(angles),
        columns,
        *matrices,
    )

    row_kv = lax.all_gather(kv, "y", axis=0)
    states = to_all(states, "y")
    weights = lax.all_gather(states[:, 2 * SLICE :, :], "z", axis=0)

    first = initial_state.reshape(4, RD)
    first = jnp.concatenate([first[:, :SD], first[:, SD:]], axis=0)
    zq = call(
        totals_kernel, sds((NZ, ROWS + 2 * SLICE + 8, SD), bf16), [SMEM] + [VMEM] * 3, 10000000
    )(ret_log_decay, states, sq, first)
    col_q = to_all(zq, "z")

    slices = call(
        entering_kernel,
        sds((NY, SLICE, RD), bf16),
        [SMEM, SMEM, VMEM, VMEM],
        10000000,
        [pltpu.VMEM((SLICE, RD), f32)],
    )(pos, ret_log_decay, states, col_q)
    entering = to_all(slices, "y")
    inner = call(inner_kernel, sds((ROWS, RD), f32), [SMEM] + [VMEM] * 3, 2000000000)(
        ret_log_decay, tq, tk, rv
    )

    row_kv, entering = lax.optimization_barrier((row_kv, entering))
    parts = call(
        stick_kernel,
        sds((NZ, ROWS + 8, SD), bf16),
        [SMEM, SMEM, HBM, VMEM],
        4000000000,
        [
            pltpu.VMEM((ROWS, ROWS), bf16),
            pltpu.VMEM((NY, ROWS, 2 * SD), bf16),
            pltpu.VMEM((TALL, 2 * SD), bf16),
            pltpu.VMEM((TALL, SD), f32),
            pltpu.VMEM((TALL, SD), f32),
            pltpu.VMEM((NY, ROWS, 2 * SD), bf16),
            pltpu.SemaphoreType.DMA((NY,)),
        ],
    )(pos, stick_offset, row_kv, col_q)
    parts = to_all(parts, "z")

    total, squares = call(
        join_kernel,
        (sds((ROWS, SD), f32), sds((8, 8, ROWS), f32)),
        [VMEM],
        10000000,
    )(parts)
    squares = to_all(squares, TP)

    ret_normed = call(retain_kernel, sds((ROWS, RD), bf16), [SMEM] + [VMEM] * 4, 100000000)(
        ret_log_decay, tq, inner, entering, ret_gain[None, :]
    )

    out = call(
        output_kernel,
        sds((2, 4, 32, D), bf16),
        [VMEM] * 4 + [HBM],
        400000000,
        [pltpu.VMEM((NZ, NY, 96, SD), bf16), pltpu.SemaphoreType.DMA((NZ,))],
    )(
        total, squares, stick_gain[None, :], ret_normed, weights
    )
    pair = to_all(out, "c").astype(f32).sum(axis=0).astype(bf16)
    layer = to_all(pair, "x").astype(f32).sum(axis=0)
    return layer.astype(bf16)


def solution(mesh):
    split = Mesh(mesh.devices.reshape(NZ, NY, 4, 2), ALL)
    in_specs = (
        P(SP, TP),
        P(TP),
        P(None, TP),
        P(None, TP),
        P(None, TP),
        P(None, TP),
        P(None, TP),
        P(None, TP),
        P(TP),
        P(TP),
        P(TP, SP, None),
        P(TP),
        P(TP),
        P(TP, SP),
        P(TP, SP),
    )
    return jax.shard_map(
        body, mesh=split, in_specs=in_specs, out_specs=P(ALL, None), check_vma=False
    )
```

time: 194 us -> 189 us (0.974)
  waiting for transfers between devices: 86 us -> 51.4 us
  blocking collectives: 16.6 us -> 34 us
  Pallas kernels: 25.9 us -> 35.1 us
  local copies, waits for them, and re-layouts: 6.51 us -> 10.4 us
    all_to_all x6 -> x5, waiting for transfers between devices: 85 us -> 51.4 us  [to_all(): return lax.all_to_all(x, axis, 0, 0, tiled=True)]
    all_to_all x2 -> x3, blocking collectives: 16.6 us -> 34 us  [to_all(): return lax.all_to_all(x, axis, 0, 0, tiled=True)]
    pallas_call x3 -> x5, Pallas kernels: 21.5 us -> 30.7 us  [the longest x1 12.5 us: body(): call(stick_kernel, sds((NZ, ROWS + 8, SD), bf16), [SMEM, SMEM, HBM, VMEM]...]
    unnamed x22 -> x24, local copies, waits for them, and re-layouts: 4.86 us -> 8.2 us
    all_to_all x6 -> x5, starting transfers between devices: 31.9 us -> 30.7 us  [to_all(): return lax.all_to_all(x, axis, 0, 0, tiled=True)]
  transfers between devices with their start and end apart: 8 -> 8, of which waited for: 7 -> 5; matrix products, arithmetic and copies ran while one was open for 1% -> 1% of each run, Pallas kernels for 11% -> 12%
where the time goes in v2:
time: 189 us; the launch traced here: 187 us
  waiting for transfers between devices  51.4 us (27%)
  starting transfers between devices  39.2 us (21%)
  Pallas kernels  35.1 us (19%)
  blocking collectives  34 us (18%)
  between operations  14.9 us (8%)
  local copies, waits for them, and re-layouts  10.4 us (6%)
  other arithmetic  2.38 us (1%)
    all_to_all x5, waiting for transfers between devices, to_all(): return lax.all_to_all(x, axis, 0, 0, tiled=True)  51.4 us
    all_to_all x3, blocking collectives, to_all(): return lax.all_to_all(x, axis, 0, 0, tiled=True)  34 us
    all_to_all x5, starting transfers between devices, to_all(): return lax.all_to_all(x, axis, 0, 0, tiled=True)  30.7 us
    pallas_call x1, Pallas kernels, body(): call(stick_kernel, sds((NZ, ROWS + 8, SD), bf16), [SMEM, SMEM, HBM, VMEM]...  12.5 us
    ppermute x1, starting transfers between devices, body(): other = lax.ppermute(own, 'c', [(0, 1), (1, 0)])  8.5 us
    unnamed x24, local copies, waits for them, and re-layouts  8.2 us
    pallas_call x1, Pallas kernels, body(): call(second_half_kernel, (sds((ROWS, 2 * SD), bf16), sds((NY, 2 * SLICE +...  6.55 us
    pallas_call x1, Pallas kernels, body(): call(first_half_kernel, (sds((ROWS, ALL_WIDTH), f32), sds((ROWS, RD), f32...  6.14 us
  transfers between devices with their start and end apart: 8, of which 5 were waited for; matrix products, arithmetic and copies ran while one was open for 1% of the time, Pallas kernels for 12%

profile of v2, /device:TPU:1, one launch (start us, length us, event | category | flops | bytes accessed | tf_op | source)
XLA Modules:
  0.0 187.5 jit_solution(11572411753601088261)
XLA Ops:
  6.5 0.8 broadcast_in_dim.11.gain
  7.3 0.9 copy-done.7
  8.3 0.9 shard_map.145
  9.1 4.8 %all-to-all-start = ((bf16[4,264,256]{2,1,0:T(8,128)(2,1)}), bf16[4,264,256]{2,1,0:T(8,128)(2,1)S(1)}, u32[]{:S(2)}, u32[]{:S(2)}) async-start(bf16[4,264,256]{2,1,0:T(8,128)(2,1)} %shard_map.145), calls=%async_computation | async-start | bytes 1081344 | tf_op jit(solution)/shard_map/all_to_all | solution.py:322
  14.0 0.7 fusion
  14.7 6.3 %all-to-all-done.feats = bf16[4,264,256]{2,1,0:T(8,128)(2,1)S(1)} async-done(((bf16[4,264,256]{2,1,0:T(8,128)(2,1)}), bf16[4,264,256]{2,1,0:T(8,128)(2,1)S(1)}, u32[]{:S(2)}, u32[]{:S(2)}) %all-to-all-start) | async-done | bytes 540704 | tf_op jit(solution)/shard_map/all_to_all | solution.py:322
  21.0 8.5 %collective-permute-start = (bf16[4,264,256]{2,1,0:T(8,128)(2,1)S(1)}, bf16[4,264,256]{2,1,0:T(8,128)(2,1)S(1)}, u32[]{:S(2)}, u32[]{:S(2)}) collective-permute-start(bf16[4,264,256]{2,1,0:T(8,128)(2,1)S(1)} %all-to-all-done.feats), channel_id=1, source_target_pairs={{0,1},{1,0},{2,3},{3,2},{4,5},{5,4},{6,7},{7,6},{8,9},{9,8},{10,11... | collective-permute-start | bytes 1622024 | tf_op jit(solution)/shard_map/ppermute | solution.py:353
  31.5 1.2 copy-done.2
  32.7 1.0 copy-done.3
  33.8 1.0 copy-done.4
  34.8 1.0 copy-done.5
  35.8 6.1 %shard_map.146 = (f32[256,1152]{1,0:T(8,128)}, f32[256,256]{1,0:T(8,128)S(1)}) custom-call(s32[3]{0:T(128)S(1)} %pad_add_fusion.pos, bf16[4,264,256]{2,1,0:T(8,128)(2,1)S(1)} %all-to-all-done.feats, bf16[2048,128]{1,0:T(8,128)(2,1)S(1)} %copy-done.3, bf16[2048,128]{1,0:T(8,128)(2,1)S(1)} %copy-done.4, bf16[2048,128]{1,0:T(8,128)(2,1)S(1)} %copy-done.5, ...), custom_call_target="tpu_custom_call" | custom-call | flops 600000000 | bytes 1048576 | tf_op jit(solution)/shard_map/pallas_call | solution.py:362
  42.0 6.6 %shard_map.147 = (bf16[256,256]{1,0:T(8,128)(2,1)}, bf16[8,160,128]{2,1,0:T(8,128)(2,1)}, bf16[256,128]{1,0:T(8,128)(2,1)S(1)}, bf16[256,256]{1,0:T(8,128)(2,1)S...) custom-call(s32[3]{0:T(128)S(1)} %pad_add_fusion.pos, f32[1]{0:T(128)S(6)} %copy.17.lam, ...), custom_call_target="tpu_custom_call" | custom-call | flops 600000000 | bytes 1048576 | tf_op jit(solution)/shard_map/pallas_call | solution.py:369
  48.6 3.8 %all-to-all-start.1 = ((bf16[8,160,128]{2,1,0:T(8,128)(2,1)}), bf16[8,160,128]{2,1,0:T(8,128)(2,1)S(1)}, u32[]{:S(2)}, u32[]{:S(2)}) async-start(bf16[8,160,128]{2,1,0:T(8,128)(2,1)} %get-tuple-element.20), calls=%async_computation.1 | async-start | bytes 655360 | tf_op jit(solution)/shard_map/all_to_all | solution.py:322
  52.5 13.7 %all-to-all-done.1.states = bf16[8,160,128]{2,1,0:T(8,128)(2,1)S(1)} async-done(((bf16[8,160,128]{2,1,0:T(8,128)(2,1)}), bf16[8,160,128]{2,1,0:T(8,128)(2,1)S(1)}, u32[]{:S(2)}, u32[]{:S(2)}) %all-to-all-start.1) | async-done | bytes 327712 | tf_op jit(solution)/shard_map/all_to_all | solution.py:322
  66.2 0.9 shard_map.148
  67.1 11.6 %all-to-all-start.2 = ((bf16[8,328,128]{2,1,0:T(8,128)(2,1)}), bf16[8,328,128]{2,1,0:T(8,128)(2,1)S(1)}, u32[]{:S(2)}, u32[]{:S(2)}) async-start(bf16[8,328,128]{2,1,0:T(8,128)(2,1)} %shard_map.148), calls=%async_computation.2 | async-start | bytes 1343488 | tf_op jit(solution)/shard_map/all_to_all | solution.py:322
  79.5 20.4 %all-to-all-done.2.zq = bf16[8,328,128]{2,1,0:T(8,128)(2,1)S(1)} async-done(((bf16[8,328,128]{2,1,0:T(8,128)(2,1)}), bf16[8,328,128]{2,1,0:T(8,128)(2,1)S(1)}, u32[]{:S(2)}, u32[]{:S(2)}) %all-to-all-start.2) | async-done | bytes 671776 | tf_op jit(solution)/shard_map/all_to_all | solution.py:322
  99.9 1.3 shard_map.149
  101.1 3.4 %all-to-all-start.3 = ((bf16[8,32,256]{2,1,0:T(8,128)(2,1)}), bf16[8,32,256]{2,1,0:T(8,128)(2,1)S(1)}, u32[]{:S(2)}, u32[]{:S(2)}) async-start(bf16[8,32,256]{2,1,0:T(8,128)(2,1)} %shard_map.149), calls=%async_computation.3 | async-start | bytes 262144 | tf_op jit(solution)/shard_map/all_to_all | solution.py:322
  105.2 7.4 %all-to-all-done.3.entering = bf16[8,32,256]{2,1,0:T(8,128)(2,1)S(1)} async-done(((bf16[8,32,256]{2,1,0:T(8,128)(2,1)}), bf16[8,32,256]{2,1,0:T(8,128)(2,1)S(1)}, u32[]{:S(2)}, u32[]{:S(2)}) %all-to-all-start.3) | async-done | bytes 131104 | tf_op jit(solution)/shard_map/all_to_all | solution.py:322
  112.6 1.2 copy-done.10
  113.8 12.5 %shard_map.150 = bf16[8,264,128]{2,1,0:T(8,128)(2,1)S(1)} custom-call(s32[3]{0:T(128)S(1)} %pad_add_fusion.pos, f32[1]{0:T(128)S(6)} %copy.16.off, bf16[8,256,256]{2,1,0:T(8,128)(2,1)S(1)} %bitcast.13, bf16[8,328,128]{2,1,0:T(8,128)(2,1)S(1)} %all-to-all-done.2.zq), custom_call_target="tpu_custom_call" | custom-call | flops 4000000000 | bytes 1048576 | tf_op jit(solution)/shard_map/pallas_call | solution.py:418
  126.2 17.4 %all_to_all.40.parts = bf16[8,264,128]{2,1,0:T(8,128)(2,1)S(1)} all-to-all(bf16[8,264,128]{2,1,0:T(8,128)(2,1)S(1)} %shard_map.150), channel_id=1, replica_groups=mesh['z'=8,'y'=8,'x'=4,'c'=2] {'z'}, dimensions={0} | all-to-all | bytes 1081344 | tf_op jit(solution)/shard_map/all_to_all | solution.py:322
  143.7 1.3 shard_map.151
  145.0 7.0 %all-to-all-start.5 = ((f32[8,8,256]{2,1,0:T(8,128)}), f32[8,8,256]{2,1,0:T(8,128)S(1)}, u32[]{:S(2)}, u32[]{:S(2)}) async-start(f32[8,8,256]{2,1,0:T(8,128)} %get-tuple-element.24), calls=%async_computation.5 | async-start | bytes 131072 | tf_op jit(solution)/shard_map/all_to_all | solution.py:322
  153.2 3.6 %all-to-all-done.5.squares = f32[8,8,256]{2,1,0:T(8,128)S(1)} async-done(((f32[8,8,256]{2,1,0:T(8,128)}), f32[8,8,256]{2,1,0:T(8,128)S(1)}, u32[]{:S(2)}, u32[]{:S(2)}) %all-to-all-start.5) | async-done | bytes 65568 | tf_op jit(solution)/shard_map/all_to_all | solution.py:322
  156.9 1.4 copy-done.6
  158.3 4.7 %shard_map.154 = bf16[2,4,32,2048]{3,2,1,0:T(8,128)(2,1)S(1)} custom-call(f32[256,128]{1,0:T(8,128)S(1)} %get-tuple-element.23.total, f32[8,8,256]{2,1,0:T(8,128)S(1)} %all-to-all-done.5.squares, f32[1,128]{1,0:T(1,128)S(1)} %bitcast.12, bf16[256,256]{1,0:T(8,128)(2,1)S(1)} %shard_map.153.ret, bf16[8,8,96,128]{3,2,1,0:T(8,128)(2,1)S(1)} %bitcast.10), custom_call_target="tpu_custom_call" | custom-call | flops 400000000 | bytes 1048576 | tf_op jit(solution)/shard_map/pallas_call | solution.py:447
  163.0 5.0 %all_to_all.41 = bf16[2,4,32,2048]{3,2,1,0:T(8,128)(2,1)S(1)} all-to-all(bf16[2,4,32,2048]{3,2,1,0:T(8,128)(2,1)S(1)} %shard_map.154), channel_id=1, replica_groups=mesh['z'=8,'y'=8,'x'=4,'c'=2] {'c'}, dimensions={0} | all-to-all | bytes 2097152 | tf_op jit(solution)/shard_map/all_to_all | solution.py:322
  168.3 11.6 %all_to_all.42 = bf16[4,32,2048]{2,1,0:T(8,128)(2,1)S(1)} all-to-all(bf16[4,32,2048]{2,1,0:T(8,128)(2,1)S(1)} %reduce_sum.24), channel_id=1, replica_groups=mesh['z'=8,'y'=8,'x'=4,'c'=2] {'x'}, dimensions={0} | all-to-all | bytes 1048576 | tf_op jit(solution)/shard_map/all_to_all | solution.py:322
  179.9 0.7 reduce_sum.25
  (35 shorter events, 3.7 us)
Async XLA Ops:
  6.5 24.9 %copy-start = (bf16[2048,256]{1,0:T(8,128)(2,1)S(1)}, bf16[2048,256]{1,0:T(8,128)(2,1)}, u32[]{:S(2)}) copy-start(bf16[2048,256]{1,0:T(8,128)(2,1)} %refs_3_.3) | copy-start | bytes 3145732
  6.5 24.9 %copy-start.1 = (bf16[2048,256]{1,0:T(8,128)(2,1)S(1)}, bf16[2048,256]{1,0:T(8,128)(2,1)}, u32[]{:S(2)}) copy-start(bf16[2048,256]{1,0:T(8,128)(2,1)} %refs_4_.3) | copy-start | bytes 3145732
  7.3 0.9 copy-start.7
  9.1 11.9 %all-to-all-start = ((bf16[4,264,256]{2,1,0:T(8,128)(2,1)}), bf16[4,264,256]{2,1,0:T(8,128)(2,1)S(1)}, u32[]{:S(2)}, u32[]{:S(2)}) async-start(bf16[4,264,256]{2,1,0:T(8,128)(2,1)} %shard_map.145), calls=%async_computation | async-start | bytes 1081344 | tf_op jit(solution)/shard_map/all_to_all | solution.py:322
  13.9 91.2 %all-gather.5.cloned.1.call-start = ((), (), s32[]{:S(2)}) async-start(), calls=%async_computation.8 | async-start | bytes 1179648 | tf_op jit(solution)/shard_map/all_gather | solution.py:394
  21.0 21.0 %collective-permute-start = (bf16[4,264,256]{2,1,0:T(8,128)(2,1)S(1)}, bf16[4,264,256]{2,1,0:T(8,128)(2,1)S(1)}, u32[]{:S(2)}, u32[]{:S(2)}) collective-permute-start(bf16[4,264,256]{2,1,0:T(8,128)(2,1)S(1)} %all-to-all-done.feats), channel_id=1, source_target_pairs={{0,1},{1,0},{2,3},{3,2},{4,5},{5,4},{6,7},{7,6},{8,9},{9,8},{10,11... | collective-permute-start | bytes 1622024 | tf_op jit(solution)/shard_map/ppermute | solution.py:353
  31.5 1.2 copy-start.2
  32.7 1.0 copy-start.3
  33.7 1.0 copy-start.4
  34.8 1.0 copy-start.5
  42.0 10.4 %copy-start.11 = (f32[1,4,256]{2,1,0:T(4,128)S(1)}, f32[1,4,256]{2,1,0:T(4,128)}, u32[]{:S(2)}) copy-start(f32[1,4,256]{2,1,0:T(4,128)} %param.25) | copy-start | bytes 12292
  48.6 17.6 %all-to-all-start.1 = ((bf16[8,160,128]{2,1,0:T(8,128)(2,1)}), bf16[8,160,128]{2,1,0:T(8,128)(2,1)S(1)}, u32[]{:S(2)}, u32[]{:S(2)}) async-start(bf16[8,160,128]{2,1,0:T(8,128)(2,1)} %get-tuple-element.20), calls=%async_computation.1 | async-start | bytes 655360 | tf_op jit(solution)/shard_map/all_to_all | solution.py:322
  67.1 32.8 %all-to-all-start.2 = ((bf16[8,328,128]{2,1,0:T(8,128)(2,1)}), bf16[8,328,128]{2,1,0:T(8,128)(2,1)S(1)}, u32[]{:S(2)}, u32[]{:S(2)}) async-start(bf16[8,328,128]{2,1,0:T(8,128)(2,1)} %shard_map.148), calls=%async_computation.2 | async-start | bytes 1343488 | tf_op jit(solution)/shard_map/all_to_all | solution.py:322
  78.8 78.1 %all-gather.7.cloned.1.call-start = ((), (), s32[]{:S(2)}) async-start(), calls=%async_computation.9 | async-start | bytes 1769472 | tf_op jit(solution)/shard_map/all_gather | solution.py:396
  101.1 11.4 %all-to-all-start.3 = ((bf16[8,32,256]{2,1,0:T(8,128)(2,1)}), bf16[8,32,256]{2,1,0:T(8,128)(2,1)S(1)}, u32[]{:S(2)}, u32[]{:S(2)}) async-start(bf16[8,32,256]{2,1,0:T(8,128)(2,1)} %shard_map.149), calls=%async_computation.3 | async-start | bytes 262144 | tf_op jit(solution)/shard_map/all_to_all | solution.py:322
  112.6 1.2 copy-start.10
  145.0 11.9 %all-to-all-start.5 = ((f32[8,8,256]{2,1,0:T(8,128)}), f32[8,8,256]{2,1,0:T(8,128)S(1)}, u32[]{:S(2)}, u32[]{:S(2)}) async-start(f32[8,8,256]{2,1,0:T(8,128)} %get-tuple-element.24), calls=%async_computation.5 | async-start | bytes 131072 | tf_op jit(solution)/shard_map/all_to_all | solution.py:322
  152.0 0.7 copy-start.8
  152.0 4.9 %copy-start.9 = (f32[128]{0:T(128)S(1)}, f32[128]{0:T(128)}, u32[]{:S(2)}) copy-start(f32[128]{0:T(128)} %param.26) | copy-start | bytes 1540
  156.9 1.4 copy-start.6
Sparse Core Ops, SparseCore 0:
  48.7 35.1 all-gather.4
  86.0 42.8 all-gather.6

commit v3 on v2

--- a/solution.py
+++ b/solution.py
@@ -27,6 +27,8 @@
 bf16 = jnp.bfloat16
 f32 = jnp.float32
 
+WHOLE = 66 * 1000 * 1000
+
 VMEM = pl.BlockSpec(memory_space=pltpu.VMEM)
 SMEM = pl.BlockSpec(memory_space=pltpu.SMEM)
 HBM = pl.BlockSpec(memory_space=pltpu.HBM)
@@ -47,14 +49,14 @@
     return (c == SLICE * z + 4 * j + k).astype(f32).astype(bf16)
 
 
-def call(kernel, out, in_specs, flops, scratch=()):
+def call(kernel, out, in_specs, flops, scratch=(), limit=48 * 1024 * 1024):
     return pl.pallas_call(
         kernel,
         out_shape=out,
         in_specs=in_specs,
         out_specs=jax.tree.map(lambda _: VMEM, out),
         scratch_shapes=list(scratch),
-        compiler_params=pltpu.CompilerParams(vmem_limit_bytes=48 * 1024 * 1024),
+        compiler_params=pltpu.CompilerParams(vmem_limit_bytes=limit),
         cost_estimate=pl.CostEstimate(flops=flops, bytes_accessed=1 << 20, transcendentals=0),
     )
 
@@ -70,57 +72,34 @@
 ALL_WIDTH = sum(WIDTHS)
 
 
-def chunk_copies(part, matrices, buffers, sems):
-    return [
-        [
-            pltpu.make_async_copy(
-                w.at[pl.ds(pl.multiple_of((2 * x + part) * RD, RD), RD), :],
-                buf.at[x],
-                sems.at[x, k],
-            )
-            for k, (w, buf) in enumerate(zip(matrices, buffers))
-        ]
-        for x in range(4)
+def project_kernel(pos, lam, own, other, cos, sin, columns, *refs):
+    matrices, outs, buf, scaled, sums, sems = refs[:6], refs[6:12], *refs[12:16]
+    kv, states, sq, tq, tk, rv = outs
+    copies = [
+        pltpu.make_async_copy(w, buf.at[:, s : s + n], sems.at[k])
+        for k, (w, s, n) in enumerate(zip(matrices, STARTS, WIDTHS))
     ]
-
-
-def projected(copies, feats, buffers, sums, squares):
-    for x in range(4):
-        raw = feats[x, :ROWS, :].astype(f32)
-        gain = feats[x, ROWS : ROWS + 1, :].astype(f32)
-        squares = squares + raw * raw
-        scaled = (raw * gain).astype(bf16)
-        for copy in copies[x]:
-            copy.wait()
-        for k, buf in enumerate(buffers):
-            new = mm(scaled, buf[x])
-            sums[k] = new if sums[k] is None else sums[k] + new
-    return sums, squares
-
-
-def first_half_kernel(pos, feats, *refs):
-    matrices, (sums, squares), buffers, sems = refs[:6], refs[6:8], refs[8:14], refs[14]
-    copies = chunk_copies(pos[2], matrices, buffers, sems)
-    for per_chunk in copies:
-        for copy in per_chunk:
-            copy.start()
-    out, square = projected(copies, feats, buffers, [None] * 6, jnp.zeros((ROWS, RD), f32))
-    for k in range(6):
-        sums[:, STARTS[k] : STARTS[k] + WIDTHS[k]] = out[k]
-    squares[...] = square
-
-
-def second_half_kernel(pos, lam, feats, before, before_squares, cos, sin, columns, *refs):
-    matrices, outs, buffers, sems = refs[:6], refs[6:12], refs[12:18], refs[18]
-    kv, states, sq, tq, tk, rv = outs
-    copies = chunk_copies(1 - pos[2], matrices, buffers, sems)
-    for per_chunk in copies:
-        for copy in per_chunk:
-            copy.start()
-    start = [before[:, STARTS[k] : STARTS[k] + WIDTHS[k]] for k in range(6)]
-    sums, squares = projected(copies, feats, buffers, start, before_squares[...])
+    for copy in copies:
+        copy.start()
+    squares = jnp.zeros((ROWS, RD), f32)
+    for part, ref in ((pos[2], own), (1 - pos[2], other)):
+        for x in range(4):
+            raw = ref[x, :ROWS, :].astype(f32)
+            gain = ref[x, ROWS : ROWS + 1, :].astype(f32)
+            squares = squares + raw * raw
+            col = pl.multiple_of((2 * x + part) * RD, RD)
+            scaled[:, pl.ds(col, RD)] = (raw * gain).astype(bf16)
+    ready = 0
+    for left in range(0, ALL_WIDTH, RD):
+        right = min(left + RD, ALL_WIDTH)
+        while ready < 6 and STARTS[ready] < right:
+            copies[ready].wait()
+            ready += 1
+        sums[:, left:right] = mm(scaled[...], buf[:, left:right])
     scale = lax.rsqrt(jnp.sum(squares, axis=1, keepdims=True) / D + epsilon)
-    sq_v, sk_v, sv_v, rq_v, rk_v, rv_v = [(s * scale).astype(bf16) for s in sums]
+    sq_v, sk_v, sv_v, rq_v, rk_v, rv_v = [
+        (sums[:, s : s + n] * scale).astype(bf16) for s, n in zip(STARTS, WIDTHS)
+    ]
     kv[:, :SD] = sk_v
     kv[:, SD:] = sv_v
     sq[...] = sq_v
@@ -346,7 +325,7 @@
     ret_cols = ret_out_w.T
     columns = jnp.concatenate([stick_out_w.T, ret_cols[:, :SD], ret_cols[:, SD:]], axis=0)
 
-    piece = call(piece_kernel, sds((4, ROWS + 8, RD), bf16), [VMEM, VMEM], 1000)(
+    piece = call(piece_kernel, sds((4, ROWS + 8, RD), bf16), [VMEM, VMEM], 1000, (), WHOLE)(
         inputs, input_gain[None, :]
     )
     own = to_all(piece, "x")
@@ -358,16 +337,8 @@
     angles = position[:, None] * inverse[None, :]
 
     matrices = (stick_query_w, stick_key_w, stick_value_w, ret_query_w, ret_key_w, ret_value_w)
-    buffers = [pltpu.VMEM((4, RD, w), bf16) for w in WIDTHS] + [pltpu.SemaphoreType.DMA((4, 6))]
-    sums, squares = call(
-        first_half_kernel,
-        (sds((ROWS, ALL_WIDTH), f32), sds((ROWS, RD), f32)),
-        [SMEM, VMEM] + [HBM] * 6,
-        600000000,
-        buffers,
-    )(pos, own, *matrices)
     kv, states, sq, tq, tk, rv = call(
-        second_half_kernel,
+        project_kernel,
         (
             sds((ROWS, 2 * SD), bf16),
             sds((NY, 2 * SLICE + 96, SD), bf16),
@@ -376,15 +347,20 @@
             sds((ROWS, RD), bf16),
             sds((ROWS, RD), bf16),
         ),
-        [SMEM, SMEM] + [VMEM] * 6 + [HBM] * 6,
-        600000000,
-        buffers,
+        [SMEM, SMEM] + [VMEM] * 5 + [HBM] * 6,
+        1200000000,
+        [
+            pltpu.VMEM((D, ALL_WIDTH), bf16),
+            pltpu.VMEM((ROWS, D), bf16),
+            pltpu.VMEM((ROWS, ALL_WIDTH), f32),
+            pltpu.SemaphoreType.DMA((6,)),
+        ],
+        WHOLE,
     )(
         pos,
         ret_log_decay,
+        own,
         other,
-        sums,
-        squares,
         jnp.cos(angles),
         jnp.sin(angles),
         columns,
@@ -429,6 +405,7 @@
             pltpu.VMEM((NY, ROWS, 2 * SD), bf16),
             pltpu.SemaphoreType.DMA((NY,)),
         ],
+        WHOLE,
     )(pos, stick_offset, row_kv, col_q)
     parts = to_all(parts, "z")
 
@@ -450,6 +427,7 @@
         [VMEM] * 4 + [HBM],
         400000000,
         [pltpu.VMEM((NZ, NY, 96, SD), bf16), pltpu.SemaphoreType.DMA((NZ,))],
+        WHOLE,
     )(
         total, squares, stick_gain[None, :], ret_normed, weights
     )

time: 189 us -> 183 us (0.968)
  local copies, waits for them, and re-layouts: 10.4 us -> 5.84 us
  Pallas kernels: 35.1 us -> 32.3 us
  blocking collectives: 34 us -> 36.3 us
    pallas_call x3 -> x2, Pallas kernels: 13.6 us -> 8.75 us  [the longest x1 7 us: body(): call(project_kernel, (sds((ROWS, 2 * SD), bf16), sds((NY, 2 * SLICE + 96,...]
    unnamed x24 -> x30, local copies, waits for them, and re-layouts: 8.2 us -> 3.9 us
    all_to_all x3, blocking collectives: 34 us -> 36.3 us  [to_all(): return lax.all_to_all(x, axis, 0, 0, tiled=True)]
  transfers between devices with their start and end apart: 8 -> 8, of which waited for: 5 -> 5; matrix products, arithmetic and copies ran while one was open for 1% -> 2% of each run, Pallas kernels for 12% -> 10%
where the time goes in v3:
time: 183 us; the launch traced here: 182 us
  waiting for transfers between devices  50.2 us (27%)
  starting transfers between devices  39.2 us (21%)
  blocking collectives  36.3 us (20%)
  Pallas kernels  32.3 us (18%)
  between operations  14.9 us (8%)
  local copies, waits for them, and re-layouts  5.84 us (3%)
  other arithmetic  3.53 us (2%)
    all_to_all x5, waiting for transfers between devices, to_all(): return lax.all_to_all(x, axis, 0, 0, tiled=True)  50.1 us
    all_to_all x3, blocking collectives, to_all(): return lax.all_to_all(x, axis, 0, 0, tiled=True)  36.3 us
    all_to_all x5, starting transfers between devices, to_all(): return lax.all_to_all(x, axis, 0, 0, tiled=True)  30.7 us
    pallas_call x1, Pallas kernels, body(): call(stick_kernel, sds((NZ, ROWS + 8, SD), bf16), [SMEM, SMEM, HBM, VMEM]...  13.6 us
    ppermute x1, starting transfers between devices, body(): other = lax.ppermute(own, 'c', [(0, 1), (1, 0)])  8.5 us
    pallas_call x1, Pallas kernels, body(): call(project_kernel, (sds((ROWS, 2 * SD), bf16), sds((NY, 2 * SLICE + 96,...  7 us
    pallas_call x1, Pallas kernels, body(): call(output_kernel, sds((2, 4, 32, D), bf16), [VMEM] * 4 + [HBM], 4000000...  5.55 us
    unnamed x30, local copies, waits for them, and re-layouts  3.9 us
  transfers between devices with their start and end apart: 8, of which 5 were waited for; matrix products, arithmetic and copies ran while one was open for 2% of the time, Pallas kernels for 10%

profile of v3, /device:TPU:1, one launch (start us, length us, event | category | flops | bytes accessed | tf_op | source)
XLA Modules:
  0.0 182.3 jit_solution(6919261934186795861)
XLA Ops:
  6.5 1.2 broadcast_in_dim.11.gain
  7.8 1.8 shard_map.145
  9.5 4.8 %all-to-all-start = ((bf16[4,264,256]{2,1,0:T(8,128)(2,1)}), bf16[4,264,256]{2,1,0:T(8,128)(2,1)S(1)}, u32[]{:S(2)}, u32[]{:S(2)}) async-start(bf16[4,264,256]{2,1,0:T(8,128)(2,1)} %shard_map.145), calls=%async_computation | async-start | bytes 1081344 | tf_op jit(solution)/shard_map/all_to_all | solution.py:301
  15.0 0.6 pad_add_fusion.pos
  15.7 5.7 %all-to-all-done.own = bf16[4,264,256]{2,1,0:T(8,128)(2,1)S(1)} async-done(((bf16[4,264,256]{2,1,0:T(8,128)(2,1)}), bf16[4,264,256]{2,1,0:T(8,128)(2,1)S(1)}, u32[]{:S(2)}, u32[]{:S(2)}) %all-to-all-start) | async-done | bytes 540704 | tf_op jit(solution)/shard_map/all_to_all | solution.py:301
  21.4 8.5 %collective-permute-start = (bf16[4,264,256]{2,1,0:T(8,128)(2,1)S(1)}, bf16[4,264,256]{2,1,0:T(8,128)(2,1)S(1)}, u32[]{:S(2)}, u32[]{:S(2)}) collective-permute-start(bf16[4,264,256]{2,1,0:T(8,128)(2,1)S(1)} %all-to-all-done.own), channel_id=1, source_target_pairs={{0,1},{1,0},{2,3},{3,2},{4,5},{5,4},{6,7},{7,6},{8,9},{9,8},{10,11... | collective-permute-start | bytes 1622024 | tf_op jit(solution)/shard_map/ppermute | solution.py:332
  29.9 0.6 pad_maximum_fusion.columns
  30.5 1.2 multiply_sine_fusion
  31.8 0.8 copy-done.10
  32.6 7.0 %shard_map.146 = (bf16[256,256]{1,0:T(8,128)(2,1)}, bf16[8,160,128]{2,1,0:T(8,128)(2,1)}, bf16[256,128]{1,0:T(8,128)(2,1)}, bf16[256,256]{1,0:T(8,128)(2,1)}, bf...) custom-call(s32[3]{0:T(128)} %pad_add_fusion.pos, f32[1]{0:T(128)S(6)} %copy.17.lam, bf16[4,264,256]{2,1,0:T(8,128)(2,1)} %copy-done.9, ...), custom_call_target="tpu_custom_call" | custom-call | flops 1200000000 | bytes 1048576 | tf_op jit(solution)/shard_map/pallas_call | solution.py:340
  39.6 3.8 %all-to-all-start.1 = ((bf16[8,160,128]{2,1,0:T(8,128)(2,1)}), bf16[8,160,128]{2,1,0:T(8,128)(2,1)S(1)}, u32[]{:S(2)}, u32[]{:S(2)}) async-start(bf16[8,160,128]{2,1,0:T(8,128)(2,1)} %get-tuple-element.16), calls=%async_computation.1 | async-start | bytes 655360 | tf_op jit(solution)/shard_map/all_to_all | solution.py:301
  43.5 13.7 %all-to-all-done.1.states = bf16[8,160,128]{2,1,0:T(8,128)(2,1)S(1)} async-done(((bf16[8,160,128]{2,1,0:T(8,128)(2,1)}), bf16[8,160,128]{2,1,0:T(8,128)(2,1)S(1)}, u32[]{:S(2)}, u32[]{:S(2)}) %all-to-all-start.1) | async-done | bytes 327712 | tf_op jit(solution)/shard_map/all_to_all | solution.py:301
  57.2 0.8 copy-done.4
  58.1 0.9 shard_map.147
  59.0 11.6 %all-to-all-start.2 = ((bf16[8,328,128]{2,1,0:T(8,128)(2,1)}), bf16[8,328,128]{2,1,0:T(8,128)(2,1)S(1)}, u32[]{:S(2)}, u32[]{:S(2)}) async-start(bf16[8,328,128]{2,1,0:T(8,128)(2,1)} %shard_map.147), calls=%async_computation.2 | async-start | bytes 1343488 | tf_op jit(solution)/shard_map/all_to_all | solution.py:301
  70.6 0.7 slice.24
  71.4 20.4 %all-to-all-done.2.zq = bf16[8,328,128]{2,1,0:T(8,128)(2,1)S(1)} async-done(((bf16[8,328,128]{2,1,0:T(8,128)(2,1)}), bf16[8,328,128]{2,1,0:T(8,128)(2,1)S(1)}, u32[]{:S(2)}, u32[]{:S(2)}) %all-to-all-start.2) | async-done | bytes 671776 | tf_op jit(solution)/shard_map/all_to_all | solution.py:301
  91.7 1.3 shard_map.148
  93.0 3.4 %all-to-all-start.3 = ((bf16[8,32,256]{2,1,0:T(8,128)(2,1)}), bf16[8,32,256]{2,1,0:T(8,128)(2,1)S(1)}, u32[]{:S(2)}, u32[]{:S(2)}) async-start(bf16[8,32,256]{2,1,0:T(8,128)(2,1)} %shard_map.148), calls=%async_computation.3 | async-start | bytes 262144 | tf_op jit(solution)/shard_map/all_to_all | solution.py:301
  97.0 7.4 %all-to-all-done.3.entering = bf16[8,32,256]{2,1,0:T(8,128)(2,1)S(1)} async-done(((bf16[8,32,256]{2,1,0:T(8,128)(2,1)}), bf16[8,32,256]{2,1,0:T(8,128)(2,1)S(1)}, u32[]{:S(2)}, u32[]{:S(2)}) %all-to-all-start.3) | async-done | bytes 131104 | tf_op jit(solution)/shard_map/all_to_all | solution.py:301
  104.4 13.6 %shard_map.149 = bf16[8,264,128]{2,1,0:T(8,128)(2,1)} custom-call(s32[3]{0:T(128)} %pad_add_fusion.pos, f32[1]{0:T(128)S(6)} %copy.16.off, bf16[8,256,256]{2,1,0:T(8,128)(2,1)} %bitcast.16, bf16[8,328,128]{2,1,0:T(8,128)(2,1)} %copy-done), custom_call_target="tpu_custom_call" | custom-call | flops 4000000000 | bytes 1048576 | tf_op jit(solution)/shard_map/pallas_call | solution.py:394
  118.1 18.6 %all_to_all.40.parts = bf16[8,264,128]{2,1,0:T(8,128)(2,1)S(1)} all-to-all(bf16[8,264,128]{2,1,0:T(8,128)(2,1)} %shard_map.149), channel_id=1, replica_groups=mesh['z'=8,'y'=8,'x'=4,'c'=2] {'z'}, dimensions={0} | all-to-all | bytes 1081344 | tf_op jit(solution)/shard_map/all_to_all | solution.py:301
  136.6 1.3 shard_map.150
  137.9 0.7 copy-done.2
  138.6 7.0 %all-to-all-start.5 = ((f32[8,8,256]{2,1,0:T(8,128)}), f32[8,8,256]{2,1,0:T(8,128)S(1)}, u32[]{:S(2)}, u32[]{:S(2)}) async-start(f32[8,8,256]{2,1,0:T(8,128)} %get-tuple-element.20), calls=%async_computation.5 | async-start | bytes 131072 | tf_op jit(solution)/shard_map/all_to_all | solution.py:301
  146.9 0.6 copy-done.1
  147.5 3.0 %all-to-all-done.5.squares = f32[8,8,256]{2,1,0:T(8,128)S(1)} async-done(((f32[8,8,256]{2,1,0:T(8,128)}), f32[8,8,256]{2,1,0:T(8,128)S(1)}, u32[]{:S(2)}, u32[]{:S(2)}) %all-to-all-start.5) | async-done | bytes 65568 | tf_op jit(solution)/shard_map/all_to_all | solution.py:301
  150.5 0.6 copy-done.11
  151.1 5.6 %shard_map.153 = bf16[2,4,32,2048]{3,2,1,0:T(8,128)(2,1)} custom-call(f32[256,128]{1,0:T(8,128)} %copy-done.2, f32[8,8,256]{2,1,0:T(8,128)} %copy-done.11, f32[1,128]{1,0:T(1,128)} %bitcast.15, bf16[256,256]{1,0:T(8,128)(2,1)} %copy-done.1, bf16[8,8,96,128]{3,2,1,0:T(8,128)(2,1)} %bitcast.11), custom_call_target="tpu_custom_call" | custom-call | flops 400000000 | bytes 1048576 | tf_op jit(solution)/shard_map/pallas_call | solution.py:424
  156.7 6.1 %all_to_all.41 = bf16[2,4,32,2048]{3,2,1,0:T(8,128)(2,1)S(1)} all-to-all(bf16[2,4,32,2048]{3,2,1,0:T(8,128)(2,1)} %shard_map.153), channel_id=1, replica_groups=mesh['z'=8,'y'=8,'x'=4,'c'=2] {'c'}, dimensions={0} | all-to-all | bytes 2097152 | tf_op jit(solution)/shard_map/all_to_all | solution.py:301
  163.1 11.6 %all_to_all.42 = bf16[4,32,2048]{2,1,0:T(8,128)(2,1)S(1)} all-to-all(bf16[4,32,2048]{2,1,0:T(8,128)(2,1)S(1)} %reduce_sum.24), channel_id=1, replica_groups=mesh['z'=8,'y'=8,'x'=4,'c'=2] {'x'}, dimensions={0} | all-to-all | bytes 1048576 | tf_op jit(solution)/shard_map/all_to_all | solution.py:301
  174.7 0.7 reduce_sum.25
  (40 shorter events, 1.7 us)
Async XLA Ops:
  6.5 23.4 %copy-start.12 = (bf16[256,32]{0,1:T(8,128)(2,1)S(1)}, bf16[256,32]{0,1:T(8,128)(2,1)}, u32[]{:S(2)}) copy-start(bf16[256,32]{0,1:T(8,128)(2,1)} %param.29) | copy-start | bytes 49156
  6.5 23.4 %copy-start.13 = (bf16[128,32]{0,1:T(8,128)(2,1)S(1)}, bf16[128,32]{0,1:T(8,128)(2,1)}, u32[]{:S(2)}) copy-start(bf16[128,32]{0,1:T(8,128)(2,1)} %param.28) | copy-start | bytes 24580
  9.5 11.9 %all-to-all-start = ((bf16[4,264,256]{2,1,0:T(8,128)(2,1)}), bf16[4,264,256]{2,1,0:T(8,128)(2,1)S(1)}, u32[]{:S(2)}, u32[]{:S(2)}) async-start(bf16[4,264,256]{2,1,0:T(8,128)(2,1)} %shard_map.145), calls=%async_computation | async-start | bytes 1081344 | tf_op jit(solution)/shard_map/all_to_all | solution.py:301
  14.4 82.7 %all-gather.5.cloned.1.call-start = ((), (), s32[]{:S(2)}) async-start(), calls=%async_computation.8 | async-start | bytes 1179648 | tf_op jit(solution)/shard_map/all_gather | solution.py:370
  21.4 11.2 %copy-start.9 = (bf16[4,264,256]{2,1,0:T(8,128)(2,1)}, bf16[4,264,256]{2,1,0:T(8,128)(2,1)S(1)}, u32[]{:S(2)}) copy-start(bf16[4,264,256]{2,1,0:T(8,128)(2,1)S(1)} %all-to-all-done.own) | copy-start | bytes 1622020
  21.4 10.4 %collective-permute-start = (bf16[4,264,256]{2,1,0:T(8,128)(2,1)S(1)}, bf16[4,264,256]{2,1,0:T(8,128)(2,1)S(1)}, u32[]{:S(2)}, u32[]{:S(2)}) collective-permute-start(bf16[4,264,256]{2,1,0:T(8,128)(2,1)S(1)} %all-to-all-done.own), channel_id=1, source_target_pairs={{0,1},{1,0},{2,3},{3,2},{4,5},{5,4},{6,7},{7,6},{8,9},{9,8},{10,11... | collective-permute-start | bytes 1622024 | tf_op jit(solution)/shard_map/ppermute | solution.py:332
  31.8 0.8 copy-start.10
  32.6 10.9 %copy-start.14 = (f32[1,4,256]{2,1,0:T(4,128)S(1)}, f32[1,4,256]{2,1,0:T(4,128)}, u32[]{:S(2)}) copy-start(f32[1,4,256]{2,1,0:T(4,128)} %param.25) | copy-start | bytes 12292
  39.6 17.6 %all-to-all-start.1 = ((bf16[8,160,128]{2,1,0:T(8,128)(2,1)}), bf16[8,160,128]{2,1,0:T(8,128)(2,1)S(1)}, u32[]{:S(2)}, u32[]{:S(2)}) async-start(bf16[8,160,128]{2,1,0:T(8,128)(2,1)} %get-tuple-element.16), calls=%async_computation.1 | async-start | bytes 655360 | tf_op jit(solution)/shard_map/all_to_all | solution.py:301
  43.4 48.3 %copy-start.5 = (s32[3]{0:T(128)S(1)}, s32[3]{0:T(128)}, u32[]{:S(2)}) copy-start(s32[3]{0:T(128)} %pad_add_fusion.pos) | copy-start | bytes 40
  57.2 0.8 copy-start.4
  59.0 32.7 %all-to-all-start.2 = ((bf16[8,328,128]{2,1,0:T(8,128)(2,1)}), bf16[8,328,128]{2,1,0:T(8,128)(2,1)S(1)}, u32[]{:S(2)}, u32[]{:S(2)}) async-start(bf16[8,328,128]{2,1,0:T(8,128)(2,1)} %shard_map.147), calls=%async_computation.2 | async-start | bytes 1343488 | tf_op jit(solution)/shard_map/all_to_all | solution.py:301
  70.6 79.9 %all-gather.7.cloned.1.call-start = ((), (), s32[]{:S(2)}) async-start(), calls=%async_computation.9 | async-start | bytes 1769472 | tf_op jit(solution)/shard_map/all_gather | solution.py:372
  91.7 12.7 %copy-start = (bf16[8,328,128]{2,1,0:T(8,128)(2,1)}, bf16[8,328,128]{2,1,0:T(8,128)(2,1)S(1)}, u32[]{:S(2)}) copy-start(bf16[8,328,128]{2,1,0:T(8,128)(2,1)S(1)} %all-to-all-done.2.zq) | copy-start | bytes 2015236
  93.0 11.4 %all-to-all-start.3 = ((bf16[8,32,256]{2,1,0:T(8,128)(2,1)}), bf16[8,32,256]{2,1,0:T(8,128)(2,1)S(1)}, u32[]{:S(2)}, u32[]{:S(2)}) async-start(bf16[8,32,256]{2,1,0:T(8,128)(2,1)} %shard_map.148), calls=%async_computation.3 | async-start | bytes 262144 | tf_op jit(solution)/shard_map/all_to_all | solution.py:301
  118.0 27.6 %copy-start.3 = (bf16[256,256]{1,0:T(8,128)(2,1)S(1)}, bf16[256,256]{1,0:T(8,128)(2,1)}, u32[]{:S(2)}) copy-start(bf16[256,256]{1,0:T(8,128)(2,1)} %get-tuple-element.21.tq) | copy-start | bytes 393220
  118.0 27.6 %copy-start.7 = (bf16[256,256]{1,0:T(8,128)(2,1)S(1)}, bf16[256,256]{1,0:T(8,128)(2,1)}, u32[]{:S(2)}) copy-start(bf16[256,256]{1,0:T(8,128)(2,1)} %get-tuple-element.22.tk) | copy-start | bytes 393220
  118.0 27.6 %copy-start.8 = (bf16[256,256]{1,0:T(8,128)(2,1)S(1)}, bf16[256,256]{1,0:T(8,128)(2,1)}, u32[]{:S(2)}) copy-start(bf16[256,256]{1,0:T(8,128)(2,1)} %get-tuple-element.23.rv) | copy-start | bytes 393220
  137.9 0.7 copy-start.2
  138.6 11.9 %all-to-all-start.5 = ((f32[8,8,256]{2,1,0:T(8,128)}), f32[8,8,256]{2,1,0:T(8,128)S(1)}, u32[]{:S(2)}, u32[]{:S(2)}) async-start(f32[8,8,256]{2,1,0:T(8,128)} %get-tuple-element.20), calls=%async_computation.5 | async-start | bytes 131072 | tf_op jit(solution)/shard_map/all_to_all | solution.py:301
  145.6 0.7 copy-start.6
  146.9 0.6 copy-start.1
  150.5 0.6 copy-start.11
Sparse Core Ops, SparseCore 0:
  39.8 35.1 all-gather.4
  77.1 42.2 all-gather.6

commit v4 on v3

--- a/solution.py
+++ b/solution.py
@@ -1,5 +1,3 @@
-import functools
-
 import jax
 import jax.numpy as jnp
 from jax import lax
@@ -8,6 +6,7 @@
 from jax.sharding import Mesh
 from jax.sharding import PartitionSpec as P
 
+
 D = 2048
 STICK_WIDTH = 1024
 ROWS = 256
@@ -15,7 +14,6 @@
 RD = 256
 NZ = 8
 NY = 8
-SLICE = RD // NY
 LOG2E = 1.4426950408889634
 
 SP = ("z", "y")
@@ -42,11 +40,9 @@
     return lax.broadcasted_iota(jnp.int32, shape, dim)
 
 
-def slice_order():
-    r = iota((RD, RD), 0)
-    c = iota((RD, RD), 1)
-    j, z, k = r // SLICE, (r % SLICE) // 4, r % 4
-    return (c == SLICE * z + 4 * j + k).astype(f32).astype(bf16)
+def spread(h):
+    r = iota((2 * RD, RD), 0)
+    return ((r // 8 * 4 + r % 4 == iota((2 * RD, RD), 1)) & (r // 4 % 2 == h)).astype(f32).astype(bf16)
 
 
 def call(kernel, out, in_specs, flops, scratch=(), limit=48 * 1024 * 1024):
@@ -67,17 +63,11 @@
         out[x, ROWS:, :] = jnp.broadcast_to(gain[...], (8, RD))
 
 
-WIDTHS = (SD, SD, SD, RD, RD, RD)
-STARTS = (0, SD, 2 * SD, 3 * SD, 3 * SD + RD, 3 * SD + 2 * RD)
-ALL_WIDTH = sum(WIDTHS)
-
-
-def project_kernel(pos, lam, own, other, cos, sin, columns, *refs):
-    matrices, outs, buf, scaled, sums, sems = refs[:6], refs[6:12], *refs[12:16]
-    kv, states, sq, tq, tk, rv = outs
+def three_products(pos, own, other, matrices, buf, scaled, sums, sems):
+    width = buf.shape[1] // 3
     copies = [
-        pltpu.make_async_copy(w, buf.at[:, s : s + n], sems.at[k])
-        for k, (w, s, n) in enumerate(zip(matrices, STARTS, WIDTHS))
+        pltpu.make_async_copy(w, buf.at[:, k * width : (k + 1) * width], sems.at[k])
+        for k, w in enumerate(matrices)
     ]
     for copy in copies:
         copy.start()
@@ -90,20 +80,30 @@
             col = pl.multiple_of((2 * x + part) * RD, RD)
             scaled[:, pl.ds(col, RD)] = (raw * gain).astype(bf16)
     ready = 0
-    for left in range(0, ALL_WIDTH, RD):
-        right = min(left + RD, ALL_WIDTH)
-        while ready < 6 and STARTS[ready] < right:
+    for left in range(0, 3 * width, RD):
+        right = min(left + RD, 3 * width)
+        while ready < 3 and ready * width < right:
             copies[ready].wait()
             ready += 1
         sums[:, left:right] = mm(scaled[...], buf[:, left:right])
     scale = lax.rsqrt(jnp.sum(squares, axis=1, keepdims=True) / D + epsilon)
-    sq_v, sk_v, sv_v, rq_v, rk_v, rv_v = [
-        (sums[:, s : s + n] * scale).astype(bf16) for s, n in zip(STARTS, WIDTHS)
-    ]
-    kv[:, :SD] = sk_v
-    kv[:, SD:] = sv_v
-    sq[...] = sq_v
-    rv[...] = rv_v
+    return [(sums[:, k * width : (k + 1) * width] * scale).astype(bf16) for k in range(3)]
+
+
+def stick_project_kernel(pos, own, other, columns, wq, wk, wv, kv, queries, *work):
+    query, key, value = three_products(pos, own, other, (wq, wk, wv), *work)
+    kv[:, :SD] = key
+    kv[:, SD:] = value
+    for z in range(NZ):
+        queries[z, :ROWS, :] = query
+        queries[z, ROWS:, :] = columns[...]
+
+
+def ret_project_kernel(
+    pos, lam, own, other, cos, sin, wq, wk, wv, states, tq, tk, rv, *work
+):
+    query, key, value = three_products(pos, own, other, (wq, wk, wv), *work)
+    rv[...] = value
     cosine, sine = cos[...], sin[...]
     half = RD // 2
 
@@ -111,18 +111,14 @@
         a, b = v[:, :half].astype(f32), v[:, half:].astype(f32)
         return jnp.concatenate([a * cosine - b * sine, b * cosine + a * sine], axis=1)
 
-    tq[...] = turn(rq_v).astype(bf16)
-    key = turn(rk_v) * (RD**-0.5)
+    tq[...] = turn(query).astype(bf16)
+    key = turn(key) * (RD**-0.5)
     tk[...] = key.astype(bf16)
     left = (ROWS - 1 - iota((ROWS, RD), 0)).astype(f32)
     decayed = (key * jnp.exp(lam[0] * left)).astype(bf16)
-    state = mm(decayed, rv_v, ((0,), (0,))).astype(bf16)
-    ordered = mm(slice_order(), state).astype(bf16)
-    for y in range(NY):
-        rows = slice(SLICE * y, SLICE * (y + 1))
-        states[y, :SLICE, :] = ordered[rows, :SD]
-        states[y, SLICE : 2 * SLICE, :] = ordered[rows, SD:]
-        states[y, 2 * SLICE :, :] = columns[...]
+    state = mm(decayed, value, ((0,), (0,))).astype(bf16)
+    slices = mm(spread(0), state[:, :SD]) + mm(spread(1), state[:, SD:])
+    states[...] = slices.astype(bf16).reshape(NZ * NY, 8, SD)
 
 
 def inner_kernel(lam, tq, tk, rv, inner):
@@ -132,42 +128,12 @@
     inner[...] = mm(scores.astype(bf16), rv[...])
 
 
-def halves(ref, i, top):
-    return jnp.concatenate(
-        [ref[i, top : top + SLICE, :], ref[i, top + SLICE : top + 2 * SLICE, :]], axis=1
-    ).astype(f32)
-
-
-def totals_kernel(lam, states, sq, init, out):
-    step = jnp.exp(jnp.full((1, RD), lam[0] * ROWS, f32))
-    run = jnp.zeros((SLICE, RD), f32)
-    for y in range(NY):
-        run = run * step + halves(states, y, 0)
-    total = run.astype(bf16)
-    first = init[...].astype(bf16)
-    for z in range(NZ):
-        out[z, :ROWS, :] = sq[...]
-        out[z, ROWS : ROWS + SLICE, :] = total[:, :SD]
-        out[z, ROWS + SLICE : ROWS + 2 * SLICE, :] = total[:, SD:]
-        out[z, ROWS + 2 * SLICE :, :] = first
-
-
-def entering_kernel(pos, lam, states, zq, out, start):
-    mine = pos[0]
-    step = jnp.exp(jnp.full((1, RD), lam[0] * ROWS, f32))
-    row_step = jnp.exp(jnp.full((1, RD), lam[0] * (ROWS * NY), f32))
-    top = ROWS + 2 * SLICE
-    for z in range(NZ):
-        both = zq[z, top : top + 8, :].astype(f32)
-        start[4 * z : 4 * z + 4, :SD] = both[:4]
-        start[4 * z : 4 * z + 4, SD:] = both[4:]
-    before = start[...]
-    for z in range(NZ):
-        before = jnp.where(z < mine, before * row_step + halves(zq, z, ROWS), before)
-    run = before
-    for y in range(NY):
-        out[y, :, :] = run.astype(bf16)
-        run = run * step + halves(states, y, 0)
+def scan_kernel(lam, states, first, out):
+    step = jnp.exp(jnp.full((8, SD), lam[0] * ROWS, f32))
+    run = first[...]
+    for b in range(NZ * NY):
+        out[b, :, :] = run.astype(bf16)
+        run = run * step + states[b].astype(f32)
 
 
 PAIR = 2
@@ -261,19 +227,17 @@
 
 
 def retain_kernel(lam, tq, inner, entering, gain, out):
-    turned = mm(tq[...], slice_order(), ((1,), (1,))).astype(bf16)
-    state = jnp.concatenate([entering[y] for y in range(NY)], axis=0)
+    slices = entering[...].reshape(2 * RD, SD)
+    state = [mm(spread(h), slices, ((0,), (0,))).astype(bf16) for h in range(2)]
+    state = jnp.concatenate(state, axis=1)
     steps = (iota((ROWS, RD), 0) + 1).astype(f32)
-    value = inner[...] + mm(turned, state) * jnp.exp(lam[0] * steps)
+    value = inner[...] + mm(tq[...], state) * jnp.exp(lam[0] * steps)
     value = value - jnp.mean(value, axis=1, keepdims=True)
     value = value * lax.rsqrt(jnp.mean(value * value, axis=1, keepdims=True) + epsilon)
     out[...] = (value * gain[...]).astype(bf16)
 
 
-def output_kernel(total, squares, gain, ret, weights, out, local, sems):
-    copies = [pltpu.make_async_copy(weights.at[n], local.at[n], sems.at[n]) for n in range(NZ)]
-    for copy in copies:
-        copy.start()
+def output_kernel(total, squares, gain, ret, weights, out):
     mean = jnp.zeros((8, ROWS), f32)
     for t in range(8):
         mean = mean + squares[t]
@@ -284,10 +248,9 @@
     both = jnp.concatenate([stick, ret[...]], axis=1)
     for n in range(8):
         cols = slice(n * 256, (n + 1) * 256)
-        copies[n].wait()
         block = jnp.concatenate(
             [
-                jnp.concatenate([local[n, y, 32 * b : 32 * b + 32, :] for y in range(NY)], axis=0)
+                jnp.concatenate([weights[y, n, 32 * b : 32 * b + 32, :] for y in range(NY)], axis=0)
                 for b in range(3)
             ],
             axis=1,
@@ -336,56 +299,53 @@
     inverse = rope_base ** (-jnp.arange(half, dtype=f32) / half)
     angles = position[:, None] * inverse[None, :]
 
-    matrices = (stick_query_w, stick_key_w, stick_value_w, ret_query_w, ret_key_w, ret_value_w)
-    kv, states, sq, tq, tk, rv = call(
-        project_kernel,
-        (
-            sds((ROWS, 2 * SD), bf16),
-            sds((NY, 2 * SLICE + 96, SD), bf16),
-            sds((ROWS, SD), bf16),
-            sds((ROWS, RD), bf16),
-            sds((ROWS, RD), bf16),
-            sds((ROWS, RD), bf16),
-        ),
-        [SMEM, SMEM] + [VMEM] * 5 + [HBM] * 6,
-        1200000000,
-        [
-            pltpu.VMEM((D, ALL_WIDTH), bf16),
+    def work(width):
+        return [
+            pltpu.VMEM((D, 3 * width), bf16),
             pltpu.VMEM((ROWS, D), bf16),
-            pltpu.VMEM((ROWS, ALL_WIDTH), f32),
-            pltpu.SemaphoreType.DMA((6,)),
-        ],
+            pltpu.VMEM((ROWS, 3 * width), f32),
+            pltpu.SemaphoreType.DMA((3,)),
+        ]
+
+    kv, queries = call(
+        stick_project_kernel,
+        (sds((ROWS, 2 * SD), bf16), sds((NZ, ROWS + 96, SD), bf16)),
+        [SMEM] + [VMEM] * 3 + [HBM] * 3,
+        400000000,
+        work(SD),
         WHOLE,
-    )(
+    )(pos, own, other, columns, stick_query_w, stick_key_w, stick_value_w)
+    ret_project = call(
+        ret_project_kernel,
+        (sds((NZ * NY, 8, SD), bf16),) + (sds((ROWS, RD), bf16),) * 3,
+        [SMEM, SMEM] + [VMEM] * 4 + [HBM] * 3,
+        6000000000,
+        work(RD),
+        WHOLE,
+    )
+    cosine, sine = jnp.cos(angles), jnp.sin(angles)
+    states, tq, tk, rv = ret_project(
         pos,
         ret_log_decay,
         own,
         other,
-        jnp.cos(angles),
-        jnp.sin(angles),
-        columns,
-        *matrices,
+        cosine,
+        sine,
+        ret_query_w,
+        ret_key_w,
+        ret_value_w,
     )
 
     row_kv = lax.all_gather(kv, "y", axis=0)
-    states = to_all(states, "y")
-    weights = lax.all_gather(states[:, 2 * SLICE :, :], "z", axis=0)
+    col_q = to_all(queries, "z")
+    weights = lax.all_gather(col_q[:, ROWS:, :], "y", axis=0)
 
     first = initial_state.reshape(4, RD)
     first = jnp.concatenate([first[:, :SD], first[:, SD:]], axis=0)
-    zq = call(
-        totals_kernel, sds((NZ, ROWS + 2 * SLICE + 8, SD), bf16), [SMEM] + [VMEM] * 3, 10000000
-    )(ret_log_decay, states, sq, first)
-    col_q = to_all(zq, "z")
-
-    slices = call(
-        entering_kernel,
-        sds((NY, SLICE, RD), bf16),
-        [SMEM, SMEM, VMEM, VMEM],
-        10000000,
-        [pltpu.VMEM((SLICE, RD), f32)],
-    )(pos, ret_log_decay, states, col_q)
-    entering = to_all(slices, "y")
+    slices = call(scan_kernel, sds((NZ * NY, 8, SD), bf16), [SMEM, VMEM, VMEM], 1000000)(
+        ret_log_decay, to_all(states, SP), first
+    )
+    entering = to_all(slices, SP)
     inner = call(inner_kernel, sds((ROWS, RD), f32), [SMEM] + [VMEM] * 3, 2000000000)(
         ret_log_decay, tq, tk, rv
     )
@@ -424,10 +384,8 @@
     out = call(
         output_kernel,
         sds((2, 4, 32, D), bf16),
-        [VMEM] * 4 + [HBM],
+        [VMEM] * 5,
         400000000,
-        [pltpu.VMEM((NZ, NY, 96, SD), bf16), pltpu.SemaphoreType.DMA((NZ,))],
-        WHOLE,
     )(
         total, squares, stick_gain[None, :], ret_normed, weights
     )

time: 183 us -> 184 us (level)
  blocking collectives: 36.3 us -> 45.7 us
  starting transfers between devices: 39.2 us -> 36.4 us
  Pallas kernels: 32.3 us -> 30.1 us
  local copies, waits for them, and re-layouts: 5.84 us -> 3.76 us
    all_to_all x3 -> x4, blocking collectives: 36.3 us -> 45.7 us  [to_all(): return lax.all_to_all(x, axis, 0, 0, tiled=True)]
    all_to_all x5 -> x4, starting transfers between devices: 30.7 us -> 27.9 us  [to_all(): return lax.all_to_all(x, axis, 0, 0, tiled=True)]
    pallas_call x4, Pallas kernels: 14.8 us -> 12.1 us  [the longest x1 5.8 us: body(): ret_project(pos, ret_log_decay, own, other, cosine, sine, ret_query_w, re...]
    unnamed x30 -> x22, local copies, waits for them, and re-layouts: 3.9 us -> 1.74 us
    all_to_all x5 -> x4, waiting for transfers between devices: 50.1 us -> 48 us  [to_all(): return lax.all_to_all(x, axis, 0, 0, tiled=True)]
  transfers between devices with their start and end apart: 8 -> 7, of which waited for: 5 -> 5; matrix products, arithmetic and copies ran while one was open for 2% -> 2% of each run, Pallas kernels for 10% -> 12%
where the time goes in v4:
time: 184 us; the launch traced here: 183 us
  waiting for transfers between devices  48.5 us (26%)
  blocking collectives  45.7 us (25%)
  starting transfers between devices  36.4 us (20%)
  Pallas kernels  30.1 us (16%)
  between operations  14.9 us (8%)
  local copies, waits for them, and re-layouts  3.76 us (2%)
  other arithmetic  3.55 us (2%)
    all_to_all x4, waiting for transfers between devices, to_all(): return lax.all_to_all(x, axis, 0, 0, tiled=True)  48 us
    all_to_all x4, blocking collectives, to_all(): return lax.all_to_all(x, axis, 0, 0, tiled=True)  45.7 us
    all_to_all x4, starting transfers between devices, to_all(): return lax.all_to_all(x, axis, 0, 0, tiled=True)  27.9 us
    pallas_call x1, Pallas kernels, body(): call(stick_kernel, sds((NZ, ROWS + 8, SD), bf16), [SMEM, SMEM, HBM, VMEM]...  13.7 us
    ppermute x1, starting transfers between devices, body(): other = lax.ppermute(own, 'c', [(0, 1), (1, 0)])  8.49 us
    pallas_call x1, Pallas kernels, body(): ret_project(pos, ret_log_decay, own, other, cosine, sine, ret_query_w, re...  5.8 us
    pallas_call x1, Pallas kernels, body(): call(stick_project_kernel, (sds((ROWS, 2 * SD), bf16), sds((NZ, ROWS + 96...  4.73 us
  transfers between devices with their start and end apart: 7, of which 5 were waited for; matrix products, arithmetic and copies ran while one was open for 2% of the time, Pallas kernels for 12%

profile of v4, /device:TPU:1, one launch (start us, length us, event | category | flops | bytes accessed | tf_op | source)
XLA Modules:
  0.0 182.9 jit_solution(15835010945735034615)
XLA Ops:
  6.5 1.2 broadcast_in_dim.11.gain
  7.8 1.8 shard_map.145
  9.5 11.9 %all_to_all.40.own = bf16[4,264,256]{2,1,0:T(8,128)(2,1)S(1)} all-to-all(bf16[4,264,256]{2,1,0:T(8,128)(2,1)} %shard_map.145), channel_id=1, replica_groups=mesh['z'=8,'y'=8,'x'=4,'c'=2] {'x'}, dimensions={0} | all-to-all | bytes 1081344 | tf_op jit(solution)/shard_map/all_to_all | solution.py:264
  21.4 8.5 %collective-permute-start = (bf16[4,264,256]{2,1,0:T(8,128)(2,1)S(1)}, bf16[4,264,256]{2,1,0:T(8,128)(2,1)}, u32[]{:S(2)}, u32[]{:S(2)}) collective-permute-start(bf16[4,264,256]{2,1,0:T(8,128)(2,1)S(1)} %all_to_all.40.own), channel_id=1, source_target_pairs={{0,1},{1,0},{2,3},{3,2},{4,5},{5,4},{6,7},{7,6},{8,9},{9,8},{10,11... | collective-permute-start | bytes 1622024 | tf_op jit(solution)/shard_map/ppermute | solution.py:295
  29.9 0.6 pad_add_fusion.pos
  30.5 0.6 pad_maximum_fusion.columns
  31.1 0.4 collective-permute-done.other
  31.6 4.7 %shard_map.146 = (bf16[256,256]{1,0:T(8,128)(2,1)}, bf16[8,352,128]{2,1,0:T(8,128)(2,1)}) custom-call(s32[3]{0:T(128)} %pad_add_fusion.pos, bf16[4,264,256]{2,1,0:T(8,128)(2,1)} %copy-done.6, bf16[4,264,256]{2,1,0:T(8,128)(2,1)} %collective-permute-done.other, bf16[96,128]{1,0:T(8,128)(2,1)} %pad_maximum_fusion.columns, bf16[2048,128]{1,0:T(8,128)(2,1)} %wq.2, ...), custom_call_target="tpu_custom_call" | custom-call | flops 400000000 | bytes 1048576 | tf_op jit(solution)/shard_map/pallas_call | solution.py:310
  36.3 7.0 %all-to-all-start.3 = ((bf16[8,352,128]{2,1,0:T(8,128)(2,1)}), bf16[8,352,128]{2,1,0:T(8,128)(2,1)S(1)}, u32[]{:S(2)}, u32[]{:S(2)}) async-start(bf16[8,352,128]{2,1,0:T(8,128)(2,1)} %get-tuple-element.18), calls=%async_computation.3 | async-start | bytes 1441792 | tf_op jit(solution)/shard_map/all_to_all | solution.py:264
  43.5 22.1 %all-to-all-done.3.zq = bf16[8,352,128]{2,1,0:T(8,128)(2,1)S(1)} async-done(((bf16[8,352,128]{2,1,0:T(8,128)(2,1)}), bf16[8,352,128]{2,1,0:T(8,128)(2,1)S(1)}, u32[]{:S(2)}, u32[]{:S(2)}) %all-to-all-start.3) | async-done | bytes 720928 | tf_op jit(solution)/shard_map/all_to_all | solution.py:264
  65.5 0.8 slice.24
  66.3 1.3 multiply_sine_fusion
  68.3 5.8 %shard_map.147 = (bf16[64,8,128]{2,1,0:T(8,128)(2,1)}, bf16[256,256]{1,0:T(8,128)(2,1)}, bf16[256,256]{1,0:T(8,128)(2,1)}, bf16[256,256]{1,0:T(8,128)(2,1)}) custom-call(s32[3]{0:T(128)} %pad_add_fusion.pos, f32[1]{0:T(128)S(6)} %copy.17.lam, bf16[4,264,256]{2,1,0:T(8,128)(2,1)} %copy-done.6, bf16[4,264,256]{2,1,0:T(8,128)(2,1)} %collective-permute-done.other, ...), custom_call_target="tpu_custom_call" | custom-call | flops 6000000000 | bytes 1048576 | tf_op jit(solution)/shard_map/pallas_call | solution.py:327
  74.1 7.8 %all-to-all-start.1 = ((bf16[64,8,128]{2,1,0:T(8,128)(2,1)}), bf16[64,8,128]{2,1,0:T(8,128)(2,1)S(1)}, u32[]{:S(2)}, u32[]{:S(2)}) async-start(bf16[64,8,128]{2,1,0:T(8,128)(2,1)} %get-tuple-element.16), calls=%async_computation.1 | async-start | bytes 262144 | tf_op jit(solution)/shard_map/all_to_all | solution.py:264
  82.0 11.5 %all-to-all-done.1.states = bf16[64,8,128]{2,1,0:T(8,128)(2,1)S(1)} async-done(((bf16[64,8,128]{2,1,0:T(8,128)(2,1)}), bf16[64,8,128]{2,1,0:T(8,128)(2,1)S(1)}, u32[]{:S(2)}, u32[]{:S(2)}) %all-to-all-start.1) | async-done | bytes 131104 | tf_op jit(solution)/shard_map/all_to_all | solution.py:264
  93.5 0.8 shard_map.148
  94.3 4.6 %all-to-all-start.2 = ((bf16[64,8,128]{2,1,0:T(8,128)(2,1)}), bf16[64,8,128]{2,1,0:T(8,128)(2,1)S(1)}, u32[]{:S(2)}, u32[]{:S(2)}) async-start(bf16[64,8,128]{2,1,0:T(8,128)(2,1)} %shard_map.148), calls=%async_computation.2 | async-start | bytes 262144 | tf_op jit(solution)/shard_map/all_to_all | solution.py:264
  99.5 11.1 %all-to-all-done.2.entering = bf16[64,8,128]{2,1,0:T(8,128)(2,1)S(1)} async-done(((bf16[64,8,128]{2,1,0:T(8,128)(2,1)}), bf16[64,8,128]{2,1,0:T(8,128)(2,1)S(1)}, u32[]{:S(2)}, u32[]{:S(2)}) %all-to-all-start.2) | async-done | bytes 131104 | tf_op jit(solution)/shard_map/all_to_all | solution.py:264
  110.6 13.7 %shard_map.149 = bf16[8,264,128]{2,1,0:T(8,128)(2,1)} custom-call(s32[3]{0:T(128)} %pad_add_fusion.pos, f32[1]{0:T(128)S(6)} %copy.16.off, bf16[8,256,256]{2,1,0:T(8,128)(2,1)} %bitcast.16, bf16[8,352,128]{2,1,0:T(8,128)(2,1)} %copy-done.7), custom_call_target="tpu_custom_call" | custom-call | flops 4000000000 | bytes 1048576 | tf_op jit(solution)/shard_map/pallas_call | solution.py:354
  124.4 17.2 %all_to_all.41.parts = bf16[8,264,128]{2,1,0:T(8,128)(2,1)S(1)} all-to-all(bf16[8,264,128]{2,1,0:T(8,128)(2,1)} %shard_map.149), channel_id=1, replica_groups=mesh['z'=8,'y'=8,'x'=4,'c'=2] {'z'}, dimensions={0} | all-to-all | bytes 1081344 | tf_op jit(solution)/shard_map/all_to_all | solution.py:264
  141.7 1.3 shard_map.150
  143.0 8.4 %all-to-all-start.5 = ((f32[8,8,256]{2,1,0:T(8,128)}), f32[8,8,256]{2,1,0:T(8,128)S(1)}, u32[]{:S(2)}, u32[]{:S(2)}) async-start(f32[8,8,256]{2,1,0:T(8,128)} %get-tuple-element.20), calls=%async_computation.5 | async-start | bytes 131072 | tf_op jit(solution)/shard_map/all_to_all | solution.py:264
  151.4 0.4 shard_map.151.inner
  151.8 0.3 copy-done.2
  152.1 0.8 shard_map.152.ret
  152.9 3.3 %all-to-all-done.5.squares = f32[8,8,256]{2,1,0:T(8,128)S(1)} async-done(((f32[8,8,256]{2,1,0:T(8,128)}), f32[8,8,256]{2,1,0:T(8,128)S(1)}, u32[]{:S(2)}, u32[]{:S(2)}) %all-to-all-start.5) | async-done | bytes 65568 | tf_op jit(solution)/shard_map/all_to_all | solution.py:264
  156.2 1.4 copy-done
  157.6 0.8 shard_map.153
  158.4 5.0 %all_to_all.42 = bf16[2,4,32,2048]{3,2,1,0:T(8,128)(2,1)S(1)} all-to-all(bf16[2,4,32,2048]{3,2,1,0:T(8,128)(2,1)S(1)} %shard_map.153), channel_id=1, replica_groups=mesh['z'=8,'y'=8,'x'=4,'c'=2] {'c'}, dimensions={0} | all-to-all | bytes 2097152 | tf_op jit(solution)/shard_map/all_to_all | solution.py:264
  163.4 0.3 reduce_sum.24
  163.7 11.6 %all_to_all.43 = bf16[4,32,2048]{2,1,0:T(8,128)(2,1)S(1)} all-to-all(bf16[4,32,2048]{2,1,0:T(8,128)(2,1)S(1)} %reduce_sum.24), channel_id=1, replica_groups=mesh['z'=8,'y'=8,'x'=4,'c'=2] {'x'}, dimensions={0} | all-to-all | bytes 1048576 | tf_op jit(solution)/shard_map/all_to_all | solution.py:264
  175.3 0.7 reduce_sum.25
  (31 shorter events, 0.2 us)
Async XLA Ops:
  6.5 24.0 %copy-start.8 = (bf16[256,32]{0,1:T(8,128)(2,1)S(1)}, bf16[256,32]{0,1:T(8,128)(2,1)}, u32[]{:S(2)}) copy-start(bf16[256,32]{0,1:T(8,128)(2,1)} %param.29) | copy-start | bytes 49156
  6.5 24.0 %copy-start.9 = (bf16[128,32]{0,1:T(8,128)(2,1)S(1)}, bf16[128,32]{0,1:T(8,128)(2,1)}, u32[]{:S(2)}) copy-start(bf16[128,32]{0,1:T(8,128)(2,1)} %param.28) | copy-start | bytes 24580
  6.5 104.1 %all-gather.5.cloned.1.call-start = ((), (), s32[]{:S(2)}) async-start(), calls=%async_computation.8 | async-start | bytes 1179648 | tf_op jit(solution)/shard_map/all_gather | solution.py:339
  21.4 10.2 %copy-start.6 = (bf16[4,264,256]{2,1,0:T(8,128)(2,1)}, bf16[4,264,256]{2,1,0:T(8,128)(2,1)S(1)}, u32[]{:S(2)}) copy-start(bf16[4,264,256]{2,1,0:T(8,128)(2,1)S(1)} %all_to_all.40.own) | copy-start | bytes 1622020
  21.4 10.2 %collective-permute-start = (bf16[4,264,256]{2,1,0:T(8,128)(2,1)S(1)}, bf16[4,264,256]{2,1,0:T(8,128)(2,1)}, u32[]{:S(2)}, u32[]{:S(2)}) collective-permute-start(bf16[4,264,256]{2,1,0:T(8,128)(2,1)S(1)} %all_to_all.40.own), channel_id=1, source_target_pairs={{0,1},{1,0},{2,3},{3,2},{4,5},{5,4},{6,7},{7,6},{8,9},{9,8},{10,11... | collective-permute-start | bytes 1622024 | tf_op jit(solution)/shard_map/ppermute | solution.py:295
  36.3 29.2 %all-to-all-start.3 = ((bf16[8,352,128]{2,1,0:T(8,128)(2,1)}), bf16[8,352,128]{2,1,0:T(8,128)(2,1)S(1)}, u32[]{:S(2)}, u32[]{:S(2)}) async-start(bf16[8,352,128]{2,1,0:T(8,128)(2,1)} %get-tuple-element.18), calls=%async_computation.3 | async-start | bytes 1441792 | tf_op jit(solution)/shard_map/all_to_all | solution.py:264
  43.4 112.9 %all-gather.7.cloned.1.call-start = ((), (), s32[]{:S(2)}) async-start(), calls=%async_computation.9 | async-start | bytes 1769472 | tf_op jit(solution)/shard_map/all_gather | solution.py:341
  65.5 8.5 %copy-start.7 = (bf16[8,352,128]{2,1,0:T(8,128)(2,1)}, bf16[8,352,128]{2,1,0:T(8,128)(2,1)S(1)}, u32[]{:S(2)}) copy-start(bf16[8,352,128]{2,1,0:T(8,128)(2,1)S(1)} %all-to-all-done.3.zq) | copy-start | bytes 2162692
  68.3 13.7 %copy-start.10 = (f32[1,4,256]{2,1,0:T(4,128)S(1)}, f32[1,4,256]{2,1,0:T(4,128)}, u32[]{:S(2)}) copy-start(f32[1,4,256]{2,1,0:T(4,128)} %param.25) | copy-start | bytes 12292
  74.1 19.4 %all-to-all-start.1 = ((bf16[64,8,128]{2,1,0:T(8,128)(2,1)}), bf16[64,8,128]{2,1,0:T(8,128)(2,1)S(1)}, u32[]{:S(2)}, u32[]{:S(2)}) async-start(bf16[64,8,128]{2,1,0:T(8,128)(2,1)} %get-tuple-element.16), calls=%async_computation.1 | async-start | bytes 262144 | tf_op jit(solution)/shard_map/all_to_all | solution.py:264
  94.3 16.4 %all-to-all-start.2 = ((bf16[64,8,128]{2,1,0:T(8,128)(2,1)}), bf16[64,8,128]{2,1,0:T(8,128)(2,1)S(1)}, u32[]{:S(2)}, u32[]{:S(2)}) async-start(bf16[64,8,128]{2,1,0:T(8,128)(2,1)} %shard_map.148), calls=%async_computation.2 | async-start | bytes 262144 | tf_op jit(solution)/shard_map/all_to_all | solution.py:264
  124.4 27.0 %copy-start.1 = (bf16[256,256]{1,0:T(8,128)(2,1)S(1)}, bf16[256,256]{1,0:T(8,128)(2,1)}, u32[]{:S(2)}) copy-start(bf16[256,256]{1,0:T(8,128)(2,1)} %get-tuple-element.21.tq) | copy-start | bytes 393220
  124.4 27.0 %copy-start.4 = (bf16[256,256]{1,0:T(8,128)(2,1)S(1)}, bf16[256,256]{1,0:T(8,128)(2,1)}, u32[]{:S(2)}) copy-start(bf16[256,256]{1,0:T(8,128)(2,1)} %get-tuple-element.22.tk) | copy-start | bytes 393220
  124.4 27.0 %copy-start.5 = (bf16[256,256]{1,0:T(8,128)(2,1)S(1)}, bf16[256,256]{1,0:T(8,128)(2,1)}, u32[]{:S(2)}) copy-start(bf16[256,256]{1,0:T(8,128)(2,1)} %get-tuple-element.23.rv) | copy-start | bytes 393220
  143.0 13.3 %all-to-all-start.5 = ((f32[8,8,256]{2,1,0:T(8,128)}), f32[8,8,256]{2,1,0:T(8,128)S(1)}, u32[]{:S(2)}, u32[]{:S(2)}) async-start(f32[8,8,256]{2,1,0:T(8,128)} %get-tuple-element.20), calls=%async_computation.5 | async-start | bytes 131072 | tf_op jit(solution)/shard_map/all_to_all | solution.py:264
  151.4 0.7 copy-start.2
  151.4 4.8 %copy-start.3 = (f32[128]{0:T(128)S(1)}, f32[128]{0:T(128)}, u32[]{:S(2)}) copy-start(f32[128]{0:T(128)} %param.26) | copy-start | bytes 1540
  156.2 1.4 copy-start
Sparse Core Ops, SparseCore 0:
  36.5 35.3 all-gather.4
  74.0 43.1 all-gather.6

commit v5 on v4

--- a/solution.py
+++ b/solution.py
@@ -60,7 +60,7 @@
 def piece_kernel(inputs, gain, out):
     for x in range(4):
         out[x, :ROWS, :] = inputs[...]
-        out[x, ROWS:, :] = jnp.broadcast_to(gain[...], (8, RD))
+        out[x, ROWS:, :] = jnp.broadcast_to(gain[...][None, :], (8, RD))
 
 
 def three_products(pos, own, other, matrices, buf, scaled, sums, sems):
@@ -289,7 +289,7 @@
     columns = jnp.concatenate([stick_out_w.T, ret_cols[:, :SD], ret_cols[:, SD:]], axis=0)
 
     piece = call(piece_kernel, sds((4, ROWS + 8, RD), bf16), [VMEM, VMEM], 1000, (), WHOLE)(
-        inputs, input_gain[None, :]
+        inputs, input_gain
     )
     own = to_all(piece, "x")
     other = lax.ppermute(own, "c", [(0, 1), (1, 0)])
@@ -350,8 +350,7 @@
         ret_log_decay, tq, tk, rv
     )
 
-    row_kv, entering = lax.optimization_barrier((row_kv, entering))
-    parts = call(
+    stick = call(
         stick_kernel,
         sds((NZ, ROWS + 8, SD), bf16),
         [SMEM, SMEM, HBM, VMEM],
@@ -366,7 +365,9 @@
             pltpu.SemaphoreType.DMA((NY,)),
         ],
         WHOLE,
-    )(pos, stick_offset, row_kv, col_q)
+    )
+    parts = stick(pos, stick_offset, row_kv, col_q)
+    parts, entering = lax.optimization_barrier((parts, entering))
     parts = to_all(parts, "z")
 
     total, squares = call(

time: 184 us -> 170 us (0.924)
  waiting for transfers between devices: 48.5 us -> 36.1 us
    all_to_all x4, waiting for transfers between devices: 48 us -> 35.6 us  [to_all(): return lax.all_to_all(x, axis, 0, 0, tiled=True)]
  transfers between devices with their start and end apart: 7 -> 7, of which waited for: 5 -> 4; matrix products, arithmetic and copies ran while one was open for 2% -> 2% of each run, Pallas kernels for 12% -> 13%
where the time goes in v5:
time: 170 us; the launch traced here: 169 us
  blocking collectives  46.7 us (27%)
  waiting for transfers between devices  36.1 us (21%)
  starting transfers between devices  35.3 us (21%)
  Pallas kernels  30.1 us (18%)
  between operations  14.9 us (9%)
  other arithmetic  3.55 us (2%)
  local copies, waits for them, and re-layouts  2.51 us (1%)
    all_to_all x4, blocking collectives, to_all(): return lax.all_to_all(x, axis, 0, 0, tiled=True)  46.7 us
    all_to_all x4, waiting for transfers between devices, to_all(): return lax.all_to_all(x, axis, 0, 0, tiled=True)  35.6 us
    all_to_all x4, starting transfers between devices, to_all(): return lax.all_to_all(x, axis, 0, 0, tiled=True)  26.8 us
    pallas_call x1, Pallas kernels, body(): parts = stick(pos, stick_offset, row_kv, col_q)  13.7 us
    ppermute x1, starting transfers between devices, body(): other = lax.ppermute(own, 'c', [(0, 1), (1, 0)])  8.49 us
    pallas_call x1, Pallas kernels, body(): ret_project(pos, ret_log_decay, own, other, cosine, sine, ret_query_w, re...  5.82 us
    pallas_call x1, Pallas kernels, body(): call(stick_project_kernel, (sds((ROWS, 2 * SD), bf16), sds((NZ, ROWS + 96...  4.73 us
  transfers between devices with their start and end apart: 7, of which 4 were waited for; matrix products, arithmetic and copies ran while one was open for 2% of the time, Pallas kernels for 13%

profile of v5, /device:TPU:1, one launch (start us, length us, event | category | flops | bytes accessed | tf_op | source)
XLA Modules:
  0.0 169.3 jit_solution(1817849325754942885)
XLA Ops:
  6.5 1.8 %shard_map.145 = bf16[4,264,256]{2,1,0:T(8,128)(2,1)} custom-call(bf16[256,256]{1,0:T(8,128)(2,1)} %inputs.1, bf16[256]{0:T(256)(128)(2,1)} %gain.1), custom_call_target="tpu_custom_call" | custom-call | flops 1000 | bytes 1048576 | tf_op jit(solution)/shard_map/pallas_call | solution.py:291
  8.3 11.9 %all_to_all.40.own = bf16[4,264,256]{2,1,0:T(8,128)(2,1)S(1)} all-to-all(bf16[4,264,256]{2,1,0:T(8,128)(2,1)} %shard_map.145), channel_id=1, replica_groups=mesh['z'=8,'y'=8,'x'=4,'c'=2] {'x'}, dimensions={0} | all-to-all | bytes 1081344 | tf_op jit(solution)/shard_map/all_to_all | solution.py:264
  20.2 8.5 %collective-permute-start = (bf16[4,264,256]{2,1,0:T(8,128)(2,1)S(1)}, bf16[4,264,256]{2,1,0:T(8,128)(2,1)}, u32[]{:S(2)}, u32[]{:S(2)}) collective-permute-start(bf16[4,264,256]{2,1,0:T(8,128)(2,1)S(1)} %all_to_all.40.own), channel_id=1, source_target_pairs={{0,1},{1,0},{2,3},{3,2},{4,5},{5,4},{6,7},{7,6},{8,9},{9,8},{10,11... | collective-permute-start | bytes 1622024 | tf_op jit(solution)/shard_map/ppermute | solution.py:295
  28.7 0.6 pad_add_fusion.pos
  29.3 0.6 pad_maximum_fusion.columns
  29.9 0.4 collective-permute-done.other
  30.4 4.7 %shard_map.146 = (bf16[256,256]{1,0:T(8,128)(2,1)}, bf16[8,352,128]{2,1,0:T(8,128)(2,1)}) custom-call(s32[3]{0:T(128)} %pad_add_fusion.pos, bf16[4,264,256]{2,1,0:T(8,128)(2,1)} %copy-done.6, bf16[4,264,256]{2,1,0:T(8,128)(2,1)} %collective-permute-done.other, bf16[96,128]{1,0:T(8,128)(2,1)} %pad_maximum_fusion.columns, bf16[2048,128]{1,0:T(8,128)(2,1)} %wq.2, ...), custom_call_target="tpu_custom_call" | custom-call | flops 400000000 | bytes 1048576 | tf_op jit(solution)/shard_map/pallas_call | solution.py:310
  35.1 7.0 %all-to-all-start.1 = ((bf16[8,352,128]{2,1,0:T(8,128)(2,1)}), bf16[8,352,128]{2,1,0:T(8,128)(2,1)S(1)}, u32[]{:S(2)}, u32[]{:S(2)}) async-start(bf16[8,352,128]{2,1,0:T(8,128)(2,1)} %get-tuple-element.16), calls=%async_computation.1 | async-start | bytes 1441792 | tf_op jit(solution)/shard_map/all_to_all | solution.py:264
  42.2 0.0 all-gather.7.cloned.1.call-start
  43.5 20.8 %all-to-all-done.1.zq = bf16[8,352,128]{2,1,0:T(8,128)(2,1)S(1)} async-done(((bf16[8,352,128]{2,1,0:T(8,128)(2,1)}), bf16[8,352,128]{2,1,0:T(8,128)(2,1)S(1)}, u32[]{:S(2)}, u32[]{:S(2)}) %all-to-all-start.1) | async-done | bytes 720928 | tf_op jit(solution)/shard_map/all_to_all | solution.py:264
  64.3 0.8 slice.24
  65.1 1.3 multiply_sine_fusion
  66.4 5.8 %shard_map.148 = (bf16[64,8,128]{2,1,0:T(8,128)(2,1)}, bf16[256,256]{1,0:T(8,128)(2,1)}, bf16[256,256]{1,0:T(8,128)(2,1)}, bf16[256,256]{1,0:T(8,128)(2,1)}) custom-call(s32[3]{0:T(128)} %pad_add_fusion.pos, f32[1]{0:T(128)S(6)} %copy.17.lam, bf16[4,264,256]{2,1,0:T(8,128)(2,1)} %copy-done.6, bf16[4,264,256]{2,1,0:T(8,128)(2,1)} %collective-permute-done.other, ...), custom_call_target="tpu_custom_call" | custom-call | flops 6000000000 | bytes 1048576 | tf_op jit(solution)/shard_map/pallas_call | solution.py:327
  72.2 7.8 %all-to-all-start.2 = ((bf16[64,8,128]{2,1,0:T(8,128)(2,1)}), bf16[64,8,128]{2,1,0:T(8,128)(2,1)S(1)}, u32[]{:S(2)}, u32[]{:S(2)}) async-start(bf16[64,8,128]{2,1,0:T(8,128)(2,1)} %get-tuple-element.17), calls=%async_computation.2 | async-start | bytes 262144 | tf_op jit(solution)/shard_map/all_to_all | solution.py:264
  80.1 11.5 %all-to-all-done.2.states = bf16[64,8,128]{2,1,0:T(8,128)(2,1)S(1)} async-done(((bf16[64,8,128]{2,1,0:T(8,128)(2,1)}), bf16[64,8,128]{2,1,0:T(8,128)(2,1)S(1)}, u32[]{:S(2)}, u32[]{:S(2)}) %all-to-all-start.2) | async-done | bytes 131104 | tf_op jit(solution)/shard_map/all_to_all | solution.py:264
  91.6 0.8 shard_map.149
  92.4 4.6 %all-to-all-start.3 = ((bf16[64,8,128]{2,1,0:T(8,128)(2,1)}), bf16[64,8,128]{2,1,0:T(8,128)(2,1)S(1)}, u32[]{:S(2)}, u32[]{:S(2)}) async-start(bf16[64,8,128]{2,1,0:T(8,128)(2,1)} %shard_map.149), calls=%async_computation.3 | async-start | bytes 262144 | tf_op jit(solution)/shard_map/all_to_all | solution.py:264
  97.0 0.0 all-gather.5.cloned.1.call-done
  97.0 13.7 %shard_map.147 = bf16[8,264,128]{2,1,0:T(8,128)(2,1)} custom-call(s32[3]{0:T(128)} %pad_add_fusion.pos, f32[1]{0:T(128)S(6)} %copy.16.off, bf16[8,256,256]{2,1,0:T(8,128)(2,1)} %bitcast.16, bf16[8,352,128]{2,1,0:T(8,128)(2,1)} %copy-done.7), custom_call_target="tpu_custom_call" | custom-call | flops 4000000000 | bytes 1048576 | tf_op jit(solution)/shard_map/pallas_call | solution.py:369
  110.8 18.3 %all_to_all.41.parts = bf16[8,264,128]{2,1,0:T(8,128)(2,1)S(1)} all-to-all(bf16[8,264,128]{2,1,0:T(8,128)(2,1)} %shard_map.147), channel_id=1, replica_groups=mesh['z'=8,'y'=8,'x'=4,'c'=2] {'z'}, dimensions={0} | all-to-all | bytes 1081344 | tf_op jit(solution)/shard_map/all_to_all | solution.py:264
  129.1 1.3 shard_map.150
  130.4 7.3 %all-to-all-start.5 = ((f32[8,8,256]{2,1,0:T(8,128)}), f32[8,8,256]{2,1,0:T(8,128)S(1)}, u32[]{:S(2)}, u32[]{:S(2)}) async-start(f32[8,8,256]{2,1,0:T(8,128)} %get-tuple-element.20), calls=%async_computation.5 | async-start | bytes 131072 | tf_op jit(solution)/shard_map/all_to_all | solution.py:264
  137.8 0.4 shard_map.151.inner
  138.2 0.3 copy-done.2
  138.4 0.8 shard_map.152.ret
  139.3 3.3 %all-to-all-done.5.squares = f32[8,8,256]{2,1,0:T(8,128)S(1)} async-done(((f32[8,8,256]{2,1,0:T(8,128)}), f32[8,8,256]{2,1,0:T(8,128)S(1)}, u32[]{:S(2)}, u32[]{:S(2)}) %all-to-all-start.5) | async-done | bytes 65568 | tf_op jit(solution)/shard_map/all_to_all | solution.py:264
  142.6 1.4 copy-done
  144.0 0.8 shard_map.153
  144.8 5.0 %all_to_all.42 = bf16[2,4,32,2048]{3,2,1,0:T(8,128)(2,1)S(1)} all-to-all(bf16[2,4,32,2048]{3,2,1,0:T(8,128)(2,1)S(1)} %shard_map.153), channel_id=1, replica_groups=mesh['z'=8,'y'=8,'x'=4,'c'=2] {'c'}, dimensions={0} | all-to-all | bytes 2097152 | tf_op jit(solution)/shard_map/all_to_all | solution.py:264
  149.8 0.3 reduce_sum.24
  150.1 11.6 %all_to_all.43 = bf16[4,32,2048]{2,1,0:T(8,128)(2,1)S(1)} all-to-all(bf16[4,32,2048]{2,1,0:T(8,128)(2,1)S(1)} %reduce_sum.24), channel_id=1, replica_groups=mesh['z'=8,'y'=8,'x'=4,'c'=2] {'x'}, dimensions={0} | all-to-all | bytes 1048576 | tf_op jit(solution)/shard_map/all_to_all | solution.py:264
  161.7 0.7 reduce_sum.25
  (30 shorter events, 0.1 us)
Async XLA Ops:
  6.5 22.8 %copy-start.8 = (bf16[256,32]{0,1:T(8,128)(2,1)S(1)}, bf16[256,32]{0,1:T(8,128)(2,1)}, u32[]{:S(2)}) copy-start(bf16[256,32]{0,1:T(8,128)(2,1)} %param.29) | copy-start | bytes 49156
  6.5 22.8 %copy-start.9 = (bf16[128,32]{0,1:T(8,128)(2,1)S(1)}, bf16[128,32]{0,1:T(8,128)(2,1)}, u32[]{:S(2)}) copy-start(bf16[128,32]{0,1:T(8,128)(2,1)} %param.28) | copy-start | bytes 24580
  6.5 90.5 %all-gather.5.cloned.1.call-start = ((), (), s32[]{:S(2)}) async-start(), calls=%async_computation.8 | async-start | bytes 1179648 | tf_op jit(solution)/shard_map/all_gather | solution.py:339
  20.2 10.2 %copy-start.6 = (bf16[4,264,256]{2,1,0:T(8,128)(2,1)}, bf16[4,264,256]{2,1,0:T(8,128)(2,1)S(1)}, u32[]{:S(2)}) copy-start(bf16[4,264,256]{2,1,0:T(8,128)(2,1)S(1)} %all_to_all.40.own) | copy-start | bytes 1622020
  20.2 10.2 %collective-permute-start = (bf16[4,264,256]{2,1,0:T(8,128)(2,1)S(1)}, bf16[4,264,256]{2,1,0:T(8,128)(2,1)}, u32[]{:S(2)}, u32[]{:S(2)}) collective-permute-start(bf16[4,264,256]{2,1,0:T(8,128)(2,1)S(1)} %all_to_all.40.own), channel_id=1, source_target_pairs={{0,1},{1,0},{2,3},{3,2},{4,5},{5,4},{6,7},{7,6},{8,9},{9,8},{10,11... | collective-permute-start | bytes 1622024 | tf_op jit(solution)/shard_map/ppermute | solution.py:295
  35.1 29.2 %all-to-all-start.1 = ((bf16[8,352,128]{2,1,0:T(8,128)(2,1)}), bf16[8,352,128]{2,1,0:T(8,128)(2,1)S(1)}, u32[]{:S(2)}, u32[]{:S(2)}) async-start(bf16[8,352,128]{2,1,0:T(8,128)(2,1)} %get-tuple-element.16), calls=%async_computation.1 | async-start | bytes 1441792 | tf_op jit(solution)/shard_map/all_to_all | solution.py:264
  42.2 100.5 %all-gather.7.cloned.1.call-start = ((), (), s32[]{:S(2)}) async-start(), calls=%async_computation.9 | async-start | bytes 1769472 | tf_op jit(solution)/shard_map/all_gather | solution.py:341
  64.3 7.9 %copy-start.7 = (bf16[8,352,128]{2,1,0:T(8,128)(2,1)}, bf16[8,352,128]{2,1,0:T(8,128)(2,1)S(1)}, u32[]{:S(2)}) copy-start(bf16[8,352,128]{2,1,0:T(8,128)(2,1)S(1)} %all-to-all-done.1.zq) | copy-start | bytes 2162692
  66.4 13.7 %copy-start.10 = (f32[1,4,256]{2,1,0:T(4,128)S(1)}, f32[1,4,256]{2,1,0:T(4,128)}, u32[]{:S(2)}) copy-start(f32[1,4,256]{2,1,0:T(4,128)} %param.25) | copy-start | bytes 12292
  72.2 19.4 %all-to-all-start.2 = ((bf16[64,8,128]{2,1,0:T(8,128)(2,1)}), bf16[64,8,128]{2,1,0:T(8,128)(2,1)S(1)}, u32[]{:S(2)}, u32[]{:S(2)}) async-start(bf16[64,8,128]{2,1,0:T(8,128)(2,1)} %get-tuple-element.17), calls=%async_computation.2 | async-start | bytes 262144 | tf_op jit(solution)/shard_map/all_to_all | solution.py:264
  92.4 18.4 %all-to-all-start.3 = ((bf16[64,8,128]{2,1,0:T(8,128)(2,1)}), bf16[64,8,128]{2,1,0:T(8,128)(2,1)S(1)}, u32[]{:S(2)}, u32[]{:S(2)}) async-start(bf16[64,8,128]{2,1,0:T(8,128)(2,1)} %shard_map.149), calls=%async_computation.3 | async-start | bytes 262144 | tf_op jit(solution)/shard_map/all_to_all | solution.py:264
  110.8 27.0 %copy-start.1 = (bf16[256,256]{1,0:T(8,128)(2,1)S(1)}, bf16[256,256]{1,0:T(8,128)(2,1)}, u32[]{:S(2)}) copy-start(bf16[256,256]{1,0:T(8,128)(2,1)} %get-tuple-element.21.tq) | copy-start | bytes 393220
  110.8 27.0 %copy-start.4 = (bf16[256,256]{1,0:T(8,128)(2,1)S(1)}, bf16[256,256]{1,0:T(8,128)(2,1)}, u32[]{:S(2)}) copy-start(bf16[256,256]{1,0:T(8,128)(2,1)} %get-tuple-element.22.tk) | copy-start | bytes 393220
  110.8 27.0 %copy-start.5 = (bf16[256,256]{1,0:T(8,128)(2,1)S(1)}, bf16[256,256]{1,0:T(8,128)(2,1)}, u32[]{:S(2)}) copy-start(bf16[256,256]{1,0:T(8,128)(2,1)} %get-tuple-element.23.rv) | copy-start | bytes 393220
  130.4 12.2 %all-to-all-start.5 = ((f32[8,8,256]{2,1,0:T(8,128)}), f32[8,8,256]{2,1,0:T(8,128)S(1)}, u32[]{:S(2)}, u32[]{:S(2)}) async-start(f32[8,8,256]{2,1,0:T(8,128)} %get-tuple-element.20), calls=%async_computation.5 | async-start | bytes 131072 | tf_op jit(solution)/shard_map/all_to_all | solution.py:264
  137.8 0.7 copy-start.2
  137.8 4.8 %copy-start.3 = (f32[128]{0:T(128)S(1)}, f32[128]{0:T(128)}, u32[]{:S(2)}) copy-start(f32[128]{0:T(128)} %param.26) | copy-start | bytes 1540
  142.6 1.4 copy-start
Sparse Core Ops, SparseCore 0:
  35.2 35.3 all-gather.4
  72.7 42.8 all-gather.6

commit v6 on v5

--- a/solution.py
+++ b/solution.py
@@ -338,12 +338,14 @@
 
     row_kv = lax.all_gather(kv, "y", axis=0)
     col_q = to_all(queries, "z")
-    weights = lax.all_gather(col_q[:, ROWS:, :], "y", axis=0)
+    cut = col_q[:, ROWS:, :]
+    weights = lax.all_gather(cut, "y", axis=0)
 
     first = initial_state.reshape(4, RD)
     first = jnp.concatenate([first[:, :SD], first[:, SD:]], axis=0)
+    arrived = to_all(states, SP)
     slices = call(scan_kernel, sds((NZ * NY, 8, SD), bf16), [SMEM, VMEM, VMEM], 1000000)(
-        ret_log_decay, to_all(states, SP), first
+        ret_log_decay, arrived, first
     )
     entering = to_all(slices, SP)
     inner = call(inner_kernel, sds((ROWS, RD), f32), [SMEM] + [VMEM] * 3, 2000000000)(
@@ -376,6 +378,7 @@
         [VMEM],
         10000000,
     )(parts)
+    squares, weights = lax.optimization_barrier((squares, weights))
     squares = to_all(squares, TP)
 
     ret_normed = call(retain_kernel, sds((ROWS, RD), bf16), [SMEM] + [VMEM] * 4, 100000000)(

time: 170 us -> 170 us (level)
  blocking collectives: 46.7 us -> 74.9 us
  waiting for transfers between devices: 36.1 us -> 15.5 us
  starting transfers between devices: 35.3 us -> 29 us
    all_to_all x4 -> x5, blocking collectives: 46.7 us -> 74.9 us  [to_all(): return lax.all_to_all(x, axis, 0, 0, tiled=True)]
    all_to_all x4 -> x3, waiting for transfers between devices: 35.6 us -> 14.9 us  [to_all(): return lax.all_to_all(x, axis, 0, 0, tiled=True)]
    all_to_all x4 -> x3, starting transfers between devices: 26.8 us -> 20.4 us  [to_all(): return lax.all_to_all(x, axis, 0, 0, tiled=True)]
  transfers between devices with their start and end apart: 7 -> 6, of which waited for: 4 -> 3; matrix products, arithmetic and copies ran while one was open for 2% -> 2% of each run, Pallas kernels for 13% -> 14%
where the time goes in v6:
time: 170 us; the launch traced here: 169 us
  blocking collectives  74.9 us (44%)
  Pallas kernels  30.1 us (18%)
  starting transfers between devices  29 us (17%)
  waiting for transfers between devices  15.5 us (9%)
  between operations  14.9 us (9%)
  other arithmetic  3.52 us (2%)
    all_to_all x5, blocking collectives, to_all(): return lax.all_to_all(x, axis, 0, 0, tiled=True)  74.9 us
    all_to_all x3, starting transfers between devices, to_all(): return lax.all_to_all(x, axis, 0, 0, tiled=True)  20.4 us
    all_to_all x3, waiting for transfers between devices, to_all(): return lax.all_to_all(x, axis, 0, 0, tiled=True)  14.9 us
    pallas_call x1, Pallas kernels, body(): parts = stick(pos, stick_offset, row_kv, col_q)  13.8 us
    ppermute x1, starting transfers between devices, body(): other = lax.ppermute(own, 'c', [(0, 1), (1, 0)])  8.49 us
    pallas_call x1, Pallas kernels, body(): ret_project(pos, ret_log_decay, own, other, cosine, sine, ret_query_w, re...  5.82 us
    pallas_call x1, Pallas kernels, body(): call(stick_project_kernel, (sds((ROWS, 2 * SD), bf16), sds((NZ, ROWS + 96...  4.73 us
  transfers between devices with their start and end apart: 6, of which 3 were waited for; matrix products, arithmetic and copies ran while one was open for 2% of the time, Pallas kernels for 14%

profile of v6, /device:TPU:1, one launch (start us, length us, event | category | flops | bytes accessed | tf_op | source)
XLA Modules:
  0.0 168.9 jit_solution(16938530842455680444)
XLA Ops:
  6.5 1.8 %shard_map.145 = bf16[4,264,256]{2,1,0:T(8,128)(2,1)} custom-call(bf16[256,256]{1,0:T(8,128)(2,1)} %inputs.1, bf16[256]{0:T(256)(128)(2,1)} %gain.1), custom_call_target="tpu_custom_call" | custom-call | flops 1000 | bytes 1048576 | tf_op jit(solution)/shard_map/pallas_call | solution.py:291
  8.3 11.9 %all_to_all.40.own = bf16[4,264,256]{2,1,0:T(8,128)(2,1)S(1)} all-to-all(bf16[4,264,256]{2,1,0:T(8,128)(2,1)} %shard_map.145), channel_id=1, replica_groups=mesh['z'=8,'y'=8,'x'=4,'c'=2] {'x'}, dimensions={0} | all-to-all | bytes 1081344 | tf_op jit(solution)/shard_map/all_to_all | solution.py:264
  20.2 8.5 %collective-permute-start = (bf16[4,264,256]{2,1,0:T(8,128)(2,1)S(1)}, bf16[4,264,256]{2,1,0:T(8,128)(2,1)}, u32[]{:S(2)}, u32[]{:S(2)}) collective-permute-start(bf16[4,264,256]{2,1,0:T(8,128)(2,1)S(1)} %all_to_all.40.own), channel_id=1, source_target_pairs={{0,1},{1,0},{2,3},{3,2},{4,5},{5,4},{6,7},{7,6},{8,9},{9,8},{10,11... | collective-permute-start | bytes 1622024 | tf_op jit(solution)/shard_map/ppermute | solution.py:295
  28.7 0.6 pad_add_fusion.pos
  29.3 0.6 pad_maximum_fusion.columns
  29.9 0.5 collective-permute-done.other
  30.3 4.7 %shard_map.146 = (bf16[256,256]{1,0:T(8,128)(2,1)}, bf16[8,352,128]{2,1,0:T(8,128)(2,1)}) custom-call(s32[3]{0:T(128)} %pad_add_fusion.pos, bf16[4,264,256]{2,1,0:T(8,128)(2,1)} %copy-done.6, bf16[4,264,256]{2,1,0:T(8,128)(2,1)} %collective-permute-done.other, bf16[96,128]{1,0:T(8,128)(2,1)} %pad_maximum_fusion.columns, bf16[2048,128]{1,0:T(8,128)(2,1)} %wq.2, ...), custom_call_target="tpu_custom_call" | custom-call | flops 400000000 | bytes 1048576 | tf_op jit(solution)/shard_map/pallas_call | solution.py:310
  35.1 0.0 all-gather.5.cloned.1.call-update
  35.1 0.0 all-gather.7.cloned.1.call-start
  35.2 27.9 %all_to_all.41.zq = bf16[8,352,128]{2,1,0:T(8,128)(2,1)S(1)} all-to-all(bf16[8,352,128]{2,1,0:T(8,128)(2,1)} %get-tuple-element.18), channel_id=1, replica_groups=mesh['z'=8,'y'=8,'x'=4,'c'=2] {'z'}, dimensions={0} | all-to-all | bytes 1441792 | tf_op jit(solution)/shard_map/all_to_all | solution.py:264
  63.1 0.8 slice.24
  63.8 0.0 all-gather.7.cloned.1.call-update
  65.2 1.3 multiply_sine_fusion
  66.5 5.8 %shard_map.148 = (bf16[64,8,128]{2,1,0:T(8,128)(2,1)}, bf16[256,256]{1,0:T(8,128)(2,1)}, bf16[256,256]{1,0:T(8,128)(2,1)}, bf16[256,256]{1,0:T(8,128)(2,1)}) custom-call(s32[3]{0:T(128)} %pad_add_fusion.pos, f32[1]{0:T(128)S(6)} %copy.17.lam, bf16[4,264,256]{2,1,0:T(8,128)(2,1)} %copy-done.6, bf16[4,264,256]{2,1,0:T(8,128)(2,1)} %collective-permute-done.other, ...), custom_call_target="tpu_custom_call" | custom-call | flops 6000000000 | bytes 1048576 | tf_op jit(solution)/shard_map/pallas_call | solution.py:327
  72.3 8.7 %all-to-all-start.2 = ((bf16[64,8,128]{2,1,0:T(8,128)(2,1)}), bf16[64,8,128]{2,1,0:T(8,128)(2,1)S(1)}, u32[]{:S(2)}, u32[]{:S(2)}) async-start(bf16[64,8,128]{2,1,0:T(8,128)(2,1)} %get-tuple-element.19), calls=%async_computation.2 | async-start | bytes 262144 | tf_op jit(solution)/shard_map/all_to_all | solution.py:264
  81.1 11.6 %all-to-all-done.2.states = bf16[64,8,128]{2,1,0:T(8,128)(2,1)S(1)} async-done(((bf16[64,8,128]{2,1,0:T(8,128)(2,1)}), bf16[64,8,128]{2,1,0:T(8,128)(2,1)S(1)}, u32[]{:S(2)}, u32[]{:S(2)}) %all-to-all-start.2) | async-done | bytes 131104 | tf_op jit(solution)/shard_map/all_to_all | solution.py:264
  92.7 0.8 shard_map.149
  93.4 4.6 %all-to-all-start.3 = ((bf16[64,8,128]{2,1,0:T(8,128)(2,1)}), bf16[64,8,128]{2,1,0:T(8,128)(2,1)S(1)}, u32[]{:S(2)}, u32[]{:S(2)}) async-start(bf16[64,8,128]{2,1,0:T(8,128)(2,1)} %shard_map.149), calls=%async_computation.3 | async-start | bytes 262144 | tf_op jit(solution)/shard_map/all_to_all | solution.py:264
  98.0 0.0 all-gather.5.cloned.1.call-done
  98.1 13.8 %shard_map.147 = bf16[8,264,128]{2,1,0:T(8,128)(2,1)} custom-call(s32[3]{0:T(128)} %pad_add_fusion.pos, f32[1]{0:T(128)S(6)} %copy.16.off, bf16[8,256,256]{2,1,0:T(8,128)(2,1)} %bitcast.16, bf16[8,352,128]{2,1,0:T(8,128)(2,1)} %copy-done.7), custom_call_target="tpu_custom_call" | custom-call | flops 4000000000 | bytes 1048576 | tf_op jit(solution)/shard_map/pallas_call | solution.py:371
  111.9 18.5 %all_to_all.42.parts = bf16[8,264,128]{2,1,0:T(8,128)(2,1)S(1)} all-to-all(bf16[8,264,128]{2,1,0:T(8,128)(2,1)} %shard_map.147), channel_id=1, replica_groups=mesh['z'=8,'y'=8,'x'=4,'c'=2] {'z'}, dimensions={0} | all-to-all | bytes 1081344 | tf_op jit(solution)/shard_map/all_to_all | solution.py:264
  130.4 1.3 shard_map.150
  131.7 7.1 %all-to-all-start.5 = ((f32[8,8,256]{2,1,0:T(8,128)}), f32[8,8,256]{2,1,0:T(8,128)S(1)}, u32[]{:S(2)}, u32[]{:S(2)}) async-start(f32[8,8,256]{2,1,0:T(8,128)} %get-tuple-element.23), calls=%async_computation.5 | async-start | bytes 131072 | tf_op jit(solution)/shard_map/all_to_all | solution.py:264
  138.9 0.4 shard_map.151.inner
  139.2 0.3 copy-done.2
  139.5 0.8 shard_map.152.ret
  140.3 3.3 %all-to-all-done.5.squares = f32[8,8,256]{2,1,0:T(8,128)S(1)} async-done(((f32[8,8,256]{2,1,0:T(8,128)}), f32[8,8,256]{2,1,0:T(8,128)S(1)}, u32[]{:S(2)}, u32[]{:S(2)}) %all-to-all-start.5) | async-done | bytes 65568 | tf_op jit(solution)/shard_map/all_to_all | solution.py:264
  143.7 0.8 shard_map.153
  144.5 5.0 %all_to_all.43 = bf16[2,4,32,2048]{3,2,1,0:T(8,128)(2,1)S(1)} all-to-all(bf16[2,4,32,2048]{3,2,1,0:T(8,128)(2,1)S(1)} %shard_map.153), channel_id=1, replica_groups=mesh['z'=8,'y'=8,'x'=4,'c'=2] {'c'}, dimensions={0} | all-to-all | bytes 2097152 | tf_op jit(solution)/shard_map/all_to_all | solution.py:264
  149.4 0.3 reduce_sum.24
  149.7 11.6 %all_to_all.44 = bf16[4,32,2048]{2,1,0:T(8,128)(2,1)S(1)} all-to-all(bf16[4,32,2048]{2,1,0:T(8,128)(2,1)S(1)} %reduce_sum.24), channel_id=1, replica_groups=mesh['z'=8,'y'=8,'x'=4,'c'=2] {'x'}, dimensions={0} | all-to-all | bytes 1048576 | tf_op jit(solution)/shard_map/all_to_all | solution.py:264
  161.4 0.7 reduce_sum.25
  (29 shorter events, 0.1 us)
Async XLA Ops:
  6.5 22.7 %copy-start.8 = (bf16[256,32]{0,1:T(8,128)(2,1)S(1)}, bf16[256,32]{0,1:T(8,128)(2,1)}, u32[]{:S(2)}) copy-start(bf16[256,32]{0,1:T(8,128)(2,1)} %param.29) | copy-start | bytes 49156
  6.5 22.7 %copy-start.9 = (bf16[128,32]{0,1:T(8,128)(2,1)S(1)}, bf16[128,32]{0,1:T(8,128)(2,1)}, u32[]{:S(2)}) copy-start(bf16[128,32]{0,1:T(8,128)(2,1)} %param.28) | copy-start | bytes 24580
  6.5 91.5 %all-gather.5.cloned.1.call-start = ((), (), s32[]{:S(2)}) async-start(), calls=%async_computation.8 | async-start | bytes 1179648 | tf_op jit(solution)/shard_map/all_gather | solution.py:339
  20.2 10.2 %copy-start.6 = (bf16[4,264,256]{2,1,0:T(8,128)(2,1)}, bf16[4,264,256]{2,1,0:T(8,128)(2,1)S(1)}, u32[]{:S(2)}) copy-start(bf16[4,264,256]{2,1,0:T(8,128)(2,1)S(1)} %all_to_all.40.own) | copy-start | bytes 1622020
  20.2 10.2 %collective-permute-start = (bf16[4,264,256]{2,1,0:T(8,128)(2,1)S(1)}, bf16[4,264,256]{2,1,0:T(8,128)(2,1)}, u32[]{:S(2)}, u32[]{:S(2)}) collective-permute-start(bf16[4,264,256]{2,1,0:T(8,128)(2,1)S(1)} %all_to_all.40.own), channel_id=1, source_target_pairs={{0,1},{1,0},{2,3},{3,2},{4,5},{5,4},{6,7},{7,6},{8,9},{9,8},{10,11... | collective-permute-start | bytes 1622024 | tf_op jit(solution)/shard_map/ppermute | solution.py:295
  35.1 96.6 %all-gather.7.cloned.1.call-start = ((), (), s32[]{:S(2)}) async-start(), calls=%async_computation.9 | async-start | bytes 1769472 | tf_op jit(solution)/shard_map/all_gather | solution.py:342
  63.1 9.2 %copy-start.7 = (bf16[8,352,128]{2,1,0:T(8,128)(2,1)}, bf16[8,352,128]{2,1,0:T(8,128)(2,1)S(1)}, u32[]{:S(2)}) copy-start(bf16[8,352,128]{2,1,0:T(8,128)(2,1)S(1)} %all_to_all.41.zq) | copy-start | bytes 2162692
  66.5 14.6 %copy-start.10 = (f32[1,4,256]{2,1,0:T(4,128)S(1)}, f32[1,4,256]{2,1,0:T(4,128)}, u32[]{:S(2)}) copy-start(f32[1,4,256]{2,1,0:T(4,128)} %param.25) | copy-start | bytes 12292
  72.3 20.4 %all-to-all-start.2 = ((bf16[64,8,128]{2,1,0:T(8,128)(2,1)}), bf16[64,8,128]{2,1,0:T(8,128)(2,1)S(1)}, u32[]{:S(2)}, u32[]{:S(2)}) async-start(bf16[64,8,128]{2,1,0:T(8,128)(2,1)} %get-tuple-element.19), calls=%async_computation.2 | async-start | bytes 262144 | tf_op jit(solution)/shard_map/all_to_all | solution.py:264
  93.4 18.4 %all-to-all-start.3 = ((bf16[64,8,128]{2,1,0:T(8,128)(2,1)}), bf16[64,8,128]{2,1,0:T(8,128)(2,1)S(1)}, u32[]{:S(2)}, u32[]{:S(2)}) async-start(bf16[64,8,128]{2,1,0:T(8,128)(2,1)} %shard_map.149), calls=%async_computation.3 | async-start | bytes 262144 | tf_op jit(solution)/shard_map/all_to_all | solution.py:264
  111.8 27.0 %copy-start.1 = (bf16[256,256]{1,0:T(8,128)(2,1)S(1)}, bf16[256,256]{1,0:T(8,128)(2,1)}, u32[]{:S(2)}) copy-start(bf16[256,256]{1,0:T(8,128)(2,1)} %get-tuple-element.24.tq) | copy-start | bytes 393220
  111.8 27.0 %copy-start.4 = (bf16[256,256]{1,0:T(8,128)(2,1)S(1)}, bf16[256,256]{1,0:T(8,128)(2,1)}, u32[]{:S(2)}) copy-start(bf16[256,256]{1,0:T(8,128)(2,1)} %get-tuple-element.25.tk) | copy-start | bytes 393220
  111.9 27.0 %copy-start.5 = (bf16[256,256]{1,0:T(8,128)(2,1)S(1)}, bf16[256,256]{1,0:T(8,128)(2,1)}, u32[]{:S(2)}) copy-start(bf16[256,256]{1,0:T(8,128)(2,1)} %get-tuple-element.26.rv) | copy-start | bytes 393220
  131.7 12.0 %all-to-all-start.5 = ((f32[8,8,256]{2,1,0:T(8,128)}), f32[8,8,256]{2,1,0:T(8,128)S(1)}, u32[]{:S(2)}, u32[]{:S(2)}) async-start(f32[8,8,256]{2,1,0:T(8,128)} %get-tuple-element.23), calls=%async_computation.5 | async-start | bytes 131072 | tf_op jit(solution)/shard_map/all_to_all | solution.py:264
  138.8 0.7 copy-start.2
  138.8 4.8 %copy-start = (bf16[64,96,128]{2,1,0:T(8,128)(2,1)S(1)}, bf16[64,96,128]{2,1,0:T(8,128)(2,1)}, u32[]{:S(2)}) copy-start(bf16[64,96,128]{2,1,0:T(8,128)(2,1)} %all-gather.7.cloned.1.call-done) | copy-start | bytes 4718596
  138.9 4.8 %copy-start.3 = (f32[128]{0:T(128)S(1)}, f32[128]{0:T(128)}, u32[]{:S(2)}) copy-start(f32[128]{0:T(128)} %param.26) | copy-start | bytes 1540
Sparse Core Ops, SparseCore 0:
  35.2 35.6 all-gather.4
  73.1 43.1 all-gather.6

commit v7 on v6

--- a/solution.py
+++ b/solution.py
@@ -140,18 +140,14 @@
 TALL = PAIR * ROWS
 
 
-def stick_kernel(pos, off, kvs, zq, out, upper, twice, split, acc, car, local, sems):
-    copies = [pltpu.make_async_copy(kvs.at[y], local.at[y], sems.at[y]) for y in range(NY)]
-    for copy in copies:
-        copy.start()
+def stick_kernel(pos, off, kvs, zq, out, upper, twice, split, acc, car):
     mine, col = pos[0], pos[1]
     c1 = (SD**-0.5) * LOG2E
     c2 = off[0] * LOG2E
     upper[...] = (iota((ROWS, ROWS), 0) > iota((ROWS, ROWS), 1)).astype(f32).astype(bf16)
     for y in range(NY):
-        copies[y].wait()
-        twice[y, :, :SD] = local[y, :, :SD]
-        twice[y, :, SD:] = local[y, :, :SD]
+        twice[y, :, :SD] = kvs[y, :, :SD]
+        twice[y, :, SD:] = kvs[y, :, :SD]
 
     def rows_of(c, masked):
         for k in range(PAIR):
@@ -177,7 +173,7 @@
             weight = jnp.exp2(power - (later + carry))
             if masked:
                 weight = jnp.where(allowed, weight, 0.0)
-            total = total + mm(weight.astype(bf16), local[y, :, SD:])
+            total = total + mm(weight.astype(bf16), kvs[y, :, SD:])
             carry = carry + (later[:, :1] + rounded[:, :1].astype(f32))
         acc[...] = total
         car[...] = jnp.broadcast_to(carry, (TALL, SD))
@@ -344,6 +340,7 @@
     first = initial_state.reshape(4, RD)
     first = jnp.concatenate([first[:, :SD], first[:, SD:]], axis=0)
     arrived = to_all(states, SP)
+    arrived, row_kv = lax.optimization_barrier((arrived, row_kv))
     slices = call(scan_kernel, sds((NZ * NY, 8, SD), bf16), [SMEM, VMEM, VMEM], 1000000)(
         ret_log_decay, arrived, first
     )
@@ -355,7 +352,7 @@
     stick = call(
         stick_kernel,
         sds((NZ, ROWS + 8, SD), bf16),
-        [SMEM, SMEM, HBM, VMEM],
+        [SMEM, SMEM, VMEM, VMEM],
         4000000000,
         [
             pltpu.VMEM((ROWS, ROWS), bf16),
@@ -363,10 +360,7 @@
             pltpu.VMEM((TALL, 2 * SD), bf16),
             pltpu.VMEM((TALL, SD), f32),
             pltpu.VMEM((TALL, SD), f32),
-            pltpu.VMEM((NY, ROWS, 2 * SD), bf16),
-            pltpu.SemaphoreType.DMA((NY,)),
         ],
-        WHOLE,
     )
     parts = stick(pos, stick_offset, row_kv, col_q)
     parts, entering = lax.optimization_barrier((parts, entering))

time: 170 us -> 167 us (0.982)
  Pallas kernels: 30.1 us -> 27.5 us
    pallas_call x1, Pallas kernels: 13.8 us -> 11.1 us  [body(): parts = stick(pos, stick_offset, row_kv, col_q)]
  transfers between devices with their start and end apart: 6 -> 6, of which waited for: 3 -> 3; matrix products, arithmetic and copies ran while one was open for 2% -> 2% of each run, Pallas kernels for 14% -> 12%
where the time goes in v7:
time: 167 us; the launch traced here: 166 us
  blocking collectives  73.4 us (44%)
  starting transfers between devices  29.4 us (18%)
  Pallas kernels  27.5 us (16%)
  waiting for transfers between devices  15.4 us (9%)
  between operations  14.9 us (9%)
  other arithmetic  3.54 us (2%)
  local copies, waits for them, and re-layouts  2.23 us (1%)
    all_to_all x5, blocking collectives, to_all(): return lax.all_to_all(x, axis, 0, 0, tiled=True)  73.4 us
    all_to_all x3, starting transfers between devices, to_all(): return lax.all_to_all(x, axis, 0, 0, tiled=True)  20.9 us
    all_to_all x3, waiting for transfers between devices, to_all(): return lax.all_to_all(x, axis, 0, 0, tiled=True)  14.9 us
    pallas_call x1, Pallas kernels, body(): parts = stick(pos, stick_offset, row_kv, col_q)  11.1 us
    ppermute x1, starting transfers between devices, body(): other = lax.ppermute(own, 'c', [(0, 1), (1, 0)])  8.49 us
    pallas_call x1, Pallas kernels, body(): ret_project(pos, ret_log_decay, own, other, cosine, sine, ret_query_w, re...  5.82 us
    pallas_call x1, Pallas kernels, body(): call(stick_project_kernel, (sds((ROWS, 2 * SD), bf16), sds((NZ, ROWS + 96...  4.73 us
  transfers between devices with their start and end apart: 6, of which 3 were waited for; matrix products, arithmetic and copies ran while one was open for 2% of the time, Pallas kernels for 12%

profile of v7, /device:TPU:1, one launch (start us, length us, event | category | flops | bytes accessed | tf_op | source)
XLA Modules:
  0.0 166.4 jit_solution(12154174132494317557)
XLA Ops:
  6.5 1.8 %shard_map.145 = bf16[4,264,256]{2,1,0:T(8,128)(2,1)} custom-call(bf16[256,256]{1,0:T(8,128)(2,1)} %inputs.1, bf16[256]{0:T(256)(128)(2,1)} %gain.1), custom_call_target="tpu_custom_call" | custom-call | flops 1000 | bytes 1048576 | tf_op jit(solution)/shard_map/pallas_call | solution.py:287
  8.3 11.9 %all_to_all.40.own = bf16[4,264,256]{2,1,0:T(8,128)(2,1)S(1)} all-to-all(bf16[4,264,256]{2,1,0:T(8,128)(2,1)} %shard_map.145), channel_id=1, replica_groups=mesh['z'=8,'y'=8,'x'=4,'c'=2] {'x'}, dimensions={0} | all-to-all | bytes 1081344 | tf_op jit(solution)/shard_map/all_to_all | solution.py:260
  20.2 8.5 %collective-permute-start = (bf16[4,264,256]{2,1,0:T(8,128)(2,1)S(1)}, bf16[4,264,256]{2,1,0:T(8,128)(2,1)}, u32[]{:S(2)}, u32[]{:S(2)}) collective-permute-start(bf16[4,264,256]{2,1,0:T(8,128)(2,1)S(1)} %all_to_all.40.own), channel_id=1, source_target_pairs={{0,1},{1,0},{2,3},{3,2},{4,5},{5,4},{6,7},{7,6},{8,9},{9,8},{10,11... | collective-permute-start | bytes 1622024 | tf_op jit(solution)/shard_map/ppermute | solution.py:291
  28.7 0.6 pad_add_fusion.pos
  29.3 0.6 pad_maximum_fusion.columns
  29.9 0.4 collective-permute-done.other
  30.3 4.7 %shard_map.147 = (bf16[256,256]{1,0:T(8,128)(2,1)}, bf16[8,352,128]{2,1,0:T(8,128)(2,1)}) custom-call(s32[3]{0:T(128)} %pad_add_fusion.pos, bf16[4,264,256]{2,1,0:T(8,128)(2,1)} %copy-done.8, bf16[4,264,256]{2,1,0:T(8,128)(2,1)} %collective-permute-done.other, bf16[96,128]{1,0:T(8,128)(2,1)} %pad_maximum_fusion.columns, bf16[2048,128]{1,0:T(8,128)(2,1)} %wq.3, ...), custom_call_target="tpu_custom_call" | custom-call | flops 400000000 | bytes 1048576 | tf_op jit(solution)/shard_map/pallas_call | solution.py:306
  35.1 0.0 all-gather.5.cloned.1.call-update
  35.1 0.0 all-gather.7.cloned.1.call-start
  35.2 27.9 %all_to_all.41.zq = bf16[8,352,128]{2,1,0:T(8,128)(2,1)S(1)} all-to-all(bf16[8,352,128]{2,1,0:T(8,128)(2,1)} %get-tuple-element.22), channel_id=1, replica_groups=mesh['z'=8,'y'=8,'x'=4,'c'=2] {'z'}, dimensions={0} | all-to-all | bytes 1441792 | tf_op jit(solution)/shard_map/all_to_all | solution.py:260
  63.1 0.7 slice.24
  63.7 0.0 all-gather.7.cloned.1.call-update
  65.1 1.2 multiply_sine_fusion
  66.4 5.8 %shard_map.146 = (bf16[64,8,128]{2,1,0:T(8,128)(2,1)}, bf16[256,256]{1,0:T(8,128)(2,1)}, bf16[256,256]{1,0:T(8,128)(2,1)}, bf16[256,256]{1,0:T(8,128)(2,1)}) custom-call(s32[3]{0:T(128)} %pad_add_fusion.pos, f32[1]{0:T(128)S(6)} %copy.17.lam, bf16[4,264,256]{2,1,0:T(8,128)(2,1)} %copy-done.8, bf16[4,264,256]{2,1,0:T(8,128)(2,1)} %collective-permute-done.other, ...), custom_call_target="tpu_custom_call" | custom-call | flops 6000000000 | bytes 1048576 | tf_op jit(solution)/shard_map/pallas_call | solution.py:323
  72.2 8.7 %all-to-all-start.1 = ((bf16[64,8,128]{2,1,0:T(8,128)(2,1)}), bf16[64,8,128]{2,1,0:T(8,128)(2,1)S(1)}, u32[]{:S(2)}, u32[]{:S(2)}) async-start(bf16[64,8,128]{2,1,0:T(8,128)(2,1)} %get-tuple-element.19), calls=%async_computation.1 | async-start | bytes 262144 | tf_op jit(solution)/shard_map/all_to_all | solution.py:260
  80.9 11.6 %all-to-all-done.1.states = bf16[64,8,128]{2,1,0:T(8,128)(2,1)S(1)} async-done(((bf16[64,8,128]{2,1,0:T(8,128)(2,1)}), bf16[64,8,128]{2,1,0:T(8,128)(2,1)S(1)}, u32[]{:S(2)}, u32[]{:S(2)}) %all-to-all-start.1) | async-done | bytes 131104 | tf_op jit(solution)/shard_map/all_to_all | solution.py:260
  92.5 0.8 shard_map.149
  93.3 4.6 %all-to-all-start.3 = ((bf16[64,8,128]{2,1,0:T(8,128)(2,1)}), bf16[64,8,128]{2,1,0:T(8,128)(2,1)S(1)}, u32[]{:S(2)}, u32[]{:S(2)}) async-start(bf16[64,8,128]{2,1,0:T(8,128)(2,1)} %shard_map.149), calls=%async_computation.3 | async-start | bytes 262144 | tf_op jit(solution)/shard_map/all_to_all | solution.py:260
  98.0 1.2 copy-done.5
  99.2 11.1 %shard_map.148 = bf16[8,264,128]{2,1,0:T(8,128)(2,1)S(1)} custom-call(s32[3]{0:T(128)S(1)} %copy-done.2, f32[1]{0:T(128)S(6)} %copy.16.off, bf16[8,256,256]{2,1,0:T(8,128)(2,1)S(1)} %bitcast.13, bf16[8,352,128]{2,1,0:T(8,128)(2,1)S(1)} %all_to_all.41.zq), custom_call_target="tpu_custom_call" | custom-call | flops 4000000000 | bytes 1048576 | tf_op jit(solution)/shard_map/pallas_call | solution.py:365
  110.4 17.1 %all_to_all.42.parts = bf16[8,264,128]{2,1,0:T(8,128)(2,1)S(1)} all-to-all(bf16[8,264,128]{2,1,0:T(8,128)(2,1)S(1)} %shard_map.148), channel_id=1, replica_groups=mesh['z'=8,'y'=8,'x'=4,'c'=2] {'z'}, dimensions={0} | all-to-all | bytes 1081344 | tf_op jit(solution)/shard_map/all_to_all | solution.py:260
  127.4 1.3 shard_map.150
  128.7 7.5 %all-to-all-start.5 = ((f32[8,8,256]{2,1,0:T(8,128)}), f32[8,8,256]{2,1,0:T(8,128)S(1)}, u32[]{:S(2)}, u32[]{:S(2)}) async-start(f32[8,8,256]{2,1,0:T(8,128)} %get-tuple-element.27), calls=%async_computation.5 | async-start | bytes 131072 | tf_op jit(solution)/shard_map/all_to_all | solution.py:260
  136.3 0.4 shard_map.151.inner
  136.7 0.3 copy-done.3
  137.0 0.8 shard_map.152.ret
  137.8 3.3 %all-to-all-done.5.squares = f32[8,8,256]{2,1,0:T(8,128)S(1)} async-done(((f32[8,8,256]{2,1,0:T(8,128)}), f32[8,8,256]{2,1,0:T(8,128)S(1)}, u32[]{:S(2)}, u32[]{:S(2)}) %all-to-all-start.5) | async-done | bytes 65568 | tf_op jit(solution)/shard_map/all_to_all | solution.py:260
  141.1 0.8 shard_map.153
  141.9 5.0 %all_to_all.43 = bf16[2,4,32,2048]{3,2,1,0:T(8,128)(2,1)S(1)} all-to-all(bf16[2,4,32,2048]{3,2,1,0:T(8,128)(2,1)S(1)} %shard_map.153), channel_id=1, replica_groups=mesh['z'=8,'y'=8,'x'=4,'c'=2] {'c'}, dimensions={0} | all-to-all | bytes 2097152 | tf_op jit(solution)/shard_map/all_to_all | solution.py:260
  146.9 0.3 reduce_sum.24
  147.2 11.6 %all_to_all.44 = bf16[4,32,2048]{2,1,0:T(8,128)(2,1)S(1)} all-to-all(bf16[4,32,2048]{2,1,0:T(8,128)(2,1)S(1)} %reduce_sum.24), channel_id=1, replica_groups=mesh['z'=8,'y'=8,'x'=4,'c'=2] {'x'}, dimensions={0} | all-to-all | bytes 1048576 | tf_op jit(solution)/shard_map/all_to_all | solution.py:260
  158.8 0.7 reduce_sum.25
  (31 shorter events, 0.1 us)
Async XLA Ops:
  6.5 22.8 %copy-start.9 = (bf16[256,32]{0,1:T(8,128)(2,1)S(1)}, bf16[256,32]{0,1:T(8,128)(2,1)}, u32[]{:S(2)}) copy-start(bf16[256,32]{0,1:T(8,128)(2,1)} %param.29) | copy-start | bytes 49156
  6.5 22.8 %copy-start.10 = (bf16[128,32]{0,1:T(8,128)(2,1)S(1)}, bf16[128,32]{0,1:T(8,128)(2,1)}, u32[]{:S(2)}) copy-start(bf16[128,32]{0,1:T(8,128)(2,1)} %param.28) | copy-start | bytes 24580
  6.5 86.0 %all-gather.5.cloned.1.call-start = ((), (), s32[]{:S(2)}) async-start(), calls=%async_computation.8 | async-start | bytes 1179648 | tf_op jit(solution)/shard_map/all_gather | solution.py:335
  20.2 10.2 %copy-start.8 = (bf16[4,264,256]{2,1,0:T(8,128)(2,1)}, bf16[4,264,256]{2,1,0:T(8,128)(2,1)S(1)}, u32[]{:S(2)}) copy-start(bf16[4,264,256]{2,1,0:T(8,128)(2,1)S(1)} %all_to_all.40.own) | copy-start | bytes 1622020
  20.2 10.2 %collective-permute-start = (bf16[4,264,256]{2,1,0:T(8,128)(2,1)S(1)}, bf16[4,264,256]{2,1,0:T(8,128)(2,1)}, u32[]{:S(2)}, u32[]{:S(2)}) collective-permute-start(bf16[4,264,256]{2,1,0:T(8,128)(2,1)S(1)} %all_to_all.40.own), channel_id=1, source_target_pairs={{0,1},{1,0},{2,3},{3,2},{4,5},{5,4},{6,7},{7,6},{8,9},{9,8},{10,11... | collective-permute-start | bytes 1622024 | tf_op jit(solution)/shard_map/ppermute | solution.py:291
  35.1 93.6 %all-gather.7.cloned.1.call-start = ((), (), s32[]{:S(2)}) async-start(), calls=%async_computation.9 | async-start | bytes 1769472 | tf_op jit(solution)/shard_map/all_gather | solution.py:338
  66.3 14.5 %copy-start.11 = (f32[1,4,256]{2,1,0:T(4,128)S(1)}, f32[1,4,256]{2,1,0:T(4,128)}, u32[]{:S(2)}) copy-start(f32[1,4,256]{2,1,0:T(4,128)} %param.25) | copy-start | bytes 12292
  66.4 31.6 %copy-start.2 = (s32[3]{0:T(128)S(1)}, s32[3]{0:T(128)}, u32[]{:S(2)}) copy-start(s32[3]{0:T(128)} %pad_add_fusion.pos) | copy-start | bytes 40
  72.2 20.4 %all-to-all-start.1 = ((bf16[64,8,128]{2,1,0:T(8,128)(2,1)}), bf16[64,8,128]{2,1,0:T(8,128)(2,1)S(1)}, u32[]{:S(2)}, u32[]{:S(2)}) async-start(bf16[64,8,128]{2,1,0:T(8,128)(2,1)} %get-tuple-element.19), calls=%async_computation.1 | async-start | bytes 262144 | tf_op jit(solution)/shard_map/all_to_all | solution.py:260
  93.3 17.0 %all-to-all-start.3 = ((bf16[64,8,128]{2,1,0:T(8,128)(2,1)}), bf16[64,8,128]{2,1,0:T(8,128)(2,1)S(1)}, u32[]{:S(2)}, u32[]{:S(2)}) async-start(bf16[64,8,128]{2,1,0:T(8,128)(2,1)} %shard_map.149), calls=%async_computation.3 | async-start | bytes 262144 | tf_op jit(solution)/shard_map/all_to_all | solution.py:260
  98.0 1.2 copy-start.5
  110.3 25.9 %copy-start.1 = (bf16[256,256]{1,0:T(8,128)(2,1)S(1)}, bf16[256,256]{1,0:T(8,128)(2,1)}, u32[]{:S(2)}) copy-start(bf16[256,256]{1,0:T(8,128)(2,1)} %get-tuple-element.28.tq) | copy-start | bytes 393220
  110.3 25.9 %copy-start.6 = (bf16[256,256]{1,0:T(8,128)(2,1)S(1)}, bf16[256,256]{1,0:T(8,128)(2,1)}, u32[]{:S(2)}) copy-start(bf16[256,256]{1,0:T(8,128)(2,1)} %get-tuple-element.29.tk) | copy-start | bytes 393220
  110.3 25.9 %copy-start.7 = (bf16[256,256]{1,0:T(8,128)(2,1)S(1)}, bf16[256,256]{1,0:T(8,128)(2,1)}, u32[]{:S(2)}) copy-start(bf16[256,256]{1,0:T(8,128)(2,1)} %get-tuple-element.30.rv) | copy-start | bytes 393220
  128.7 12.4 %all-to-all-start.5 = ((f32[8,8,256]{2,1,0:T(8,128)}), f32[8,8,256]{2,1,0:T(8,128)S(1)}, u32[]{:S(2)}, u32[]{:S(2)}) async-start(f32[8,8,256]{2,1,0:T(8,128)} %get-tuple-element.27), calls=%async_computation.5 | async-start | bytes 131072 | tf_op jit(solution)/shard_map/all_to_all | solution.py:260
  136.3 0.7 copy-start.3
  136.3 4.8 %copy-start = (bf16[64,96,128]{2,1,0:T(8,128)(2,1)S(1)}, bf16[64,96,128]{2,1,0:T(8,128)(2,1)}, u32[]{:S(2)}) copy-start(bf16[64,96,128]{2,1,0:T(8,128)(2,1)} %all-gather.7.cloned.1.call-done) | copy-start | bytes 4718596
  136.3 4.8 %copy-start.4 = (f32[128]{0:T(128)S(1)}, f32[128]{0:T(128)}, u32[]{:S(2)}) copy-start(f32[128]{0:T(128)} %param.26) | copy-start | bytes 1540
Sparse Core Ops, SparseCore 0:
  35.2 35.6 all-gather.4
  73.0 43.1 all-gather.6
